TPU v7x, 256 devices: a whole 4x4x8 slice. The times are simulated.
256 devices in a mesh: st: 64 (over z, y, core), tp: 4 (over x).
Axes of the slice: x: 4, y: 4, z: 8, core: 2. Of those that a mesh axis runs over, the one named last changes fastest.
Arguments:
- tokens: bfloat16 [24576, 2048], P('st', 'tp'), may hold values from -6 to 6
- cotangent: bfloat16 [24576, 1024], P('st', 'tp'), may hold values from -48 to 48
- mix_query: bfloat16 [24576, 1024], P('st', 'tp'), may hold values from -6 to 6
- mix_key: bfloat16 [24576, 1024], P('st', 'tp'), may hold values from -6 to 6
- mix_value: bfloat16 [24576, 1024], P('st', 'tp'), may hold values from -24 to 24
- beta_pre: float32 [8, 24576], P('tp', 'st'), may hold values from -9 to 9
- decay_pre: float32 [8, 24576], P('tp', 'st'), may hold values from -8 to 6
- decay_rate: float32 [8], P('tp'), may hold values from 0.001 to 0.06
- passages: bfloat16 [1024, 64, 2048], P('st'), may hold values from -16 to 16
- passage_ids: int32 [384, 4], P('st'), may hold values from 0 to 1023, as said below
- query_weight: bfloat16 [2048, 1024], P(None, 'tp'), may hold values from -0.125 to 0.125
- key_weight: bfloat16 [2048, 1024], P(None, 'tp'), may hold values from -0.125 to 0.125
- value_weight: bfloat16 [2048, 1024], P(None, 'tp'), may hold values from -0.125 to 0.125
- gate_weight: bfloat16 [4, 2048], P('tp'), may hold values from -0.125 to 0.125
Outputs:
- token_grad: bfloat16 [24576, 2048], P('st', 'tp')
- passage_grad: bfloat16 [1024, 64, 2048], P('st', None, 'tp')
- key_weight_grad: float32 [2048, 1024], P('st', 'tp')
Inputs may be any that keep to these rules, and one draw needn't show every extreme that they name: Passage p is stored on index p // 16 of st. The rows of passage_ids read by one index of st name at most 1 passages stored on any one index of st, and exactly 1 on some.
All inputs are finite; a program needn't handle non-finite values.
Results may differ from a plain program's by a relative error of at most 0.012.
The roundings to bfloat16 on the way count: a program that leaves them out, or rounds other values in their place, can miss the bound.
Values may be sent and summed in bfloat16 or wider, within the bound.
A program may use at most 128 MiB of HBM per device.

v0:
```python
import jax
import jax.numpy as jnp
from jax import lax
from jax.sharding import Mesh
from jax.sharding import PartitionSpec as P

SPAN = 64
ST = ("st_0", "st_1", "st_2")


NORM_FLOOR = 1.0
SCORE_GAIN = 4.0
CONTRACT_LAST = (((1,), (1,)), ((), ()))
CONTRACT_FIRST = (((0,), (0,)), ((), ()))


def joined_along(parts, dim):
    lengths = list(parts.shape[1:])
    lengths[dim] *= parts.shape[0]
    return jnp.moveaxis(parts, 0, dim).reshape(lengths)


def copy_for_each(shard, axis):
    copies = jnp.broadcast_to(shard, (lax.axis_size(axis), *shard.shape))
    return lax.all_to_all(copies, axis, split_axis=0, concat_axis=0, tiled=True)


def gather_directly(shard, axis, dim):
    return joined_along(copy_for_each(shard, axis), dim)


def in_blocks(shard, dim, devices):
    before, after = (shard.shape[:dim], shard.shape[dim + 1 :])
    return jnp.moveaxis(shard.reshape(*before, devices, -1, *after), dim, 0)


def sum_at_owner(shard, axis, dim):
    parts = in_blocks(shard, dim, lax.axis_size(axis))
    arrived = lax.all_to_all(parts, axis, split_axis=0, concat_axis=0, tiled=True)
    return arrived.astype(jnp.float32).sum(axis=0)


def sum_by_axis(shard, axes, dim):
    for axis in axes:
        shard = lax.psum_scatter(shard, axis, scatter_dimension=dim, tiled=True)
    return shard


def neumann_inverse(strict_part):
    span_size = strict_part.shape[-1]
    unit_eye = jnp.eye(span_size, dtype=jnp.float32)
    running = unit_eye - strict_part
    power_term = strict_part
    for _ in range(span_size.bit_length() - 2):
        power_term = jnp.einsum("...ij,...jk->...ik", power_term, power_term)
        running = jnp.einsum("...ij,...jk->...ik", running, unit_eye + power_term)
    return running


def delta_mixer(queries, keys_in, values_in, strength, log_decay):
    heads_n, length, key_dim = queries.shape
    blocks_n = length // SPAN

    def to_blocks(tensor):
        return tensor.reshape(heads_n, blocks_n, SPAN, *tensor.shape[2:])

    queries, keys_in, values_in = (to_blocks(queries), to_blocks(keys_in), to_blocks(values_in))
    strength, log_decay = (to_blocks(strength), to_blocks(log_decay))
    cumulative = jnp.cumsum(log_decay, axis=-1)
    position = jnp.arange(SPAN)
    inclusive = position[:, None] >= position[None, :]
    strictly = position[:, None] > position[None, :]
    spread = jnp.where(inclusive, cumulative[..., :, None] - cumulative[..., None, :], -jnp.inf)
    decay_map = jnp.exp(spread)
    key_gram = jnp.einsum("hncd,hnmd->hncm", keys_in, keys_in)
    strict_part = jnp.where(strictly, strength[..., :, None] * key_gram * decay_map, 0.0)
    inverse = neumann_inverse(strict_part)
    fresh_vals = jnp.einsum("hncm,hnme->hnce", inverse, values_in * strength[..., None])
    correction = jnp.einsum(
        "hncm,hnmd->hncd", inverse, keys_in * (strength * jnp.exp(cumulative))[..., None]
    )
    attend_map = jnp.where(
        inclusive, jnp.einsum("hncd,hnmd->hncm", queries, keys_in) * decay_map, 0.0
    )
    query_dec = queries * jnp.exp(cumulative)[..., None]
    key_dec = keys_in * jnp.exp(cumulative[..., -1:] - cumulative)[..., None]
    carry_decay = jnp.exp(cumulative[..., -1])

    def advance(memory_state, inputs):
        fresh_blk, correct_blk, attend_blk, query_blk, key_blk, decay_blk = inputs
        new_values = fresh_blk - jnp.einsum("hcd,hde->hce", correct_blk, memory_state)
        output = jnp.einsum("hcd,hde->hce", query_blk, memory_state) + jnp.einsum(
            "hcm,hme->hce", attend_blk, new_values
        )
        memory_state = memory_state * decay_blk[:, None, None] + jnp.einsum(
            "hcd,hce->hde", key_blk, new_values
        )
        return (memory_state, output)

    stacked = tuple(
        (
            jnp.moveaxis(tensor, 1, 0)
            for tensor in (fresh_vals, correction, attend_map, query_dec, key_dec, carry_decay)
        )
    )
    initial = jnp.zeros((heads_n, key_dim, values_in.shape[-1]), jnp.float32)
    _, outputs = lax.scan(advance, initial, stacked)
    return jnp.transpose(outputs, (1, 0, 2, 3)).reshape(heads_n, length, -1)


def mixer_output(query_raw, key_raw, value_raw, beta_raw, decay_raw, rate_vals):
    length = query_raw.shape[0]
    heads_n = beta_raw.shape[0]

    def heads_first(matrix):
        return jnp.transpose(matrix.astype(jnp.float32).reshape(length, heads_n, -1), (1, 0, 2))

    queries = heads_first(query_raw)
    keys_in = heads_first(key_raw)
    values_in = heads_first(value_raw)
    queries = (
        queries
        * lax.rsqrt(jnp.sum(queries * queries, axis=-1, keepdims=True) + NORM_FLOOR)
        * queries.shape[-1] ** (-0.5)
    )
    keys_in = keys_in * lax.rsqrt(jnp.sum(keys_in * keys_in, axis=-1, keepdims=True) + NORM_FLOOR)
    strength = jax.nn.sigmoid(beta_raw)
    log_decay = -rate_vals[:, None] * jax.nn.softplus(decay_raw)
    mixer_out = delta_mixer(queries, keys_in, values_in, strength, log_decay)
    return jnp.transpose(mixer_out, (1, 0, 2)).reshape(length, -1)


def request_slots(id_rows, pass_count):
    owners = id_rows // pass_count
    local_idx = id_rows % pass_count
    req_count = id_rows.shape[-1]
    req_order = jnp.arange(req_count, dtype=jnp.int32)
    earlier = (owners[..., :, None] == owners[..., None, :]) & (
        req_order[None, :] < req_order[:, None]
    )
    ranks = jnp.sum(earlier.astype(jnp.int32), axis=-1, dtype=jnp.int32)
    return (owners, local_idx, ranks)


def body(
    tokens,
    cotangent,
    mix_query,
    mix_key,
    mix_value,
    beta_pre,
    decay_pre,
    decay_rate,
    passages,
    passage_ids,
    query_weight,
    key_weight,
    value_weight,
    gate_weight,
):
    tok_rows = tokens.shape[0]
    model_width = query_weight.shape[0]
    head_dim = query_weight.shape[1]
    pass_local = passages.shape[0]
    span_rows = passages.shape[1]
    blocks_n = passage_ids.shape[0]
    per_block = passage_ids.shape[1]
    block_rows = tok_rows // blocks_n
    req_count = blocks_n * per_block
    st_count = lax.axis_size(ST)
    my_owner = lax.axis_index(ST)
    cap_count = max(1, req_count // st_count)
    slot_total = st_count * cap_count
    score_scale = SCORE_GAIN * head_dim ** (-0.5)
    req_order = jnp.arange(req_count, dtype=jnp.int32)
    every_id = gather_directly(passage_ids, ST, 0).reshape(st_count, req_count)
    all_owner, all_local, all_rank = request_slots(every_id, pass_local)
    cap_iota = jnp.arange(cap_count, dtype=jnp.int32)
    wanted = (all_owner == my_owner)[:, None, :] & (all_rank[:, None, :] == cap_iota[None, :, None])
    slot_used = jnp.any(wanted, axis=-1)
    slot_local = jnp.sum(jnp.where(wanted, all_local[:, None, :], 0), axis=-1, dtype=jnp.int32)
    flat_rows = passages.reshape(pass_local * span_rows, model_width)
    key_low = lax.optimization_barrier(
        jnp.dot(flat_rows, key_weight, preferred_element_type=jnp.float32).astype(jnp.bfloat16)
    )
    value_all = jnp.dot(flat_rows, value_weight, preferred_element_type=jnp.float32).astype(
        jnp.bfloat16
    )
    key_float = key_low.astype(jnp.float32)
    key_scale = lax.rsqrt(jnp.mean(key_float * key_float, axis=-1, keepdims=True) + NORM_FLOOR)
    key_hat = (key_float * key_scale).astype(jnp.bfloat16)
    packed = jnp.concatenate([key_hat, value_all], axis=-1).reshape(
        pass_local, span_rows, 2 * head_dim
    )
    send_rows = jnp.where(
        slot_used[:, :, None, None], packed[slot_local], jnp.zeros((), jnp.bfloat16)
    )
    arrived = lax.all_to_all(send_rows, ST, split_axis=0, concat_axis=0, tiled=True).reshape(
        slot_total, span_rows, 2 * head_dim
    )
    shard_piece = lax.all_gather(tokens, "tp", axis=1, tiled=True)
    query_acc = jnp.dot(shard_piece, query_weight, preferred_element_type=jnp.float32)
    gate_acc = lax.dot_general(
        shard_piece, gate_weight, CONTRACT_LAST, preferred_element_type=jnp.float32
    )
    query_low = lax.optimization_barrier(query_acc.astype(jnp.bfloat16))
    query_float = query_low.astype(jnp.float32)
    query_scale = lax.rsqrt(
        jnp.mean(query_float * query_float, axis=-1, keepdims=True) + NORM_FLOOR
    )
    query_hat = (query_float * query_scale).astype(jnp.bfloat16)
    gate_open = jax.nn.sigmoid(gate_acc[:, 0])
    mixer_out = mixer_output(mix_query, mix_key, mix_value, beta_pre, decay_pre, decay_rate)
    own_owner, own_local, own_rank = request_slots(passage_ids.reshape(req_count), pass_local)
    slot_of = own_owner * cap_count + own_rank
    mine_rows = arrived[slot_of]
    key_rows = mine_rows[:, :, :head_dim].reshape(blocks_n, per_block * span_rows, head_dim)
    value_rows = mine_rows[:, :, head_dim:].reshape(blocks_n, per_block * span_rows, head_dim)
    query_blocks = query_hat.reshape(blocks_n, block_rows, head_dim)
    scores = (
        jnp.einsum("bid,bjd->bij", query_blocks, key_rows, preferred_element_type=jnp.float32)
        * score_scale
    )
    exp_scores = jnp.exp(scores)
    attn_probs = exp_scores / jnp.sum(exp_scores, axis=-1, keepdims=True)
    probs_low = attn_probs.astype(jnp.bfloat16)
    retrieved = jnp.einsum(
        "bij,bjd->bid", probs_low, value_rows, preferred_element_type=jnp.float32
    ).reshape(tok_rows, head_dim)
    grad_out = cotangent.astype(jnp.float32)
    grad_ret = (gate_open[:, None] * grad_out).astype(jnp.bfloat16)
    gate_grad = jnp.sum(grad_out * (retrieved - mixer_out), axis=-1) * gate_open * (1.0 - gate_open)
    grad_blocks = grad_ret.reshape(blocks_n, block_rows, head_dim)
    grad_probs = jnp.einsum(
        "bid,bjd->bij", grad_blocks, value_rows, preferred_element_type=jnp.float32
    )
    score_grad = (
        attn_probs * (grad_probs - jnp.sum(grad_probs * attn_probs, axis=-1, keepdims=True))
    ).astype(jnp.bfloat16)
    slot_match = slot_of[None, :] == jnp.arange(slot_total, dtype=jnp.int32)[:, None]
    slot_filled = jnp.any(slot_match, axis=-1)
    slot_req = jnp.sum(jnp.where(slot_match, req_order[None, :], 0), axis=-1, dtype=jnp.int32)
    key_term = (
        score_scale
        * jnp.einsum("bij,bid->bjd", score_grad, query_blocks, preferred_element_type=jnp.float32)
    ).astype(jnp.bfloat16)
    value_term = jnp.einsum(
        "bij,bid->bjd", probs_low, grad_blocks, preferred_element_type=jnp.float32
    ).astype(jnp.bfloat16)
    reply_rows = jnp.concatenate([key_term, value_term], axis=-1).reshape(
        req_count, span_rows, 2 * head_dim
    )
    reply_slots = jnp.where(
        slot_filled[:, None, None], reply_rows[slot_req], jnp.zeros((), jnp.bfloat16)
    ).reshape(st_count, cap_count, span_rows, 2 * head_dim)
    reply_back = lax.all_to_all(reply_slots, ST, split_axis=0, concat_axis=0, tiled=True).astype(
        jnp.float32
    )
    key_part = reply_back[..., :head_dim]
    value_part = reply_back[..., head_dim:]
    qhat_grad = score_scale * jnp.einsum(
        "bij,bjd->bid", score_grad, key_rows, preferred_element_type=jnp.float32
    ).reshape(tok_rows, head_dim)
    query_grad = (
        query_scale * qhat_grad
        - query_scale**3 * query_float * jnp.mean(query_float * qhat_grad, axis=-1, keepdims=True)
    ).astype(jnp.bfloat16)
    token_term = (
        lax.dot_general(query_grad, query_weight, CONTRACT_LAST, preferred_element_type=jnp.float32)
        + gate_grad[:, None] * gate_weight[0].astype(jnp.float32)[None, :]
    )
    token_grad = sum_at_owner(token_term.astype(jnp.bfloat16), "tp", 1).astype(jnp.bfloat16)
    pass_iota = jnp.arange(pass_local, dtype=jnp.int32)
    onehot = (
        (slot_local.reshape(slot_total)[None, :] == pass_iota[:, None])
        & slot_used.reshape(slot_total)[None, :]
    ).astype(jnp.float32)
    key_grad_hat = jnp.dot(onehot, key_part.reshape(slot_total, span_rows * head_dim)).reshape(
        pass_local * span_rows, head_dim
    )
    value_grad_sum = jnp.dot(onehot, value_part.reshape(slot_total, span_rows * head_dim)).reshape(
        pass_local * span_rows, head_dim
    )
    key_grad = (
        key_scale * key_grad_hat
        - key_scale**3 * key_float * jnp.mean(key_float * key_grad_hat, axis=-1, keepdims=True)
    ).astype(jnp.bfloat16)
    value_grad_low = value_grad_sum.astype(jnp.bfloat16)
    row_term = lax.dot_general(
        key_grad, key_weight, CONTRACT_LAST, preferred_element_type=jnp.float32
    ) + lax.dot_general(
        value_grad_low, value_weight, CONTRACT_LAST, preferred_element_type=jnp.float32
    )
    passage_grad = sum_at_owner(
        row_term.reshape(pass_local, span_rows, model_width).astype(jnp.bfloat16), "tp", 2
    ).astype(jnp.bfloat16)
    weight_term = lax.dot_general(
        flat_rows, key_grad, CONTRACT_FIRST, preferred_element_type=jnp.float32
    )
    key_weight_grad = sum_by_axis(weight_term, ST, 0)
    return (token_grad, passage_grad, key_weight_grad)


def solution(mesh):
    torus = Mesh(mesh.devices.reshape(8, 4, 2, mesh.shape["tp"]), ("st_0", "st_1", "st_2", "tp"))
    return jax.shard_map(
        body,
        mesh=torus,
        in_specs=(
            P(ST, "tp"),
            P(ST, "tp"),
            P(ST, "tp"),
            P(ST, "tp"),
            P(ST, "tp"),
            P("tp", ST),
            P("tp", ST),
            P("tp"),
            P(ST, None, None),
            P(ST, None),
            P(None, "tp"),
            P(None, "tp"),
            P(None, "tp"),
            P("tp", None),
        ),
        out_specs=(P(ST, "tp"), P(ST, None, "tp"), P(ST, "tp")),
        check_vma=False,
    )
```

profile of v0, /device:TPU:2, one launch (start us, length us, event | category | flops | bytes accessed | tf_op | source)
XLA Modules:
  0.0 398.1 jit_solution(1694725914471764700)
XLA Ops:
  9.3 12.4 %all-to-all-start = ((s32[64,6,4]{1,2,0:T(4,128)}), s32[64,6,4]{1,2,0:T(4,128)}, u32[]{:S(2)}, u32[]{:S(2)}) async-start(s32[64,6,4]{1,2,0:T(4,128)} %broadcast_in_dim.61), calls=%async_computation | async-start | bytes 262144 | tf_op jit(solution)/shard_map/all_to_all | solution.py:25
  33.1 3.9 convolution_convert_fusion.2
  47.2 2.8 gather_fusion
  50.0 4.5 %fusion.25 = bf16[64,1,64,512]{3,2,1,0:T(8,128)(2,1)} fusion(bf16[64,64,512]{2,1,0:T(8,128)(2,1)} %gather_fusion, pred[64]{0:T(512)(128)(4,1)S(1)} %copy-done.18), kind=kLoop, calls=%fused_computation.36 | loop fusion | flops 2097152 | bytes 8388672 | tf_op jit(solution)/shard_map/jit(_where)/select_n | solution.py:195
  54.5 10.7 %all-to-all-start.1 = ((bf16[64,1,64,512]{3,2,1,0:T(8,128)(2,1)}), bf16[64,1,64,512]{3,2,1,0:T(8,128)(2,1)}, u32[]{:S(2)}, u32[]{:S(2)}) async-start(bf16[64,1,64,512]{3,2,1,0:T(8,128)(2,1)} %fusion.25), calls=%async_computation.1 | async-start | bytes 8388608 | tf_op jit(solution)/shard_map/all_to_all | solution.py:198
  65.2 26.3 %while.13 = (s32[]{:T(128)}, f32[2,128,128]{2,1,0:T(8,128)S(1)}, f32[6,2,64,128]{3,2,0,1:T(8,128)S(1)}, f32[6,2]{1,0:T(8,128)}, bf16[6,2,64,128]{3,2,0,1:T(8,128...) while((s32[]{:T(128)}, f32[2,128,128]{2,1,0:T(8,128)S(1)}, ...), condition=%wide.region_13.14_spmd.clone, body=%wide.region_12.13_spmd.clone.sunk | while | flops 14893059 | bytes 1018532 | solution.py:107
  95.0 2.4 convolution_convert_fusion.4
  98.8 62.5 %all-to-all-done.1 = bf16[64,1,64,512]{3,2,1,0:T(8,128)(2,1)} async-done(((bf16[64,1,64,512]{3,2,1,0:T(8,128)(2,1)}), bf16[64,1,64,512]{3,2,1,0:T(8,128)(2,1)}, u32[]{:S(2)}, u32[]{:S(2)}) %all-to-all-start.1) | async-done | bytes 4194336 | tf_op jit(solution)/shard_map/all_to_all | solution.py:198
  161.3 3.0 gather_fusion.1
  167.9 2.4 fusion.78
  170.4 2.5 fusion.44
  172.8 2.6 convolution_convert_fusion.1
  181.1 2.9 gather_fusion.2
  184.0 4.5 %fusion.24 = bf16[64,1,64,512]{3,2,1,0:T(8,128)(2,1)} fusion(bf16[64,64,512]{2,1,0:T(8,128)(2,1)} %gather_fusion.2, pred[64]{0:T(512)(128)(4,1)S(1)} %copy-done.26), kind=kLoop, calls=%fused_computation.34 | loop fusion | flops 2097152 | bytes 8388672 | tf_op jit(solution)/shard_map/jit(_where)/select_n | solution.py:253
  188.5 5.8 %all-to-all-start.3 = ((bf16[64,1,64,512]{3,2,1,0:T(8,128)(2,1)}), bf16[64,1,64,512]{3,2,1,0:T(8,128)(2,1)}, u32[]{:S(2)}, u32[]{:S(2)}) async-start(bf16[64,1,64,512]{3,2,1,0:T(8,128)(2,1)} %fusion.24), calls=%async_computation.3 | async-start | bytes 8388608 | tf_op jit(solution)/shard_map/all_to_all | solution.py:256
  195.1 95.5 %all-to-all-done.3 = bf16[64,1,64,512]{3,2,1,0:T(8,128)(2,1)} async-done(((bf16[64,1,64,512]{3,2,1,0:T(8,128)(2,1)}), bf16[64,1,64,512]{3,2,1,0:T(8,128)(2,1)}, u32[]{:S(2)}, u32[]{:S(2)}) %all-to-all-start.3) | async-done | bytes 4194336 | tf_op jit(solution)/shard_map/all_to_all | solution.py:256
  290.6 4.1 %fusion.106 = (bf16[64,1,64,256]{3,2,1,0:T(8,128)(2,1)}, bf16[64,1,64,256]{3,2,1,0:T(8,128)(2,1)S(1)}) fusion(bf16[64,1,64,512]{3,2,1,0:T(8,128)(2,1)} %all-to-all-done.3), kind=kLoop, calls=%fused_computation.199 | loop fusion | bytes 8388608 | tf_op jit(solution)/shard_map/slice | solution.py:260
  299.0 5.0 %convolution_bitcast_fusion = f32[2048,256]{0,1:T(8,128)} fusion(bf16[1024,2048]{1,0:T(8,128)(2,1)} %bitcast.234, bf16[1024,256]{1,0:T(8,128)(2,1)S(1)} %convolution_convert_fusion.3, f32[1024,256]{1,0:T(8,128)S(1)} %reshape.488, f32[1024]{0:T(1024)S(1)} %broadcast_multiply_fusion, f32[1024]{0:T(1024)S(1)} %get-tuple-element.194, ...), kind=kOutput, calls=%fused_computation.39 | convolution fusion | flops 1075314688 | bytes 7876608 | tf_op jit(solution)/shard_map/dot_general | solution.py:297
  304.1 1.8 add_convert_fusion.1
  307.3 4.9 %all-to-all-start.2 = ((bf16[4,384,512]{2,1,0:T(8,128)(2,1)}), bf16[4,384,512]{2,1,0:T(8,128)(2,1)}, u32[]{:S(2)}, u32[]{:S(2)}) async-start(bf16[4,384,512]{2,1,0:T(8,128)(2,1)} %bitcast.232), calls=%async_computation.2 | async-start | bytes 3145728 | tf_op jit(solution)/shard_map/all_to_all | solution.py:39
  312.1 2.9 copy.213
  317.5 1.9 fusion.110
  319.4 3.3 add_convert_fusion
  322.7 7.8 %convert_element_type.117 = bf16[16,64,4,512]{3,2,1,0:T(4,128)(2,1)} reshape(bf16[1024,2048]{1,0:T(8,128)(2,1)} %add_convert_fusion) | data formatting | bytes 8388608 | tf_op jit(solution)/shard_map/convert_element_type | solution.py:295
  330.5 5.1 %copy.216 = bf16[16,64,4,512]{3,1,0,2:T(8,128)(2,1)} copy(bf16[16,64,4,512]{3,2,1,0:T(4,128)(2,1)} %convert_element_type.117) | data formatting | bytes 8388608 | tf_op jit(solution)/shard_map/convert_element_type | solution.py:295
  335.7 5.1 %all-to-all-start.4 = ((bf16[4,16,64,512]{3,2,1,0:T(8,128)(2,1)}), bf16[4,16,64,512]{3,2,1,0:T(8,128)(2,1)}, u32[]{:S(2)}, u32[]{:S(2)}) async-start(bf16[4,16,64,512]{3,2,1,0:T(8,128)(2,1)} %bitcast.221), calls=%async_computation.4 | async-start | bytes 8388608 | tf_op jit(solution)/shard_map/all_to_all | solution.py:39
  340.8 2.3 reduce-scatter.8.cloned.1.call-done
  343.0 1.8 copy.190
  344.9 23.2 %reduce-scatter.10.cloned.1.call-done = f32[64,256]{1,0:T(8,128)} async-done(((f32[256,256]{1,0:T(8,128)}), f32[64,256]{1,0:T(8,128)}) %reduce-scatter.10.cloned.1.call-update) | async-done | bytes 65552
  368.1 2.5 reduce_sum.160
  370.6 16.8 %all-to-all-done.4 = bf16[4,16,64,512]{3,2,1,0:T(8,128)(2,1)} async-done(((bf16[4,16,64,512]{3,2,1,0:T(8,128)(2,1)}), bf16[4,16,64,512]{3,2,1,0:T(8,128)(2,1)}, u32[]{:S(2)}, u32[]{:S(2)}) %all-to-all-start.4) | async-done | bytes 4194336 | tf_op jit(solution)/shard_map/all_to_all | solution.py:39
  387.3 4.2 %reduce_sum.164 = bf16[16,64,512]{2,1,0:T(8,128)(2,1)} reduce(bf16[4,16,64,512]{3,2,1,0:T(8,128)(2,1)} %all-to-all-done.4, bf16[]{:T(256)} %constant.112.clone.1), dimensions={0}, to_apply=%region_19.20 | reduce | flops 1572864 | bytes 5242882 | tf_op jit(solution)/shard_map/reduce_sum | solution.py:40
  (191 shorter events, 72.7 us)
Async XLA Ops:
  7.2 29.8 %copy-start = (bf16[2048,256]{1,0:T(8,128)(2,1)S(1)}, bf16[2048,256]{1,0:T(8,128)(2,1)}, u32[]{:S(2)}) copy-start(bf16[2048,256]{1,0:T(8,128)(2,1)} %param.27) | copy-start | bytes 3145732
  7.2 87.8 %all-gather.2.cloned.1.call-start = ((), (), s32[]{:S(2)}) async-start(), calls=%async_computation.8 | async-start | bytes 1966080 | tf_op jit(solution)/shard_map/all_gather | solution.py:201
  9.3 32.9 %all-to-all-start = ((s32[64,6,4]{1,2,0:T(4,128)}), s32[64,6,4]{1,2,0:T(4,128)}, u32[]{:S(2)}, u32[]{:S(2)}) async-start(s32[64,6,4]{1,2,0:T(4,128)} %broadcast_in_dim.61), calls=%async_computation | async-start | bytes 262144 | tf_op jit(solution)/shard_map/all_to_all | solution.py:25
  21.7 7.4 %copy-start.12 = (pred[64,64]{1,0:T(8,128)(4,1)}, pred[64,64]{1,0:T(8,128)(4,1)S(1)}, u32[]{:S(2)}) copy-start(pred[64,64]{1,0:T(8,128)(4,1)S(1)} %get-tuple-element.203) | copy-start | bytes 12292
  33.0 3.9 copy-start.3
  37.0 1.7 copy-start.13
  37.0 2.7 copy-start.16
  37.0 2.6 copy-start.17
  47.2 2.8 copy-start.18
  54.5 106.8 %all-to-all-start.1 = ((bf16[64,1,64,512]{3,2,1,0:T(8,128)(2,1)}), bf16[64,1,64,512]{3,2,1,0:T(8,128)(2,1)}, u32[]{:S(2)}, u32[]{:S(2)}) async-start(bf16[64,1,64,512]{3,2,1,0:T(8,128)(2,1)} %fusion.25), calls=%async_computation.1 | async-start | bytes 8388608 | tf_op jit(solution)/shard_map/all_to_all | solution.py:198
  65.2 26.3 %copy-start.20 = (s32[6,4]{0,1:T(4,128)S(1)}, s32[6,4]{0,1:T(4,128)}, u32[]{:S(2)}) copy-start(s32[6,4]{0,1:T(4,128)} %param.25) | copy-start | bytes 292
  91.5 6.0 %copy-start.14 = (bf16[1,2048]{1,0:T(2,128)(2,1)S(1)}, bf16[1,2048]{1,0:T(2,128)(2,1)}, u32[]{:S(2)}) copy-start(bf16[1,2048]{1,0:T(2,128)(2,1)} %param.29) | copy-start | bytes 12292
  95.0 2.6 copy-start.7
  165.3 5.1 %copy-start.8 = (f32[384,256]{1,0:T(8,128)S(1)}, f32[384,256]{1,0:T(8,128)}, u32[]{:S(2)}) copy-start(f32[384,256]{1,0:T(8,128)} %copy.183) | copy-start | bytes 1179652
  167.3 8.1 %copy-start.4 = (bf16[24,64,256]{2,1,0:T(8,128)(2,1)S(1)}, bf16[24,64,256]{2,1,0:T(8,128)(2,1)}, u32[]{:S(2)}) copy-start(bf16[24,64,256]{2,1,0:T(8,128)(2,1)} %get-tuple-element.187) | copy-start | bytes 2359300
  175.4 2.7 copy-start.10
  181.1 2.9 copy-start.26
  188.5 5.9 %copy-start.15 = (bf16[1,2048]{1,0:T(2,128)(2,1)S(1)}, bf16[1,2048]{1,0:T(2,128)(2,1)}, u32[]{:S(2)}) copy-start(bf16[1,2048]{1,0:T(2,128)(2,1)} %param.29) | copy-start | bytes 12292
  188.5 5.9 %copy-start.2 = (bf16[24,64,256]{2,1,0:T(8,128)(2,1)S(1)}, bf16[24,64,256]{2,1,0:T(8,128)(2,1)}, u32[]{:S(2)}) copy-start(bf16[24,64,256]{2,1,0:T(8,128)(2,1)} %copy-done.1) | copy-start | bytes 2359300
  188.5 5.9 %copy-start.6 = (bf16[6,64,256]{2,1,0:T(8,128)(2,1)S(1)}, bf16[6,64,256]{2,1,0:T(8,128)(2,1)}, u32[]{:S(2)}) copy-start(bf16[6,64,256]{2,1,0:T(8,128)(2,1)} %copy-done.5) | copy-start | bytes 589828
  188.5 6.4 %copy-start.22 = (f32[384]{0:T(512)S(1)}, f32[384]{0:T(512)}, u32[]{:S(2)}) copy-start(f32[384]{0:T(512)} %get-tuple-element.196) | copy-start | bytes 4612
  188.5 6.4 %copy-start.23 = (f32[384]{0:T(512)S(1)}, f32[384]{0:T(512)}, u32[]{:S(2)}) copy-start(f32[384]{0:T(512)} %get-tuple-element.197) | copy-start | bytes 4612
  188.5 102.1 %all-to-all-start.3 = ((bf16[64,1,64,512]{3,2,1,0:T(8,128)(2,1)}), bf16[64,1,64,512]{3,2,1,0:T(8,128)(2,1)}, u32[]{:S(2)}, u32[]{:S(2)}) async-start(bf16[64,1,64,512]{3,2,1,0:T(8,128)(2,1)} %fusion.24), calls=%async_computation.3 | async-start | bytes 8388608 | tf_op jit(solution)/shard_map/all_to_all | solution.py:256
  194.4 148.7 %reduce-scatter.8.cloned.1.call-start = ((), (), s32[]{:S(2)}) async-start(), calls=%async_computation.9 | async-start | bytes 2359296 | tf_op jit(solution)/shard_map/reduce_scatter | solution.py:45
  294.7 1.3 copy-start.19
  294.7 1.3 copy-start.25
  299.0 5.1 %copy-start.21 = (f32[384]{0:T(512)S(1)}, f32[384]{0:T(512)}, u32[]{:S(2)}) copy-start(f32[384]{0:T(512)} %get-tuple-element.189) | copy-start | bytes 4612
  307.3 28.4 %all-to-all-start.2 = ((bf16[4,384,512]{2,1,0:T(8,128)(2,1)}), bf16[4,384,512]{2,1,0:T(8,128)(2,1)}, u32[]{:S(2)}, u32[]{:S(2)}) async-start(bf16[4,384,512]{2,1,0:T(8,128)(2,1)} %bitcast.232), calls=%async_computation.2 | async-start | bytes 3145728 | tf_op jit(solution)/shard_map/all_to_all | solution.py:39
  317.5 1.9 copy-start.9
  335.7 51.7 %all-to-all-start.4 = ((bf16[4,16,64,512]{3,2,1,0:T(8,128)(2,1)}), bf16[4,16,64,512]{3,2,1,0:T(8,128)(2,1)}, u32[]{:S(2)}, u32[]{:S(2)}) async-start(bf16[4,16,64,512]{3,2,1,0:T(8,128)(2,1)} %bitcast.221), calls=%async_computation.4 | async-start | bytes 8388608 | tf_op jit(solution)/shard_map/all_to_all | solution.py:39
  340.8 27.3 %reduce-scatter.10.cloned.1.call-start = ((), (), s32[]{:S(2)}) async-start(), calls=%async_computation.10 | async-start | bytes 327680
  344.8 46.7 %reduce-scatter.12.cloned.1.call-start = ((), (), s32[]{:S(2)}) async-start(), calls=%async_computation.11 | async-start | bytes 98304
  (4 other events, 2.9 us)
Sparse Core Ops, SparseCore 0:
  9.8 30.9 all-gather.1
  304.2 38.7 reduce-scatter.7
  346.1 21.8 reduce-scatter.9
  370.9 12.5 reduce-scatter.11
where the time goes:
time: 402 us; the launch traced here: 398 us
  waiting for transfers between devices  201 us (50%)
  matrix products  56.4 us (14%)
  local copies, waits for them, and re-layouts  55.7 us (14%)
  starting transfers between devices  39 us (10%)
  other arithmetic  31.7 us (8%)
  between operations  14.4 us (4%)
    all_to_all x1, waiting for transfers between devices, body(): lax.all_to_all(reply_slots, ST, split_axis=0, concat_axis=0, tiled=True)  95.5 us
    all_to_all x1, waiting for transfers between devices, body(): lax.all_to_all(send_rows, ST, split_axis=0, concat_axis=0, tiled=True)  62.5 us
    unnamed x6, waiting for transfers between devices  23.9 us
    all_to_all x2, waiting for transfers between devices, sum_at_owner(): lax.all_to_all(parts, axis, split_axis=0, concat_axis=0, tiled=True)  16.8 us
    convert_element_type x2, local copies, waits for them, and re-layouts, body(): row_term.reshape(pass_local, span_rows, model_width).astype(jnp.bfloat16)  13 us
    unnamed x61, local copies, waits for them, and re-layouts  12.5 us
    all_to_all x1, starting transfers between devices, copy_for_each(): return lax.all_to_all(copies, axis, split_axis=0, concat_axis=0, tiled=True)  12.4 us
    all_to_all x1, starting transfers between devices, body(): lax.all_to_all(send_rows, ST, split_axis=0, concat_axis=0, tiled=True)  10.7 us
  transfers between devices with their start and end apart: 9, of which 5 were waited for; matrix products, arithmetic and copies ran while one was open for 26% of the time, Pallas kernels for 0%

commit v1 on v0

v1 whole, which is shorter than its diff:
```python
import functools

import jax
import jax.numpy as jnp
from jax import lax
from jax.experimental import pallas as pl
from jax.experimental.pallas import tpu as pltpu
from jax.sharding import Mesh
from jax.sharding import PartitionSpec as P

SPAN = 64
ST = ("st_0", "st_1", "st_2")


NORM_FLOOR = 1.0
SCORE_GAIN = 4.0
CONTRACT_LAST = (((1,), (1,)), ((), ()))
CONTRACT_FIRST = (((0,), (0,)), ((), ()))


AXES = {"st_0": 8, "st_1": 4, "st_2": 2, "tp": 4}
MESH_ID = pl.DeviceIdType.MESH


def ring_starts(job, x_ref, o_ref, sems):
    axis, n, chunks = job["axis"], AXES[job["axis"]], job.get("chunks", 1)
    rows = x_ref.shape[0]
    me = lax.axis_index(axis)
    step_rows = rows // chunks

    def part(k, d, ch):
        lo, size = ch * step_rows, step_rows
        if k == n // 2 - 1:
            size = step_rows // 2
            lo = lo + (size if d else 0)
        return pl.ds(lo, size)

    def copy(k, d, ch):
        sgn = -1 if d else 1
        origin = lax.rem(me - sgn * k + 2 * n, n)
        rng = part(k, d, ch)
        src = x_ref.at[rng] if k == 0 else o_ref.at[origin, rng]
        return pltpu.make_async_remote_copy(
            src_ref=src, dst_ref=o_ref.at[origin, rng],
            send_sem=sems.at[0, d, k * chunks + ch], recv_sem=sems.at[1, d, k * chunks + ch],
            device_id={axis: lax.rem(me + sgn + n, n)}, device_id_type=MESH_ID)

    def arrival(k, d, ch):
        sgn = -1 if d else 1
        origin = lax.rem(me - sgn * (k + 1) + 2 * n, n)
        rng = part(k, d, ch)
        return pltpu.make_async_remote_copy(
            src_ref=o_ref.at[origin, rng], dst_ref=o_ref.at[origin, rng],
            send_sem=sems.at[0, d, k * chunks + ch], recv_sem=sems.at[1, d, k * chunks + ch],
            device_id={axis: lax.rem(me + sgn + n, n)}, device_id_type=MESH_ID)

    return copy, arrival, n // 2, chunks


def ring_peers(job):
    axis, n = job["axis"], AXES[job["axis"]]
    me = lax.axis_index(axis)
    return [{axis: lax.rem(me + 1, n)}, {axis: lax.rem(me + n - 1, n)}]


def shifts_of(axes):
    out = [()]
    for a in axes:
        out = [s + (d,) for s in out for d in range(AXES[a])]
    return [s for s in out if any(s)]


def index_of(axes, shift, sign):
    idx, dev = 0, {}
    for a, d in zip(axes, shift):
        n = AXES[a]
        c = lax.rem(lax.axis_index(a) + sign * d + n, n)
        dev[a] = c
        idx = idx * n + c
    return idx, dev


def a2a_copies(job, x_ref, o_ref, sems):
    axes = job["axes"]
    my_idx, _ = index_of(axes, (0,) * len(axes), 1)
    out = []
    for i, s in enumerate(shifts_of(axes)):
        dst_i, dst_d = index_of(axes, s, 1)
        src_i, _ = index_of(axes, s, -1)
        send = pltpu.make_async_remote_copy(
            src_ref=x_ref.at[dst_i], dst_ref=o_ref.at[my_idx], send_sem=sems.at[0, i],
            recv_sem=sems.at[1, i], device_id=dst_d, device_id_type=MESH_ID)
        recv = pltpu.make_async_remote_copy(
            src_ref=o_ref.at[src_i], dst_ref=o_ref.at[src_i], send_sem=sems.at[0, i],
            recv_sem=sems.at[1, i], device_id=dst_d, device_id_type=MESH_ID)
        out.append((send, recv))
    return my_idx, out


def a2a_peers(job):
    return [index_of(job["axes"], s, 1)[1] for s in shifts_of(job["axes"])]


def comm_kernel(jobs, *refs):
    nj = len(jobs)
    xs, os_, sems = refs[:nj], refs[nj:2 * nj], refs[2 * nj:]
    barrier = pltpu.get_barrier_semaphore()
    peers = []
    for job in jobs:
        peers += ring_peers(job) if job["kind"] == "ring" else a2a_peers(job)
    for p in peers:
        pl.semaphore_signal(barrier, inc=1, device_id=p, device_id_type=MESH_ID)
    pl.semaphore_wait(barrier, len(peers))
    rings, alls, sent = [], [], []
    for job, x, o, s in zip(jobs, xs, os_, sems):
        if job["kind"] == "ring":
            rings.append(ring_starts(job, x, o, s))
            c, a, steps, chunks = rings[-1]
            for ch in range(chunks):
                for d in range(2):
                    cp = c(0, d, ch); cp.start(); sent.append(cp)
    for job, x, o, s in zip(jobs, xs, os_, sems):
        if job["kind"] == "a2a":
            mine, cps = a2a_copies(job, x, o, s)
            for cp, _ in cps:
                cp.start(); sent.append(cp)
            alls.append((cps, mine, x, o))
            o[mine] = x[mine]
    for job, x, o in zip(jobs, xs, os_):
        if job["kind"] == "ring":
            o[lax.axis_index(job["axis"])] = x[...]
    for k in range(max([r[2] for r in rings], default=0)):
        for c, a, steps, chunks in rings:
            if k < steps:
                for ch in range(chunks):
                    for d in range(2):
                        a(k, d, ch).wait_recv()
                        if k + 1 < steps:
                            cp = c(k + 1, d, ch); cp.start(); sent.append(cp)
    for cps, *_ in alls:
        for _, r in cps:
            r.wait_recv()
    for cp in sent:
        cp.wait_send()


def comm(jobs, xs, cid):
    outs, sems = [], []
    for job, x in zip(jobs, xs):
        if job["kind"] == "ring":
            n = AXES[job["axis"]]
            outs.append(jax.ShapeDtypeStruct((n, *x.shape), x.dtype))
            sems.append(pltpu.SemaphoreType.DMA((2, 2, n // 2 * job.get("chunks", 1))))
        else:
            outs.append(jax.ShapeDtypeStruct(x.shape, x.dtype))
            sems.append(pltpu.SemaphoreType.DMA((2, len(shifts_of(job["axes"])))))
    return pl.pallas_call(
        functools.partial(comm_kernel, jobs),
        out_shape=outs,
        in_specs=[pl.BlockSpec(memory_space=pltpu.VMEM)] * len(xs),
        out_specs=[pl.BlockSpec(memory_space=pltpu.VMEM)] * len(xs),
        scratch_shapes=sems,
        compiler_params=pltpu.CompilerParams(collective_id=cid, has_side_effects=True),
    )(*xs)


def neumann_inverse(strict_part):
    span_size = strict_part.shape[-1]
    unit_eye = jnp.eye(span_size, dtype=jnp.float32)
    running = unit_eye - strict_part
    power_term = strict_part
    for _ in range(span_size.bit_length() - 2):
        power_term = jnp.einsum("...ij,...jk->...ik", power_term, power_term)
        running = jnp.einsum("...ij,...jk->...ik", running, unit_eye + power_term)
    return running


def delta_mixer(queries, keys_in, values_in, strength, log_decay):
    heads_n, length, key_dim = queries.shape
    blocks_n = length // SPAN

    def to_blocks(tensor):
        return tensor.reshape(heads_n, blocks_n, SPAN, *tensor.shape[2:])

    queries, keys_in, values_in = (to_blocks(queries), to_blocks(keys_in), to_blocks(values_in))
    strength, log_decay = (to_blocks(strength), to_blocks(log_decay))
    cumulative = jnp.cumsum(log_decay, axis=-1)
    position = jnp.arange(SPAN)
    inclusive = position[:, None] >= position[None, :]
    strictly = position[:, None] > position[None, :]
    spread = jnp.where(inclusive, cumulative[..., :, None] - cumulative[..., None, :], -jnp.inf)
    decay_map = jnp.exp(spread)
    key_gram = jnp.einsum("hncd,hnmd->hncm", keys_in, keys_in)
    strict_part = jnp.where(strictly, strength[..., :, None] * key_gram * decay_map, 0.0)
    inverse = neumann_inverse(strict_part)
    fresh_vals = jnp.einsum("hncm,hnme->hnce", inverse, values_in * strength[..., None])
    correction = jnp.einsum(
        "hncm,hnmd->hncd", inverse, keys_in * (strength * jnp.exp(cumulative))[..., None]
    )
    attend_map = jnp.where(
        inclusive, jnp.einsum("hncd,hnmd->hncm", queries, keys_in) * decay_map, 0.0
    )
    query_dec = queries * jnp.exp(cumulative)[..., None]
    key_dec = keys_in * jnp.exp(cumulative[..., -1:] - cumulative)[..., None]
    carry_decay = jnp.exp(cumulative[..., -1])

    def advance(memory_state, inputs):
        fresh_blk, correct_blk, attend_blk, query_blk, key_blk, decay_blk = inputs
        new_values = fresh_blk - jnp.einsum("hcd,hde->hce", correct_blk, memory_state)
        output = jnp.einsum("hcd,hde->hce", query_blk, memory_state) + jnp.einsum(
            "hcm,hme->hce", attend_blk, new_values
        )
        memory_state = memory_state * decay_blk[:, None, None] + jnp.einsum(
            "hcd,hce->hde", key_blk, new_values
        )
        return (memory_state, output)

    stacked = tuple(
        (
            jnp.moveaxis(tensor, 1, 0)
            for tensor in (fresh_vals, correction, attend_map, query_dec, key_dec, carry_decay)
        )
    )
    initial = jnp.zeros((heads_n, key_dim, values_in.shape[-1]), jnp.float32)
    _, outputs = lax.scan(advance, initial, stacked)
    return jnp.transpose(outputs, (1, 0, 2, 3)).reshape(heads_n, length, -1)


def mixer_output(query_raw, key_raw, value_raw, beta_raw, decay_raw, rate_vals):
    length = query_raw.shape[0]
    heads_n = beta_raw.shape[0]

    def heads_first(matrix):
        return jnp.transpose(matrix.astype(jnp.float32).reshape(length, heads_n, -1), (1, 0, 2))

    queries = heads_first(query_raw)
    keys_in = heads_first(key_raw)
    values_in = heads_first(value_raw)
    queries = (
        queries
        * lax.rsqrt(jnp.sum(queries * queries, axis=-1, keepdims=True) + NORM_FLOOR)
        * queries.shape[-1] ** (-0.5)
    )
    keys_in = keys_in * lax.rsqrt(jnp.sum(keys_in * keys_in, axis=-1, keepdims=True) + NORM_FLOOR)
    strength = jax.nn.sigmoid(beta_raw)
    log_decay = -rate_vals[:, None] * jax.nn.softplus(decay_raw)
    mixer_out = delta_mixer(queries, keys_in, values_in, strength, log_decay)
    return jnp.transpose(mixer_out, (1, 0, 2)).reshape(length, -1)


YC = ("st_1", "st_2")


def ring(axis, chunks=1):
    return dict(kind="ring", axis=axis, chunks=chunks)


def a2a(*axes):
    return dict(kind="a2a", axes=axes)


def rows_of(vec):
    flat = vec.reshape(-1, 128)
    return jnp.pad(flat, ((0, 16 - flat.shape[0]), (0, 0)))


def stats_kernel(x_ref, m_ref, w_ref, o_ref, wo_ref, got, tot, every, back, s1, s2, s3, sw):
    jobs = [a2a(*YC), a2a("st_0"), a2a("tp")]
    barrier = pltpu.get_barrier_semaphore()
    peers = []
    for job in jobs:
        peers += a2a_peers(job)
    for p in peers:
        pl.semaphore_signal(barrier, inc=1, device_id=p, device_id_type=MESH_ID)
    pl.semaphore_wait(barrier, len(peers))
    sent = []
    mine, cps = a2a_copies(jobs[0], x_ref, got, s1)
    for cp, _ in cps:
        cp.start()
        sent.append(cp)
    minew, cpw = a2a_copies(jobs[2], w_ref, wo_ref, sw)
    for cp, _ in cpw:
        cp.start()
        sent.append(cp)
    got[mine] = x_ref[mine]
    wo_ref[minew] = w_ref[minew]
    for _, r in cps:
        r.wait_recv()
    for b in range(6):
        acc = got[0] * m_ref[0, b]
        for j in range(1, 8):
            acc = acc + got[j] * m_ref[j, b]
        tot[b] = acc
    z = lax.axis_index("st_0")
    cps2 = []
    for s in range(1, 8):
        dst = lax.rem(z + s, 8)
        src = lax.rem(z - s + 8, 8)
        cp = pltpu.make_async_remote_copy(
            src_ref=tot, dst_ref=every.at[z], send_sem=s2.at[0, s], recv_sem=s2.at[1, s],
            device_id={"st_0": dst}, device_id_type=MESH_ID)
        rv = pltpu.make_async_remote_copy(
            src_ref=tot, dst_ref=every.at[src], send_sem=s2.at[0, s], recv_sem=s2.at[1, s],
            device_id={"st_0": dst}, device_id_type=MESH_ID)
        cp.start()
        sent.append(cp)
        cps2.append(rv)
    every[z] = tot[...]
    for rv in cps2:
        rv.wait_recv()
    whole = []
    for b in range(6):
        acc = every[0, b]
        for k in range(1, 8):
            acc = acc + every[k, b]
        whole.append(acc)
    for j in range(8):
        acc = whole[0] * m_ref[j, 0]
        for b in range(1, 6):
            acc = acc + whole[b] * m_ref[j, b]
        back[j] = acc
    mine, cps3 = a2a_copies(jobs[0], back, o_ref, s3)
    for cp, _ in cps3:
        cp.start()
        sent.append(cp)
    o_ref[mine] = back[mine]
    for _, r in cps3 + cpw:
        r.wait_recv()
    for cp in sent:
        cp.wait_send()


def stats_exchange(x, mask, w, cid):
    v = pl.BlockSpec(memory_space=pltpu.VMEM)
    f = jnp.float32
    return pl.pallas_call(
        stats_kernel,
        out_shape=[jax.ShapeDtypeStruct(x.shape, f), jax.ShapeDtypeStruct(w.shape, w.dtype)],
        in_specs=[v] * 3,
        out_specs=[v] * 2,
        scratch_shapes=[
            pltpu.VMEM((8, 8, 128), f), pltpu.VMEM((6, 8, 128), f), pltpu.VMEM((8, 6, 8, 128), f),
            pltpu.VMEM((8, 8, 128), f), pltpu.SemaphoreType.DMA((2, 7)), pltpu.SemaphoreType.DMA((2, 8)),
            pltpu.SemaphoreType.DMA((2, 7)), pltpu.SemaphoreType.DMA((2, 3))],
        compiler_params=pltpu.CompilerParams(collective_id=cid, has_side_effects=True),
    )(x, mask, w)


def dots_kernel(x_ref, m_ref, o_ref, got, tot, s1, s2):
    jobs = [a2a(*YC), a2a("st_0")]
    barrier = pltpu.get_barrier_semaphore()
    peers = a2a_peers(jobs[0]) + a2a_peers(jobs[1])
    for p in peers:
        pl.semaphore_signal(barrier, inc=1, device_id=p, device_id_type=MESH_ID)
    pl.semaphore_wait(barrier, len(peers))
    sent = []
    mine, cps = a2a_copies(jobs[0], x_ref, got, s1)
    for cp, _ in cps:
        cp.start()
        sent.append(cp)
    got[mine] = x_ref[mine]
    for _, r in cps:
        r.wait_recv()
    for b in range(6):
        acc = got[0] * m_ref[0, b]
        for j in range(1, 8):
            acc = acc + got[j] * m_ref[j, b]
        for zr in range(8):
            tot[zr, b:b + 1, :] = acc[zr:zr + 1, :]
    mine, cps2 = a2a_copies(jobs[1], tot, o_ref, s2)
    for cp, _ in cps2:
        cp.start()
        sent.append(cp)
    o_ref[mine] = tot[mine]
    for _, r in cps2:
        r.wait_recv()
    for cp in sent:
        cp.wait_send()


def dots_exchange(x, mask, cid):
    v = pl.BlockSpec(memory_space=pltpu.VMEM)
    f = jnp.float32
    return pl.pallas_call(
        dots_kernel,
        out_shape=jax.ShapeDtypeStruct((8, 8, 128), f),
        in_specs=[v] * 2,
        out_specs=v,
        scratch_shapes=[
            pltpu.VMEM((8, 8, 128), f), pltpu.VMEM((8, 8, 128), f),
            pltpu.SemaphoreType.DMA((2, 7)), pltpu.SemaphoreType.DMA((2, 7))],
        compiler_params=pltpu.CompilerParams(collective_id=cid, has_side_effects=True),
    )(x, mask)


def body(
    tokens, cotangent, mix_query, mix_key, mix_value, beta_pre, decay_pre, decay_rate,
    passages, passage_ids, query_weight, key_weight, value_weight, gate_weight,
):
    f32, bf16 = jnp.float32, jnp.bfloat16
    scale = SCORE_GAIN * 256 ** (-0.5)
    z = lax.axis_index("st_0")
    ids = passage_ids.reshape(24)
    owner, local = ids // 16, ids % 16
    match = owner[None, :] == jnp.arange(64, dtype=jnp.int32)[:, None]
    code_of = local * 8 + jnp.arange(24, dtype=jnp.int32) // 4
    code = jnp.sum(jnp.where(match, code_of[None, :], 0), axis=-1, dtype=jnp.int32)
    code = jnp.where(jnp.any(match, axis=-1), code, 128)
    table = jnp.pad(code.reshape(8, 8), ((0, 8), (0, 120)))

    tok4, cot_z, table_z = comm([ring("tp"), ring("st_0", 2), ring("st_0")], [tokens, cotangent, table], 1)
    codes = lax.dynamic_slice(table_z, (0, z, 0), (8, 1, 8)).reshape(8, 8)
    slot_block = (jnp.arange(8, dtype=jnp.int32)[:, None] * 6 + codes % 8).T
    cot_slots = cot_z.reshape(48, 64, 256)[slot_block]
    cot_here = lax.all_to_all(cot_slots, YC, split_axis=0, concat_axis=0, tiled=True).reshape(64, 64, 256)

    query_acc = lax.dot_general(
        tok4, query_weight.reshape(4, 512, 256), (((0, 2), (0, 1)), ((), ())), preferred_element_type=f32)
    gate_acc = jnp.einsum("ptk,pk->t", tok4, gate_weight.reshape(4, 512), preferred_element_type=f32)
    query_low = lax.optimization_barrier(query_acc.astype(bf16))
    query_float = query_low.astype(f32)
    query_scale = lax.rsqrt(jnp.mean(query_float * query_float, axis=-1, keepdims=True) + NORM_FLOOR)
    query_hat = (query_float * query_scale).astype(bf16)
    gate_open = jax.nn.sigmoid(gate_acc)

    gw4 = jnp.broadcast_to(gate_weight.reshape(4, 1, 512), (4, 16, 512))
    q_z, gate_z, wk_cols, wv_cols, gw_cols = comm(
        [ring("st_0", 2), ring("st_0"), a2a("tp"), a2a("tp"), a2a("tp")],
        [query_hat, rows_of(gate_open), key_weight.reshape(4, 512, 256), value_weight.reshape(4, 512, 256), gw4], 2)
    q_slots = q_z.reshape(48, 64, 256)[slot_block]
    q_here = lax.all_to_all(q_slots, YC, split_axis=0, concat_axis=0, tiled=True).reshape(64, 64, 256)
    gates = gate_z[:, :3].reshape(48, 64)[slot_block]
    side = jnp.concatenate([gates, jnp.broadcast_to(codes.T[:, :, None], (8, 8, 64)).astype(f32)], axis=-1)
    side_here = comm([a2a(*YC)], [side], 3)[0].reshape(64, 128)
    gate_here = side_here[:, :64]
    code_here = side_here[:, 64].astype(jnp.int32)
    used = code_here < 128
    loc = jnp.where(used, code_here // 8, 0)

    flat_rows = passages.reshape(1024, 2048)
    key_low = lax.optimization_barrier(
        jnp.dot(flat_rows, key_weight, preferred_element_type=f32).astype(bf16))
    value_all = jnp.dot(flat_rows, value_weight, preferred_element_type=f32).astype(bf16)
    key_float = key_low.astype(f32)
    key_scale = lax.rsqrt(jnp.mean(key_float * key_float, axis=-1, keepdims=True) + NORM_FLOOR)
    key_hat = (key_float * key_scale).astype(bf16)
    k_sel = key_hat.reshape(16, 64, 256)[loc]
    v_sel = value_all.reshape(16, 64, 256)[loc]

    scores = jnp.einsum("sid,sjd->sij", q_here, k_sel, preferred_element_type=f32) * scale
    exps = jnp.exp(scores)
    g_here = (gate_here[:, :, None] * cot_here.astype(f32)).astype(bf16)
    grad_probs = jnp.einsum("sid,sjd->sij", g_here, v_sel, preferred_element_type=f32)
    cot_dots = jnp.einsum("sid,sjd->sij", cot_here, v_sel, preferred_element_type=f32)
    sums = jnp.concatenate([jnp.sum(exps, axis=-1), jnp.sum(exps * grad_probs, axis=-1)], axis=-1)

    blk = jnp.where(codes < 128, codes % 8, 7)
    mask = (blk.T[:, None, :] == jnp.arange(6, dtype=jnp.int32)[None, :, None]).astype(f32)
    mask = jnp.broadcast_to(mask[..., None], (8, 6, 8, 128))
    whole, wq_cols = stats_exchange(sums.reshape(8, 8, 128), mask, query_weight.reshape(4, 512, 256), 4)
    whole = whole.reshape(64, 128)
    total = jnp.where(used[:, None], whole[:, :64], 1.0)
    inner = jnp.where(used[:, None], whole[:, 64:], 0.0) / total
    probs = jnp.where(used[:, None, None], exps, 0.0) / total[:, :, None]
    probs_low = probs.astype(bf16)
    score_grad = (probs * (grad_probs - inner[:, :, None])).astype(bf16)
    q_part = (scale * jnp.einsum("sij,sjd->sid", score_grad, k_sel, preferred_element_type=f32)).astype(bf16)
    q_part = jnp.moveaxis(q_part.reshape(8, 8, 64, 256), 0, 1).reshape(64, 64, 256)
    q_back = lax.all_to_all(q_part, ST, split_axis=0, concat_axis=0, tiled=True)
    dots = jnp.sum(probs_low.astype(f32) * cot_dots, axis=-1)
    dots = jnp.pad(dots, ((0, 0), (0, 64))).reshape(8, 8, 128)
    dots_back = dots_exchange(dots, mask, 5)

    key_term = (scale * jnp.einsum("sij,sid->sjd", score_grad, q_here, preferred_element_type=f32)).astype(bf16)
    value_term = jnp.einsum("sij,sid->sjd", probs_low, g_here, preferred_element_type=f32).astype(bf16)
    onehot = ((loc[None, :] == jnp.arange(16, dtype=jnp.int32)[:, None]) & used[None, :]).astype(bf16)
    key_grad_hat = jnp.dot(onehot, key_term.reshape(64, -1), preferred_element_type=f32).reshape(1024, 256)
    value_grad = jnp.dot(onehot, value_term.reshape(64, -1), preferred_element_type=f32).reshape(1024, 256)
    key_grad = (
        key_scale * key_grad_hat
        - key_scale**3 * key_float * jnp.mean(key_float * key_grad_hat, axis=-1, keepdims=True)
    ).astype(bf16)
    value_grad_low = value_grad.astype(bf16)
    weight_term = lax.dot_general(flat_rows, key_grad, CONTRACT_FIRST, preferred_element_type=f32)
    weight_term = jnp.transpose(weight_term.reshape(8, 4, 2, 32, 256), (2, 1, 0, 3, 4)).reshape(2, 1024, 256)
    vg4, w_c = comm([ring("tp", 2), a2a("st_2")], [value_grad_low, weight_term], 6)
    kg4, w_y = comm([ring("tp", 2), a2a("st_1")], [key_grad, (w_c[0] + w_c[1]).reshape(4, 256, 256)], 7)
    w_y = (w_y[0] + w_y[1]) + (w_y[2] + w_y[3])
    row_part = (
        jnp.einsum("hrd,hed->hre", kg4, wk_cols, preferred_element_type=f32)
        + jnp.einsum("hrd,hed->hre", vg4, wv_cols, preferred_element_type=f32)
    ).astype(bf16)
    passage_grad = jnp.sum(row_part.astype(f32), axis=0).astype(bf16).reshape(16, 64, 512)

    mixer_out = mixer_output(mix_query, mix_key, mix_value, beta_pre, decay_pre, decay_rate)
    qhat_grad = jnp.sum(q_back[owner].astype(f32).reshape(6, 4, 64, 256), axis=1).reshape(384, 256)
    read_dot = jnp.sum(dots_back, axis=0)[:6, :64].reshape(384)
    grad_out = cotangent.astype(f32)
    gate_grad = (read_dot - jnp.sum(grad_out * mixer_out, axis=-1)) * gate_open * (1.0 - gate_open)
    query_grad = (
        query_scale * qhat_grad
        - query_scale**3 * query_float * jnp.mean(query_float * qhat_grad, axis=-1, keepdims=True)
    ).astype(bf16)
    qg4, gg4, w_z = comm(
        [ring("tp"), ring("tp"), a2a("st_0")], [query_grad, rows_of(gate_grad), w_y.reshape(8, 32, 256)], 8)
    gg4 = gg4[:, :3].reshape(4, 384)
    token_part = (
        jnp.einsum("htd,hed->hte", qg4, wq_cols, preferred_element_type=f32)
        + gg4[:, :, None] * gw_cols[:, 0].astype(f32)[:, None, :]
    ).astype(bf16)
    token_grad = jnp.sum(token_part.astype(f32), axis=0).astype(bf16)
    key_weight_grad = jnp.sum(w_z, axis=0)
    return token_grad, passage_grad, key_weight_grad


def solution(mesh):
    torus = Mesh(mesh.devices.reshape(8, 4, 2, mesh.shape["tp"]), ("st_0", "st_1", "st_2", "tp"))
    return jax.shard_map(
        body,
        mesh=torus,
        in_specs=(
            P(ST, "tp"),
            P(ST, "tp"),
            P(ST, "tp"),
            P(ST, "tp"),
            P(ST, "tp"),
            P("tp", ST),
            P("tp", ST),
            P("tp"),
            P(ST, None, None),
            P(ST, None),
            P(None, "tp"),
            P(None, "tp"),
            P(None, "tp"),
            P("tp", None),
        ),
        out_specs=(P(ST, "tp"), P(ST, None, "tp"), P(ST, "tp")),
        check_vma=False,
    )
```

time: 402 us -> 379 us (0.943)
  Pallas kernels: 0 us -> 198 us
  waiting for transfers between devices: 201 us -> 19.8 us
  starting transfers between devices: 39 us -> 16 us
  matrix products: 56.4 us -> 78.2 us
  other arithmetic: 31.7 us -> 17.1 us
  between operations: 14.4 us -> 1.27 us
  local copies, waits for them, and re-layouts: 55.7 us -> 43.8 us
    pallas_call x0 -> x8, Pallas kernels: none -> 198 us  [the longest x6 137 us: comm(): pl.pallas_call(functools.partial(comm_kernel, jobs), out_shape=outs, in_s...]
    all_to_all x5 -> x3, waiting for transfers between devices: 175 us -> 19.8 us  [the longest x1 19.8 us: body(): lax.all_to_all(q_slots, YC, split_axis=0, concat_axis=0, tiled=True)]
    unnamed x6 -> x0, waiting for transfers between devices: 23.9 us -> none
    all_to_all x5 -> x3, starting transfers between devices: 38.8 us -> 16 us  [the longest x1 6.84 us: body(): q_back = lax.all_to_all(q_part, ST, split_axis=0, concat_axis=0, tiled=True)]
    convert_element_type x3 -> x2, local copies, waits for them, and re-layouts: 14.3 us -> 2.18 us  [the longest x1 2.11 us: body(): value_grad_low = value_grad.astype(bf16)]
    dot_general x15, matrix products: 25.2 us -> 36.5 us  [the longest x1 4.52 us: body(): jnp.einsum('sid,sjd->sij', q_here, k_sel, preferred_element_type=f32)]
    select_n x7 -> x6, other arithmetic: 9.75 us -> 1.03 us  [the longest x1 0.92 us: body(): total = jnp.where(used[:, None], whole[:, :64], 1.0)]
    reduce_sum x7 -> x5, other arithmetic: 10.4 us -> 2.63 us  [the longest x1 1.58 us: body(): key_weight_grad = jnp.sum(w_z, axis=0)]
  transfers between devices with their start and end apart: 9 -> 3, of which waited for: 5 -> 1; matrix products, arithmetic and copies ran while one was open for 26% -> 28% of each run, Pallas kernels for 0% -> 35%
where the time goes in v1:
time: 379 us; the launch traced here: 374 us
  Pallas kernels  198 us (52%)
  matrix products  78.2 us (21%)
  local copies, waits for them, and re-layouts  43.8 us (12%)
  waiting for transfers between devices  19.8 us (5%)
  other arithmetic  17.1 us (5%)
  starting transfers between devices  16 us (4%)
    pallas_call x6, Pallas kernels, comm(): pl.pallas_call(functools.partial(comm_kernel, jobs), out_shape=outs, in_s...  137 us
    pallas_call x1, Pallas kernels, dots_exchange(): pl.pallas_call(dots_kernel, out_shape=jax.ShapeDtypeStruct((8, 8, 128), f...  42.1 us
    all_to_all x1, waiting for transfers between devices, body(): lax.all_to_all(q_slots, YC, split_axis=0, concat_axis=0, tiled=True)  19.8 us
    pallas_call x1, Pallas kernels, stats_exchange(): pl.pallas_call(stats_kernel, out_shape=[jax.ShapeDtypeStruct(x.shape, f),...  19.6 us
    dot_general x6, matrix products, advance(): jnp.einsum('hcm,hme->hce', attend_blk, new_values)  9.18 us
    unnamed x61, local copies, waits for them, and re-layouts  8.39 us
  transfers between devices with their start and end apart: 3, of which 1 were waited for; matrix products, arithmetic and copies ran while one was open for 28% of the time, Pallas kernels for 35%

profile of v1, /device:TPU:2, one launch (start us, length us, event | category | flops | bytes accessed | tf_op | source)
XLA Modules:
  0.0 374.4 jit_solution(14950855616373375276)
XLA Ops:
  2.4 34.9 %shard_map.157 = (bf16[4,384,512]{2,1,0:T(8,128)(2,1)}, bf16[8,384,256]{2,1,0:T(8,128)(2,1)}, s32[8,16,128]{2,1,0:T(8,128)}) custom-call(bf16[384,512]{1,0:T(8,128)(2,1)} %refs_0_.1, bf16[384,256]{1,0:T(8,128)(2,1)} %refs_1_.1, s32[16,128]{1,0:T(8,128)} %pad.15.refs_2_), custom_call_target="tpu_custom_call" | custom-call | tf_op jit(solution)/shard_map/pallas_call | solution.py:157
  38.8 3.4 gather_fusion.3
  42.2 4.6 %all-to-all-start.1 = ((bf16[8,8,64,256]{3,2,1,0:T(8,128)(2,1)}), bf16[8,8,64,256]{3,2,1,0:T(8,128)(2,1)S(1)}, u32[]{:S(2)}, u32[]{:S(2)}) async-start(bf16[8,8,64,256]{3,2,1,0:T(8,128)(2,1)} %bitcast.247), calls=%async_computation.1 | async-start | bytes 4194304 | tf_op jit(solution)/shard_map/all_to_all | solution.py:415
  58.9 2.0 fusion.29
  66.2 26.0 %while.13 = (s32[]{:T(128)}, f32[2,128,128]{2,1,0:T(8,128)S(1)}, f32[6,2,64,128]{3,2,0,1:T(8,128)}, f32[6,2]{1,0:T(8,128)S(1)}, bf16[6,2,64,128]{3,2,0,1:T(8,128...) while((s32[]{:T(128)}, f32[2,128,128]{2,1,0:T(8,128)S(1)}, ...), condition=%wide.region_14.15_spmd.clone, body=%wide.region_13.14_spmd.clone.sunk | while | flops 14893059 | bytes 1018532 | solution.py:225
  94.1 3.9 %convolution_convert_fusion.3 = bf16[1024,256]{1,0:T(8,128)(2,1)S(1)} fusion(bf16[1024,2048]{1,0:T(8,128)(2,1)} %bitcast.286, bf16[2048,256]{1,0:T(8,128)(2,1)} %param.27), kind=kOutput, calls=%fused_computation.56 | convolution fusion | flops 1074003968 | bytes 5767168 | tf_op jit(solution)/shard_map/dot_general | solution.py:442
  101.5 31.9 %shard_map.158 = (bf16[8,384,256]{2,1,0:T(8,128)(2,1)}, f32[8,16,128]{2,1,0:T(8,128)}, bf16[4,512,256]{2,1,0:T(8,128)(2,1)}, bf16[4,512,256]{2,1,0:T(8,128)(2,1)}, bf16[4,16,512]{2,1,0:T(8,128)(2,1)}) custom-call(bf16[384,256]{1,0:T(8,128)(2,1)} %fusion.46.refs_0_, f32[16,128]{1,0:T(8,128)} %pad.16.refs_1_, bf16[4,512,256]{2,1,0:T(8,128)(2,1)} %bitcast.271, ...), custom_call_target="tpu_custom_call" | custom-call | tf_op jit(solution)/shard_map/pallas_call | solution.py:157
  135.6 7.5 %shard_map.159 = f32[8,8,128]{2,1,0:T(8,128)} custom-call(f32[8,8,128]{2,1,0:T(8,128)} %pad_maximum_fusion.refs_0_), custom_call_target="tpu_custom_call" | custom-call | tf_op jit(solution)/shard_map/pallas_call | solution.py:157
  144.8 3.5 gather_fusion.1
  148.7 3.7 convolution_convert_fusion.2
  153.8 4.5 %all-to-all-start = ((bf16[8,8,64,256]{3,2,1,0:T(8,128)(2,1)}), bf16[8,8,64,256]{3,2,1,0:T(8,128)(2,1)}, u32[]{:S(2)}, u32[]{:S(2)}) async-start(bf16[8,8,64,256]{3,2,1,0:T(8,128)(2,1)} %bitcast.248), calls=%async_computation | async-start | bytes 4194304 | tf_op jit(solution)/shard_map/all_to_all | solution.py:431
  158.4 2.0 gather_fusion.4
  162.5 3.0 fusion.25
  165.6 19.8 %all-to-all-done = bf16[8,8,64,256]{3,2,1,0:T(8,128)(2,1)} async-done(((bf16[8,8,64,256]{3,2,1,0:T(8,128)(2,1)}), bf16[8,8,64,256]{3,2,1,0:T(8,128)(2,1)}, u32[]{:S(2)}, u32[]{:S(2)}) %all-to-all-start) | async-done | bytes 2097184 | tf_op jit(solution)/shard_map/all_to_all | solution.py:431
  185.3 4.5 %fusion.95 = (f32[64,64]{1,0:T(8,128)S(1)}, f32[64,64]{1,0:T(8,128)S(1)}, f32[64,64,64]{1,2,0:T(8,128)}) fusion(f32[64,64,64]{1,2,0:T(8,128)S(1)} %fusion.25, bf16[64,64,256]{2,1,0:T(8,128)(2,1)} %bitcast.14, bf16[64,64,256]{2,1,0:T(8,128)(2,1)} %gather_fusion.2), kind=kOutput, calls=%fused_computation.209 | convolution fusion | flops 135258112 | bytes 6324224 | tf_op jit(solution)/shard_map/sid,sjd->sij/dot_general | solution.py:450
  191.3 19.6 %shard_map.160 = (f32[8,8,128]{2,1,0:T(8,128)}, bf16[4,512,256]{2,1,0:T(8,128)(2,1)}) custom-call(f32[8,8,128]{2,1,0:T(8,128)} %maximum_bitcast_fusion.x_ref, f32[8,6,8,128]{3,2,1,0:T(8,128)} %broadcast_in_dim.165.m_ref, bf16[4,512,256]{2,1,0:T(8,128)(2,1)} %bitcast.269), custom_call_target="tpu_custom_call" | custom-call | tf_op jit(solution)/shard_map/pallas_call | solution.py:336
  211.9 4.5 %convolution_convert_fusion.1 = bf16[64,64,256]{2,1,0:T(8,128)(2,1)} fusion(bf16[64,64,256]{2,1,0:T(8,128)(2,1)} %bitcast.245, f32[64,64]{1,0:T(8,128)S(1)} %bitcast.277, f32[64,64,64]{1,2,0:T(8,128)} %get-tuple-element.184, f32[64,64]{1,0:T(8,128)S(1)} %get-tuple-element.171, pred[64]{0:T(512)(128)(4,1)S(1)} %bitcast_compare_fusion), kind=kOutput, calls=%fused_computation.47 | convolution fusion | flops 139198464 | bytes 5275712 | tf_op jit(solution)/shard_map/sij,sid->sjd/dot_general | solution.py:475
  216.8 2.4 multiply_convert_fusion
  222.8 6.8 %all-to-all-start.2 = ((bf16[64,64,256]{2,1,0:T(8,128)(2,1)}), bf16[64,64,256]{2,1,0:T(8,128)(2,1)}, u32[]{:S(2)}, u32[]{:S(2)}) async-start(bf16[64,64,256]{2,1,0:T(8,128)(2,1)} %bitcast.28), calls=%async_computation.2 | async-start | bytes 4194304 | tf_op jit(solution)/shard_map/all_to_all | solution.py:469
  230.2 2.9 copy.167
  234.2 2.1 convert_element_type.164.refs_0_
  236.4 2.9 multiply_reduce_fusion
  239.9 42.1 %shard_map.161 = f32[8,8,128]{2,1,0:T(8,128)} custom-call(f32[8,8,128]{2,1,0:T(8,128)} %pad_bitcast_fusion.x_ref, f32[8,6,8,128]{3,2,1,0:T(8,128)} %broadcast_in_dim.165.m_ref), custom_call_target="tpu_custom_call" | custom-call | tf_op jit(solution)/shard_map/pallas_call | solution.py:384
  285.3 5.0 %convolution_bitcast_fusion = f32[2048,256]{0,1:T(8,128)} fusion(bf16[1024,256]{1,0:T(8,128)(2,1)S(1)} %fusion.42.refs_0_, bf16[1024,2048]{1,0:T(8,128)(2,1)} %bitcast.288), kind=kOutput, calls=%fused_computation.41 | convolution fusion | flops 1073741824 | bytes 6815744 | tf_op jit(solution)/shard_map/dot_general | solution.py:484
  293.7 24.4 %shard_map.162 = (bf16[4,1024,256]{2,1,0:T(8,128)(2,1)}, f32[2,1024,256]{2,1,0:T(8,128)}) custom-call(bf16[1024,256]{1,0:T(8,128)(2,1)} %convert_element_type.164.refs_0_, f32[2,1024,256]{2,1,0:T(8,128)} %bitcast.249), custom_call_target="tpu_custom_call" | custom-call | tf_op jit(solution)/shard_map/pallas_call | solution.py:157
  318.1 2.6 slice_add_fusion
  320.7 24.8 %shard_map.163 = (bf16[4,1024,256]{2,1,0:T(8,128)(2,1)}, f32[4,256,256]{2,1,0:T(8,128)}) custom-call(bf16[1024,256]{1,0:T(8,128)(2,1)} %copy-done.9, f32[4,256,256]{2,1,0:T(8,128)} %bitcast.256), custom_call_target="tpu_custom_call" | custom-call | tf_op jit(solution)/shard_map/pallas_call | solution.py:157
  347.5 3.0 fusion.101
  350.5 2.4 fusion.24
  352.9 2.3 gather_fusion.5
  356.4 13.1 %shard_map.164 = (bf16[4,384,256]{2,1,0:T(8,128)(2,1)}, f32[4,16,128]{2,1,0:T(8,128)}, f32[8,32,256]{2,1,0:T(8,128)}) custom-call(bf16[384,256]{1,0:T(8,128)(2,1)} %fusion.49.refs_0_, f32[16,128]{1,0:T(8,128)} %pad.18.refs_1_, f32[8,32,256]{2,1,0:T(8,128)} %bitcast.268), custom_call_target="tpu_custom_call" | custom-call | tf_op jit(solution)/shard_map/pallas_call | solution.py:157
  371.8 2.6 fusion.26
  (208 shorter events, 80.2 us)
Async XLA Ops:
  42.2 4.8 %copy-start.15 = (bf16[384,256]{1,0:T(8,128)(2,1)S(1)}, bf16[384,256]{1,0:T(8,128)(2,1)}, u32[]{:S(2)}) copy-start(bf16[384,256]{1,0:T(8,128)(2,1)} %refs_1_.1) | copy-start | bytes 589828
  42.2 5.6 %copy-start.24 = (f32[2]{0:T(128)S(1)}, f32[2]{0:T(128)}, u32[]{:S(2)}) copy-start(f32[2]{0:T(128)} %param.23) | copy-start | bytes 28
  42.2 5.6 %copy-start.21 = (f32[2,384]{1,0:T(2,128)S(1)}, f32[2,384]{1,0:T(2,128)}, u32[]{:S(2)}) copy-start(f32[2,384]{1,0:T(2,128)} %param.21) | copy-start | bytes 9220
  42.2 5.6 %copy-start.20 = (bf16[1,2048]{1,0:T(2,128)(2,1)S(1)}, bf16[1,2048]{1,0:T(2,128)(2,1)}, u32[]{:S(2)}) copy-start(bf16[1,2048]{1,0:T(2,128)(2,1)} %param.29) | copy-start | bytes 12292
  42.2 5.8 %copy-start.22 = (f32[2,384]{1,0:T(2,128)S(1)}, f32[2,384]{1,0:T(2,128)}, u32[]{:S(2)}) copy-start(f32[2,384]{1,0:T(2,128)} %param.22) | copy-start | bytes 9220
  42.2 6.7 %copy-start.18 = (bf16[384,256]{1,0:T(8,128)(2,1)S(1)}, bf16[384,256]{1,0:T(8,128)(2,1)}, u32[]{:S(2)}) copy-start(bf16[384,256]{1,0:T(8,128)(2,1)} %param.18) | copy-start | bytes 589828
  42.2 110.3 %all-to-all-start.1 = ((bf16[8,8,64,256]{3,2,1,0:T(8,128)(2,1)}), bf16[8,8,64,256]{3,2,1,0:T(8,128)(2,1)S(1)}, u32[]{:S(2)}, u32[]{:S(2)}) async-start(bf16[8,8,64,256]{3,2,1,0:T(8,128)(2,1)} %bitcast.247), calls=%async_computation.1 | async-start | bytes 4194304 | tf_op jit(solution)/shard_map/all_to_all | solution.py:415
  46.8 3.3 copy-start.19
  55.2 3.7 copy-start.6
  57.1 7.1 %copy-start.7 = (f32[2,384,128]{2,1,0:T(8,128)S(1)}, f32[2,384,128]{2,1,0:T(8,128)}, u32[]{:S(2)}) copy-start(f32[2,384,128]{2,1,0:T(8,128)} %copy.127) | copy-start | bytes 1179652
  94.1 3.9 %copy-start.11 = (bf16[4,384,512]{2,1,0:T(8,128)(2,1)S(1)}, bf16[4,384,512]{2,1,0:T(8,128)(2,1)}, u32[]{:S(2)}) copy-start(bf16[4,384,512]{2,1,0:T(8,128)(2,1)} %get-tuple-element.67) | copy-start | bytes 4718596
  94.1 4.4 %copy-start.14 = (bf16[2048,256]{1,0:T(8,128)(2,1)S(1)}, bf16[2048,256]{1,0:T(8,128)(2,1)}, u32[]{:S(2)}) copy-start(bf16[2048,256]{1,0:T(8,128)(2,1)} %param.26) | copy-start | bytes 3145732
  98.0 50.5 %copy-start.3 = (bf16[1024,256]{1,0:T(8,128)(2,1)}, bf16[1024,256]{1,0:T(8,128)(2,1)S(1)}, u32[]{:S(2)}) copy-start(bf16[1024,256]{1,0:T(8,128)(2,1)S(1)} %convolution_convert_fusion.3) | copy-start | bytes 1572868
  152.5 1.3 copy-start.1
  153.8 31.5 %all-to-all-start = ((bf16[8,8,64,256]{3,2,1,0:T(8,128)(2,1)}), bf16[8,8,64,256]{3,2,1,0:T(8,128)(2,1)}, u32[]{:S(2)}, u32[]{:S(2)}) async-start(bf16[8,8,64,256]{3,2,1,0:T(8,128)(2,1)} %bitcast.248), calls=%async_computation | async-start | bytes 4194304 | tf_op jit(solution)/shard_map/all_to_all | solution.py:431
  160.4 2.0 copy-start.12
  160.4 2.0 copy-start.16
  160.4 2.1 copy-start.17
  211.9 4.5 %copy-start.5 = (f32[64,64,64]{1,2,0:T(8,128)S(1)}, f32[64,64,64]{1,2,0:T(8,128)}, u32[]{:S(2)}) copy-start(f32[64,64,64]{1,2,0:T(8,128)} %get-tuple-element.184) | copy-start | bytes 3145732
  216.8 2.4 copy-start
  222.8 130.2 %all-to-all-start.2 = ((bf16[64,64,256]{2,1,0:T(8,128)(2,1)}), bf16[64,64,256]{2,1,0:T(8,128)(2,1)}, u32[]{:S(2)}, u32[]{:S(2)}) async-start(bf16[64,64,256]{2,1,0:T(8,128)(2,1)} %bitcast.28), calls=%async_computation.2 | async-start | bytes 4194304 | tf_op jit(solution)/shard_map/all_to_all | solution.py:469
  233.0 3.3 copy-start.2
  239.3 45.5 %copy-start.4 = (bf16[1024,256]{1,0:T(8,128)(2,1)S(1)}, bf16[1024,256]{1,0:T(8,128)(2,1)}, u32[]{:S(2)}) copy-start(bf16[1024,256]{1,0:T(8,128)(2,1)} %copy-done.3) | copy-start | bytes 1572868
  285.3 5.0 %copy-start.9 = (bf16[1024,256]{1,0:T(8,128)(2,1)}, bf16[1024,256]{1,0:T(8,128)(2,1)S(1)}, u32[]{:S(2)}) copy-start(bf16[1024,256]{1,0:T(8,128)(2,1)S(1)} %fusion.42.refs_0_) | copy-start | bytes 1572868
  320.7 26.7 %copy-start.8 = (bf16[4,512,256]{2,1,0:T(8,128)(2,1)S(1)}, bf16[4,512,256]{2,1,0:T(8,128)(2,1)}, u32[]{:S(2)}) copy-start(bf16[4,512,256]{2,1,0:T(8,128)(2,1)} %get-tuple-element.81) | copy-start | bytes 3145732
  347.5 3.0 copy-start.10
  347.5 3.0 copy-start.13
  352.9 18.9 %copy-start.23 = (bf16[4,512,256]{2,1,0:T(8,128)(2,1)S(1)}, bf16[4,512,256]{2,1,0:T(8,128)(2,1)}, u32[]{:S(2)}) copy-start(bf16[4,512,256]{2,1,0:T(8,128)(2,1)} %get-tuple-element.77) | copy-start | bytes 3145732

commit v2 on v1

v2 whole, which is shorter than its diff:
```python
import functools

import jax
import jax.numpy as jnp
from jax import lax
from jax.experimental import pallas as pl
from jax.experimental.pallas import tpu as pltpu
from jax.sharding import Mesh
from jax.sharding import PartitionSpec as P

SPAN = 64
ST = ("st_0", "st_1", "st_2")


NORM_FLOOR = 1.0
SCORE_GAIN = 4.0
CONTRACT_LAST = (((1,), (1,)), ((), ()))
CONTRACT_FIRST = (((0,), (0,)), ((), ()))


AXES = {"st_0": 8, "st_1": 4, "st_2": 2, "tp": 4}
MESH_ID = pl.DeviceIdType.MESH


def ring_starts(job, x_ref, o_ref, sems):
    axis, n, chunks = job["axis"], AXES[job["axis"]], job.get("chunks", 1)
    rows = x_ref.shape[0]
    me = lax.axis_index(axis)
    step_rows = rows // chunks

    def part(k, d, ch):
        lo, size = ch * step_rows, step_rows
        if k == n // 2 - 1:
            size = step_rows // 2
            lo = lo + (size if d else 0)
        return pl.ds(lo, size)

    def copy(k, d, ch):
        sgn = -1 if d else 1
        origin = lax.rem(me - sgn * k + 2 * n, n)
        rng = part(k, d, ch)
        src = x_ref.at[rng] if k == 0 else o_ref.at[origin, rng]
        return pltpu.make_async_remote_copy(
            src_ref=src, dst_ref=o_ref.at[origin, rng],
            send_sem=sems.at[0, d, k * chunks + ch], recv_sem=sems.at[1, d, k * chunks + ch],
            device_id={axis: lax.rem(me + sgn + n, n)}, device_id_type=MESH_ID)

    def arrival(k, d, ch):
        sgn = -1 if d else 1
        origin = lax.rem(me - sgn * (k + 1) + 2 * n, n)
        rng = part(k, d, ch)
        return pltpu.make_async_remote_copy(
            src_ref=o_ref.at[origin, rng], dst_ref=o_ref.at[origin, rng],
            send_sem=sems.at[0, d, k * chunks + ch], recv_sem=sems.at[1, d, k * chunks + ch],
            device_id={axis: lax.rem(me + sgn + n, n)}, device_id_type=MESH_ID)

    return copy, arrival, n // 2, chunks


def ring_peers(job):
    axis, n = job["axis"], AXES[job["axis"]]
    me = lax.axis_index(axis)
    return [{axis: lax.rem(me + 1, n)}, {axis: lax.rem(me + n - 1, n)}]


def shifts_of(axes):
    out = [()]
    for a in axes:
        out = [s + (d,) for s in out for d in range(AXES[a])]
    return [s for s in out if any(s)]


def index_of(axes, shift, sign):
    idx, dev = 0, {}
    for a, d in zip(axes, shift):
        n = AXES[a]
        c = lax.rem(lax.axis_index(a) + sign * d + n, n)
        dev[a] = c
        idx = idx * n + c
    return idx, dev


def a2a_copies(job, x_ref, o_ref, sems):
    axes = job["axes"]
    my_idx, _ = index_of(axes, (0,) * len(axes), 1)
    out = []
    for i, s in enumerate(shifts_of(axes)):
        dst_i, dst_d = index_of(axes, s, 1)
        src_i, _ = index_of(axes, s, -1)
        send = pltpu.make_async_remote_copy(
            src_ref=x_ref.at[dst_i], dst_ref=o_ref.at[my_idx], send_sem=sems.at[0, i],
            recv_sem=sems.at[1, i], device_id=dst_d, device_id_type=MESH_ID)
        recv = pltpu.make_async_remote_copy(
            src_ref=o_ref.at[src_i], dst_ref=o_ref.at[src_i], send_sem=sems.at[0, i],
            recv_sem=sems.at[1, i], device_id=dst_d, device_id_type=MESH_ID)
        out.append((send, recv))
    return my_idx, out


def a2a_peers(job):
    return [index_of(job["axes"], s, 1)[1] for s in shifts_of(job["axes"])]


def comm_kernel(jobs, *refs):
    nj = len(jobs)
    xs, os_, sems = refs[:nj], refs[nj:2 * nj], refs[2 * nj:]
    barrier = pltpu.get_barrier_semaphore()
    peers = []
    for job in jobs:
        peers += ring_peers(job) if job["kind"] == "ring" else a2a_peers(job)
    for p in peers:
        pl.semaphore_signal(barrier, inc=1, device_id=p, device_id_type=MESH_ID)
    pl.semaphore_wait(barrier, len(peers))
    rings, alls, sent = [], [], []
    for job, x, o, s in zip(jobs, xs, os_, sems):
        if job["kind"] == "ring":
            rings.append(ring_starts(job, x, o, s))
            c, a, steps, chunks = rings[-1]
            for ch in range(chunks):
                for d in range(2):
                    cp = c(0, d, ch); cp.start(); sent.append(cp)
    for job, x, o, s in zip(jobs, xs, os_, sems):
        if job["kind"] == "a2a":
            mine, cps = a2a_copies(job, x, o, s)
            for cp, _ in cps:
                cp.start(); sent.append(cp)
            alls.append((cps, mine, x, o))
            o[mine] = x[mine]
    for job, x, o in zip(jobs, xs, os_):
        if job["kind"] == "ring":
            o[lax.axis_index(job["axis"])] = x[...]
    for k in range(max([r[2] for r in rings], default=0)):
        for c, a, steps, chunks in rings:
            if k < steps:
                for ch in range(chunks):
                    for d in range(2):
                        a(k, d, ch).wait_recv()
                        if k + 1 < steps:
                            cp = c(k + 1, d, ch); cp.start(); sent.append(cp)
    for cps, *_ in alls:
        for _, r in cps:
            r.wait_recv()
    for cp in sent:
        cp.wait_send()


def comm(jobs, xs, cid):
    outs, sems = [], []
    for job, x in zip(jobs, xs):
        if job["kind"] == "ring":
            n = AXES[job["axis"]]
            outs.append(jax.ShapeDtypeStruct((n, *x.shape), x.dtype))
            sems.append(pltpu.SemaphoreType.DMA((2, 2, n // 2 * job.get("chunks", 1))))
        else:
            outs.append(jax.ShapeDtypeStruct(x.shape, x.dtype))
            sems.append(pltpu.SemaphoreType.DMA((2, len(shifts_of(job["axes"])))))
    return pl.pallas_call(
        functools.partial(comm_kernel, jobs),
        out_shape=outs,
        in_specs=[pl.BlockSpec(memory_space=pltpu.VMEM)] * len(xs),
        out_specs=[pl.BlockSpec(memory_space=pltpu.VMEM)] * len(xs),
        scratch_shapes=sems,
        compiler_params=pltpu.CompilerParams(collective_id=cid, has_side_effects=True),
    )(*xs)


SHIFTS = [(0, 1), (1, 0), (1, 1), (2, 0), (2, 1), (3, 0), (3, 1)]
YC = ("st_1", "st_2")


def near_ring(axis, own, right, left, far, sems, chunks):
    n = AXES[axis]
    me = lax.axis_index(axis)
    size = own.shape[0] // chunks

    def copy(k, d, ch):
        sgn = -1 if d else 1
        line = left if d else right
        last = k == n // 2 - 1
        lo, width = ch * size, size
        if last:
            width = size // 2
            lo = lo + (width if d else 0)
        rng = pl.ds(lo, width)
        src = own if k == 0 else line[k - 1]
        dst = far if last else line[k]
        return pltpu.make_async_remote_copy(
            src_ref=src.at[rng], dst_ref=dst.at[rng],
            send_sem=sems.at[0, d, k * chunks + ch], recv_sem=sems.at[1, d, k * chunks + ch],
            device_id={axis: lax.rem(me + sgn + n, n)}, device_id_type=MESH_ID)

    def start(k, sent):
        for ch in range(chunks):
            for d in range(2):
                cp = copy(k, d, ch)
                cp.start()
                sent.append(cp)

    def take(k, sent):
        for ch in range(chunks):
            for d in range(2):
                copy(k, d, ch).wait_recv()
                if k + 1 < n // 2:
                    cp = copy(k + 1, d, ch)
                    cp.start()
                    sent.append(cp)

    return start, take


def low_dot(a, b, dims=(((1,), (0,)), ((), ()))):
    return lax.dot_general(
        a.astype(jnp.bfloat16), b.astype(jnp.bfloat16), dims, preferred_element_type=jnp.float32)


def mixer_pieces(mq, mk, mv, st, ld, fresh, corr, attend, qdec, kdec, cdec, state, mixed):
    f32 = jnp.float32
    row_i = lax.broadcasted_iota(jnp.int32, (64, 64), 0)
    col_i = lax.broadcasted_iota(jnp.int32, (64, 64), 1)

    def prepare(m, n):
        def run():
            i = m * 6 + n
            rows, cols = pl.ds(n * 64, 64), pl.ds(m * 128, 128)
            q = mq[rows, cols].astype(f32)
            k = mk[rows, cols].astype(f32)
            v = mv[rows, cols].astype(f32)
            q = q * lax.rsqrt(jnp.sum(q * q, axis=-1, keepdims=True) + NORM_FLOOR) * 128 ** (-0.5)
            k = k * lax.rsqrt(jnp.sum(k * k, axis=-1, keepdims=True) + NORM_FLOOR)
            ld_row = jnp.broadcast_to(ld[i:i + 1, :], (64, 64))
            st_row = jnp.broadcast_to(st[i:i + 1, :], (64, 64))
            ld_col = jnp.sum(jnp.where(row_i == col_i, ld_row, 0.0), axis=1, keepdims=True)
            st_col = jnp.sum(jnp.where(row_i == col_i, st_row, 0.0), axis=1, keepdims=True)
            cum_col = jnp.sum(jnp.where(col_i <= row_i, ld_row, 0.0), axis=1, keepdims=True)
            cum_row = jnp.sum(jnp.where(row_i <= col_i, jnp.broadcast_to(ld_col, (64, 64)), 0.0), axis=0, keepdims=True)
            whole = jnp.sum(ld_col, axis=0, keepdims=True)
            decay = jnp.where(row_i >= col_i, jnp.exp(jnp.minimum(cum_col - cum_row, 0.0)), 0.0)
            gram = low_dot(k, k, CONTRACT_LAST)
            strict = jnp.where(row_i > col_i, st_col * gram * decay, 0.0)
            eye = jnp.where(row_i == col_i, 1.0, 0.0)
            running = eye - strict
            power = strict
            for _ in range(5):
                power = low_dot(power, power)
                running = low_dot(running, eye + power)
            grow = jnp.exp(cum_col)
            fresh[i] = low_dot(running, v * st_col)
            corr[i] = low_dot(running, k * (st_col * grow)).astype(jnp.bfloat16)
            attend[i] = (low_dot(q, k, CONTRACT_LAST) * decay).astype(jnp.bfloat16)
            qdec[i] = (q * grow).astype(jnp.bfloat16)
            kdec[i] = (k * jnp.exp(whole - cum_col)).astype(jnp.bfloat16)
            cdec[i] = jnp.broadcast_to(jnp.exp(whole), (8, 128))
        return run

    def advance(n):
        def run():
            for m in range(2):
                i = m * 6 + n
                rows, cols = pl.ds(n * 64, 64), pl.ds(m * 128, 128)
                if n == 0:
                    new = fresh[i]
                    mixed[rows, cols] = low_dot(attend[i], new)
                    state[m] = low_dot(kdec[i], new, CONTRACT_FIRST)
                else:
                    held = state[m]
                    new = fresh[i] - low_dot(corr[i], held)
                    mixed[rows, cols] = low_dot(qdec[i], held) + low_dot(attend[i], new)
                    if n < 5:
                        state[m] = held * cdec[i][0:1, :] + low_dot(kdec[i], new, CONTRACT_FIRST)
        return run

    return [prepare(m, n) for n in range(6) for m in range(2)], [advance(n) for n in range(6)]


def quarters(rows_ref, rows, w):
    acc = None
    for p in range(4):
        term = jnp.dot(rows_ref[rows, p * 512:(p + 1) * 512], w[p], preferred_element_type=jnp.float32)
        acc = term if acc is None else acc + term
    return acc


def forward_kernel(
    tok, cot, tab, tab_s, wq, gw, pas, wk, wv, mq, mk, mv, st, ld,
    cot_o, q_o, gate_o, code_o, tabs_o, qlow, gate, klow, vlow, mixed, wkc, wvc, wqc, gwc,
    t_r, t_l, t_f, c_r, c_l, c_f, q_own, q_r, q_l, q_f, g_r, g_l, g_f, b_r, b_l, b_f, tsm,
    cst, qst, gst, codest, fresh, corr, attend, qdec, kdec, cdec, state,
    s_t, s_c, s_q, s_g, s_b, s_m, s_cy, s_qy, s_gy, s_by, s_w0, s_w1, s_w2, s_w3,
):
    f32, bf16 = jnp.float32, jnp.bfloat16
    z = lax.axis_index("st_0")
    x = lax.axis_index("tp")
    jobs = [ring_peers(dict(axis="tp")), ring_peers(dict(axis="st_0")), a2a_peers(dict(axes=YC)),
            a2a_peers(dict(axes=("tp",)))]
    barrier = pltpu.get_barrier_semaphore()
    peers = [p for job in jobs for p in job]
    for p in peers:
        pl.semaphore_signal(barrier, inc=1, device_id=p, device_id_type=MESH_ID)
    pl.semaphore_wait(barrier, len(peers))
    sent = []
    b_start, b_take = near_ring("st_0", tab, b_r, b_l, b_f, s_b, 1)
    c_start, c_take = near_ring("st_0", cot, c_r, c_l, c_f, s_c, 3)
    t_start, t_take = near_ring("tp", tok, [t_r], [t_l], t_f, s_t, 3)
    q_start, q_take = near_ring("st_0", q_own, q_r, q_l, q_f, s_q, 3)
    g_start, g_take = near_ring("st_0", gate, g_r, g_l, g_f, s_g, 1)
    b_start(0, sent)
    t_start(0, sent)
    c_start(0, sent)

    my_yc, _ = index_of(YC, (0, 0), 1)
    dsts = [index_of(YC, s, 1) for s in SHIFTS]
    srcs = [index_of(YC, s, -1)[0] for s in SHIFTS]
    tabs = [None] + list(b_r) + list(b_l) + [b_f]
    origins = [lax.rem(z - d + 8, 8) for d in (0, 1, 2, 3, -1, -2, -3, 4)]

    def table_copy(i):
        return pltpu.make_async_copy(tabs[i].at[0], tsm.at[i - 1], s_m.at[i - 1])

    def block_for(i, j):
        code = tab_s[z, j] if i == 0 else tsm[i - 1, z, j]
        return lax.rem(code, 8)

    def push(i, buf, stage, out, sems):
        zr = origins[i]
        for s in range(7):
            stage[s, zr] = buf[block_for(i, dsts[s][0])]
        out[my_yc, zr] = buf[block_for(i, my_yc)]
        for s in range(7):
            cp = pltpu.make_async_remote_copy(
                src_ref=stage.at[s, zr], dst_ref=out.at[my_yc, zr], send_sem=sems.at[0, i, s],
                recv_sem=sems.at[1, i, s], device_id=dsts[s][1], device_id_type=MESH_ID)
            cp.start()
            sent.append(cp)

    def pulled(out, sems):
        for i in range(8):
            for s in range(7):
                pltpu.make_async_remote_copy(
                    src_ref=out.at[srcs[s], origins[i]], dst_ref=out.at[srcs[s], origins[i]],
                    send_sem=sems.at[0, i, s], recv_sem=sems.at[1, i, s], device_id=dsts[s][1],
                    device_id_type=MESH_ID).wait_recv()

    cots = [cot] + list(c_r) + list(c_l) + [c_f]
    qs = [q_own] + list(q_r) + list(q_l) + [q_f]
    gs = [gate] + list(g_r) + list(g_l) + [g_f]

    def project(t):
        def run():
            rows = pl.ds(t * 256, 256)
            klow[rows, :] = quarters(pas, rows, wk).astype(bf16)
            vlow[rows, :] = quarters(pas, rows, wv).astype(bf16)
        return run

    prep, scan = mixer_pieces(mq, mk, mv, st, ld, fresh, corr, attend, qdec, kdec, cdec, state, mixed)
    work = [project(t) for t in range(4)] + prep + scan
    work.reverse()

    def fill(count):
        for _ in range(count):
            if work:
                work.pop()()

    push(0, cot, cst, cot_o, s_cy)
    fill(2)
    b_take(0, sent)
    table_copy(1).start()
    table_copy(4).start()
    t_take(0, sent)
    c_take(0, sent)
    fill(1)
    for i in (1, 4):
        table_copy(i).wait()
        push(i, cots[i], cst, cot_o, s_cy)
    b_take(1, sent)
    table_copy(2).start()
    table_copy(5).start()
    c_take(1, sent)
    fill(1)
    for i in (2, 5):
        table_copy(i).wait()
        push(i, cots[i], cst, cot_o, s_cy)
    t_take(1, sent)

    parts = [(tok, x), (t_r, lax.rem(x + 3, 4)), (t_l, lax.rem(x + 1, 4)), (t_f, lax.rem(x + 2, 4))]
    for half in range(2):
        acc = None
        for buf, p in parts:
            rows = buf[half * 3:half * 3 + 3].reshape(192, 512)
            term = jnp.dot(rows, wq[p], preferred_element_type=f32)
            acc = term if acc is None else acc + term
        low = acc.astype(bf16)
        qlow[half * 192:half * 192 + 192, :] = low
        wide = low.astype(f32)
        norm = lax.rsqrt(jnp.mean(wide * wide, axis=-1, keepdims=True) + NORM_FLOOR)
        q_own[half * 3:half * 3 + 3] = (wide * norm).astype(bf16).reshape(3, 64, 256)
    for b in range(6):
        acc = None
        for buf, p in parts:
            term = lax.dot_general(gw[p], buf[b], CONTRACT_LAST, preferred_element_type=f32)
            acc = term if acc is None else acc + term
        gate[b, :, 0:64] = jax.nn.sigmoid(acc[0:8])
        gate[b, :, 64:128] = jnp.zeros((8, 64), f32)
    g_start(0, sent)
    q_start(0, sent)
    wcp = []
    for src, dst, sem in ((gw, gwc, s_w3), (wk, wkc, s_w0), (wv, wvc, s_w1), (wq, wqc, s_w2)):
        mine, cps = a2a_copies(dict(axes=("tp",)), src, dst, sem)
        for cp, _ in cps:
            cp.start()
            sent.append(cp)
        dst[mine] = src[mine]
        wcp += cps

    b_take(2, sent)
    table_copy(3).start()
    table_copy(6).start()
    c_take(2, sent)
    fill(1)
    for i in (3, 6):
        table_copy(i).wait()
        push(i, cots[i], cst, cot_o, s_cy)
    b_take(3, sent)
    table_copy(7).start()
    c_take(3, sent)
    push(0, q_own, qst, q_o, s_qy)
    fill(1)
    table_copy(7).wait()
    push(7, c_f, cst, cot_o, s_cy)
    g_take(0, sent)
    q_take(0, sent)
    for i in (1, 4):
        push(i, qs[i], qst, q_o, s_qy)
    fill(5)
    g_take(1, sent)
    q_take(1, sent)
    for i in (2, 5):
        push(i, qs[i], qst, q_o, s_qy)
    fill(5)
    g_take(2, sent)
    q_take(2, sent)
    for i in (3, 6):
        push(i, qs[i], qst, q_o, s_qy)
    fill(3)
    g_take(3, sent)
    q_take(3, sent)
    push(7, q_f, qst, q_o, s_qy)
    for i in range(8):
        zr = origins[i]
        table = tab if i == 0 else tabs[i]
        row = table[0, pl.ds(z, 1), :]
        codest[zr] = jnp.broadcast_to(row, (8, 128))
        tabs_o[zr] = jnp.broadcast_to(row, (8, 128))
        code_o[my_yc, zr] = jnp.broadcast_to(row, (8, 128))
        for s in range(7):
            gst[s, zr] = gs[i][block_for(i, dsts[s][0])]
        gate_o[my_yc, zr] = gs[i][block_for(i, my_yc)]
    side = []
    for s in range(7):
        for src, dst, sems in ((codest, code_o, s_by), (gst.at[s], gate_o, s_gy)):
            cp = pltpu.make_async_remote_copy(
                src_ref=src, dst_ref=dst.at[my_yc], send_sem=sems.at[0, s], recv_sem=sems.at[1, s],
                device_id=dsts[s][1], device_id_type=MESH_ID)
            cp.start()
            sent.append(cp)
            side.append(pltpu.make_async_remote_copy(
                src_ref=src, dst_ref=dst.at[srcs[s]], send_sem=sems.at[0, s], recv_sem=sems.at[1, s],
                device_id=dsts[s][1], device_id_type=MESH_ID))
    fill(99)
    for r in side:
        r.wait_recv()
    for _, r in wcp:
        r.wait_recv()
    pulled(cot_o, s_cy)
    pulled(q_o, s_qy)
    for cp in sent:
        cp.wait_send()


def forward(ins, cid):
    v = pl.BlockSpec(memory_space=pltpu.VMEM)
    f32, bf16, i32 = jnp.float32, jnp.bfloat16, jnp.int32
    sds = jax.ShapeDtypeStruct
    dma = pltpu.SemaphoreType.DMA
    slots = sds((8, 8, 64, 256), bf16)
    wide = sds((4, 512, 256), bf16)
    return pl.pallas_call(
        forward_kernel,
        out_shape=[
            slots, slots, sds((8, 8, 8, 128), f32), sds((8, 8, 8, 128), i32), sds((8, 8, 128), i32),
            sds((384, 256), bf16), sds((6, 8, 128), f32), sds((1024, 256), bf16), sds((1024, 256), bf16),
            sds((384, 256), f32), wide, wide, wide, sds((4, 16, 512), bf16)],
        in_specs=[v, v, v, pl.BlockSpec(memory_space=pltpu.SMEM)] + [v] * 10,
        out_specs=[v] * 14,
        scratch_shapes=[
            pltpu.VMEM((6, 64, 512), bf16), pltpu.VMEM((6, 64, 512), bf16), pltpu.VMEM((6, 64, 512), bf16),
            [pltpu.VMEM((6, 64, 256), bf16)] * 3, [pltpu.VMEM((6, 64, 256), bf16)] * 3, pltpu.VMEM((6, 64, 256), bf16),
            pltpu.VMEM((6, 64, 256), bf16),
            [pltpu.VMEM((6, 64, 256), bf16)] * 3, [pltpu.VMEM((6, 64, 256), bf16)] * 3, pltpu.VMEM((6, 64, 256), bf16),
            [pltpu.VMEM((6, 8, 128), f32)] * 3, [pltpu.VMEM((6, 8, 128), f32)] * 3, pltpu.VMEM((6, 8, 128), f32),
            [pltpu.VMEM((2, 8, 128), i32)] * 3, [pltpu.VMEM((2, 8, 128), i32)] * 3, pltpu.VMEM((2, 8, 128), i32),
            pltpu.SMEM((7, 8, 128), i32),
            pltpu.VMEM((7, 8, 64, 256), bf16), pltpu.VMEM((7, 8, 64, 256), bf16), pltpu.VMEM((7, 8, 8, 128), f32),
            pltpu.VMEM((8, 8, 128), i32),
            pltpu.VMEM((12, 64, 128), f32), pltpu.VMEM((12, 64, 128), bf16), pltpu.VMEM((12, 64, 64), bf16),
            pltpu.VMEM((12, 64, 128), bf16), pltpu.VMEM((12, 64, 128), bf16), pltpu.VMEM((12, 8, 128), f32),
            pltpu.VMEM((2, 128, 128), f32),
            dma((2, 2, 6)), dma((2, 2, 12)), dma((2, 2, 12)), dma((2, 2, 4)), dma((2, 2, 4)), dma((7,)),
            dma((2, 8, 7)), dma((2, 8, 7)), dma((2, 7)), dma((2, 7)),
            dma((2, 3)), dma((2, 3)), dma((2, 3)), dma((2, 3))],
        compiler_params=pltpu.CompilerParams(
            collective_id=cid, has_side_effects=True, vmem_limit_bytes=60 * 1024 * 1024),
    )(*ins)


def ring(axis, chunks=1):
    return dict(kind="ring", axis=axis, chunks=chunks)


def a2a(*axes):
    return dict(kind="a2a", axes=axes)


def rows_of(vec):
    flat = vec.reshape(-1, 128)
    return jnp.pad(flat, ((0, 16 - flat.shape[0]), (0, 0)))


def stats_kernel(x_ref, m_ref, o_ref, whole, got, tot, every, back, s1, s2, s3):
    job = a2a(*YC)
    barrier = pltpu.get_barrier_semaphore()
    peers = a2a_peers(job) + a2a_peers(a2a("st_0"))
    for p in peers:
        pl.semaphore_signal(barrier, inc=1, device_id=p, device_id_type=MESH_ID)
    pl.semaphore_wait(barrier, len(peers))
    sent = []
    mine, cps = a2a_copies(job, x_ref, got, s1)
    for cp, _ in cps:
        cp.start()
        sent.append(cp)
    got[mine] = x_ref[mine]
    for _, r in cps:
        r.wait_recv()
    for b in range(6):
        acc = got[0] * m_ref[0, b]
        for j in range(1, 8):
            acc = acc + got[j] * m_ref[j, b]
        tot[b] = acc
    z = lax.axis_index("st_0")
    arrivals = []
    for s in range(1, 8):
        dst = lax.rem(z + s, 8)
        src = lax.rem(z - s + 8, 8)
        cp = pltpu.make_async_remote_copy(
            src_ref=tot, dst_ref=every.at[z], send_sem=s2.at[0, s], recv_sem=s2.at[1, s],
            device_id={"st_0": dst}, device_id_type=MESH_ID)
        rv = pltpu.make_async_remote_copy(
            src_ref=tot, dst_ref=every.at[src], send_sem=s2.at[0, s], recv_sem=s2.at[1, s],
            device_id={"st_0": dst}, device_id_type=MESH_ID)
        cp.start()
        sent.append(cp)
        arrivals.append(rv)
    every[z] = tot[...]
    for rv in arrivals:
        rv.wait_recv()
    for b in range(6):
        acc = every[0, b]
        for k in range(1, 8):
            acc = acc + every[k, b]
        whole[b] = acc
    for j in range(8):
        acc = whole[0] * m_ref[j, 0]
        for b in range(1, 6):
            acc = acc + whole[b] * m_ref[j, b]
        back[j] = acc
    mine, cps3 = a2a_copies(job, back, o_ref, s3)
    for cp, _ in cps3:
        cp.start()
        sent.append(cp)
    o_ref[mine] = back[mine]
    for _, r in cps3:
        r.wait_recv()
    for cp in sent:
        cp.wait_send()


def stats_exchange(x, mask, cid):
    v = pl.BlockSpec(memory_space=pltpu.VMEM)
    f = jnp.float32
    return pl.pallas_call(
        stats_kernel,
        out_shape=[jax.ShapeDtypeStruct(x.shape, f), jax.ShapeDtypeStruct((6, 8, 256), f)],
        in_specs=[v] * 2,
        out_specs=[v] * 2,
        scratch_shapes=[
            pltpu.VMEM((8, 8, 256), f), pltpu.VMEM((6, 8, 256), f), pltpu.VMEM((8, 6, 8, 256), f),
            pltpu.VMEM((8, 8, 256), f), pltpu.SemaphoreType.DMA((2, 7)), pltpu.SemaphoreType.DMA((2, 8)),
            pltpu.SemaphoreType.DMA((2, 7))],
        compiler_params=pltpu.CompilerParams(collective_id=cid, has_side_effects=True),
    )(x, mask)


def tail_kernel(kg, vg, w, kg_o, vg_o, w_o, wc, wcs, wy, wys, wz, s_k, s_v, s_c, s_y, s_z):
    barrier = pltpu.get_barrier_semaphore()
    peers = ring_peers(ring("tp")) + a2a_peers(a2a("st_2")) + a2a_peers(a2a("st_1")) + a2a_peers(a2a("st_0"))
    for p in peers:
        pl.semaphore_signal(barrier, inc=1, device_id=p, device_id_type=MESH_ID)
    pl.semaphore_wait(barrier, len(peers))
    sent = []
    rings = []
    for src, dst, sems in ((kg, kg_o, s_k), (vg, vg_o, s_v)):
        c, a, steps, chunks = ring_starts(ring("tp", 2), src, dst, sems)
        rings.append((c, a))
        for ch in range(2):
            for d in range(2):
                cp = c(0, d, ch)
                cp.start()
                sent.append(cp)
    core = lax.axis_index("st_2")
    pair = pltpu.make_async_remote_copy(
        src_ref=w.at[1 - core], dst_ref=wc, send_sem=s_c.at[0], recv_sem=s_c.at[1],
        device_id={"st_2": 1 - core}, device_id_type=MESH_ID)
    pair.start()
    sent.append(pair)
    x = lax.axis_index("tp")
    kg_o[x] = kg[...]
    vg_o[x] = vg[...]
    pair.wait_recv()
    for y in range(4):
        wcs[y] = w[core, y] + wc[y]
    ym, ycp = a2a_copies(a2a("st_1"), wcs, wy, s_y)
    for cp, _ in ycp:
        cp.start()
        sent.append(cp)
    wy[ym] = wcs[ym]
    for c, a in rings:
        for ch in range(2):
            for d in range(2):
                a(0, d, ch).wait_recv()
                cp = c(1, d, ch)
                cp.start()
                sent.append(cp)
    for _, r in ycp:
        r.wait_recv()
    for k in range(8):
        wys[k] = (wy[0, k] + wy[1, k]) + (wy[2, k] + wy[3, k])
    zm, zcp = a2a_copies(a2a("st_0"), wys, wz, s_z)
    for cp, _ in zcp:
        cp.start()
        sent.append(cp)
    wz[zm] = wys[zm]
    for c, a in rings:
        for ch in range(2):
            for d in range(2):
                a(1, d, ch).wait_recv()
    for _, r in zcp:
        r.wait_recv()
    acc = wz[0]
    for k in range(1, 8):
        acc = acc + wz[k]
    w_o[...] = acc
    for cp in sent:
        cp.wait_send()


def tail(kg, vg, w, cid):
    v = pl.BlockSpec(memory_space=pltpu.VMEM)
    f32, bf16 = jnp.float32, jnp.bfloat16
    dma = pltpu.SemaphoreType.DMA
    return pl.pallas_call(
        tail_kernel,
        out_shape=[
            jax.ShapeDtypeStruct((4, 1024, 256), bf16), jax.ShapeDtypeStruct((4, 1024, 256), bf16),
            jax.ShapeDtypeStruct((32, 256), f32)],
        in_specs=[v] * 3,
        out_specs=[v] * 3,
        scratch_shapes=[
            pltpu.VMEM((4, 8, 32, 256), f32), pltpu.VMEM((4, 8, 32, 256), f32), pltpu.VMEM((4, 8, 32, 256), f32),
            pltpu.VMEM((8, 32, 256), f32), pltpu.VMEM((8, 32, 256), f32),
            dma((2, 2, 4)), dma((2, 2, 4)), dma((2,)), dma((2, 3)), dma((2, 7))],
        compiler_params=pltpu.CompilerParams(
            collective_id=cid, has_side_effects=True, vmem_limit_bytes=40 * 1024 * 1024),
    )(kg, vg, w)


def body(
    tokens, cotangent, mix_query, mix_key, mix_value, beta_pre, decay_pre, decay_rate,
    passages, passage_ids, query_weight, key_weight, value_weight, gate_weight,
):
    f32, bf16 = jnp.float32, jnp.bfloat16
    scale = SCORE_GAIN * 256 ** (-0.5)
    z = lax.axis_index("st_0")
    my_yc = lax.axis_index(YC)
    ids = passage_ids.reshape(24)
    owner, local = ids // 16, ids % 16
    match = owner[None, :] == jnp.arange(64, dtype=jnp.int32)[:, None]
    code_of = local * 8 + jnp.arange(24, dtype=jnp.int32) // 4
    code = jnp.sum(jnp.where(match, code_of[None, :], 0), axis=-1, dtype=jnp.int32)
    code = jnp.where(jnp.any(match, axis=-1), code, 128).reshape(8, 8)
    table = jnp.pad(code[None], ((0, 1), (0, 0), (0, 120)))
    gw4 = jnp.broadcast_to(gate_weight.reshape(4, 1, 512), (4, 16, 512))
    strength = jax.nn.sigmoid(beta_pre).reshape(12, 64)
    log_decay = (-decay_rate[:, None] * jax.nn.softplus(decay_pre)).reshape(12, 64)
    flat_rows = passages.reshape(1024, 2048)
    (cot_here, q_here, gate_o, code_o, tabs, query_low, gate6, key_low, value_all, mixer_out,
     wk_cols, wv_cols, wq_cols, gw_cols) = forward(
        [tokens.reshape(6, 64, 512), cotangent.reshape(6, 64, 256), table, code,
         query_weight.reshape(4, 512, 256), gw4, flat_rows, key_weight.reshape(4, 512, 256), value_weight.reshape(4, 512, 256),
         mix_query, mix_key, mix_value, strength, log_decay], 1)
    cot_here, q_here = cot_here.reshape(64, 64, 256), q_here.reshape(64, 64, 256)
    codes = tabs[:, 0, :8]
    gate_here = gate_o[:, :, 0, :64].reshape(64, 64)
    code_here = lax.dynamic_slice(code_o, (0, 0, 0, my_yc), (8, 8, 1, 1)).reshape(64)
    used = code_here < 128
    loc = jnp.where(used, code_here // 8, 0)
    gate_open = gate6[:, 0, :64].reshape(384)
    query_float = query_low.astype(f32)
    query_scale = lax.rsqrt(jnp.mean(query_float * query_float, axis=-1, keepdims=True) + NORM_FLOOR)

    key_float = key_low.astype(f32)
    key_scale = lax.rsqrt(jnp.mean(key_float * key_float, axis=-1, keepdims=True) + NORM_FLOOR)
    key_hat = (key_float * key_scale).astype(bf16)
    k_sel = key_hat.reshape(16, 64, 256)[loc]
    v_sel = value_all.reshape(16, 64, 256)[loc]

    scores = jnp.einsum("sid,sjd->sij", q_here, k_sel, preferred_element_type=f32) * scale
    exps = jnp.exp(scores)
    g_here = (gate_here[:, :, None] * cot_here.astype(f32)).astype(bf16)
    grad_probs = jnp.einsum("sid,sjd->sij", g_here, v_sel, preferred_element_type=f32)
    cot_dots = jnp.einsum("sid,sjd->sij", cot_here, v_sel, preferred_element_type=f32)
    sums = jnp.concatenate(
        [jnp.sum(exps, axis=-1), jnp.sum(exps * grad_probs, axis=-1), jnp.sum(exps * cot_dots, axis=-1),
         jnp.zeros((64, 64), f32)], axis=-1)

    blk = jnp.where(codes < 128, codes % 8, 7)
    mask = (blk.T[:, None, :] == jnp.arange(6, dtype=jnp.int32)[None, :, None]).astype(f32)
    mask = jnp.broadcast_to(mask[..., None], (8, 6, 8, 256))
    whole, mine = stats_exchange(sums.reshape(8, 8, 256), mask, 2)
    whole = whole.reshape(64, 256)
    mine = lax.dynamic_slice(mine, (0, z, 0), (6, 1, 256)).reshape(6, 256)
    read_dot = (mine[:, 128:192] / mine[:, :64]).reshape(384)
    total = jnp.where(used[:, None], whole[:, :64], 1.0)
    inner = jnp.where(used[:, None], whole[:, 64:128], 0.0) / total
    probs = jnp.where(used[:, None, None], exps, 0.0) / total[:, :, None]
    probs_low = probs.astype(bf16)
    score_grad = (probs * (grad_probs - inner[:, :, None])).astype(bf16)
    q_part = (scale * jnp.einsum("sij,sjd->sid", score_grad, k_sel, preferred_element_type=f32)).astype(bf16)
    q_part = jnp.moveaxis(q_part.reshape(8, 8, 64, 256), 0, 1).reshape(64, 64, 256)
    q_back = lax.all_to_all(q_part, ST, split_axis=0, concat_axis=0, tiled=True)

    key_term = (scale * jnp.einsum("sij,sid->sjd", score_grad, q_here, preferred_element_type=f32)).astype(bf16)
    value_term = jnp.einsum("sij,sid->sjd", probs_low, g_here, preferred_element_type=f32).astype(bf16)
    onehot = ((loc[None, :] == jnp.arange(16, dtype=jnp.int32)[:, None]) & used[None, :]).astype(bf16)
    key_grad_hat = jnp.dot(onehot, key_term.reshape(64, -1), preferred_element_type=f32).reshape(1024, 256)
    value_grad = jnp.dot(onehot, value_term.reshape(64, -1), preferred_element_type=f32).reshape(1024, 256)
    key_grad = (
        key_scale * key_grad_hat
        - key_scale**3 * key_float * jnp.mean(key_float * key_grad_hat, axis=-1, keepdims=True)
    ).astype(bf16)
    value_grad_low = value_grad.astype(bf16)
    weight_term = lax.dot_general(flat_rows, key_grad, CONTRACT_FIRST, preferred_element_type=f32)
    weight_term = jnp.transpose(weight_term.reshape(8, 4, 2, 32, 256), (2, 1, 0, 3, 4))
    kg4, vg4, key_weight_grad = tail(key_grad, value_grad_low, weight_term, 3)
    row_part = (
        jnp.einsum("hrd,hed->hre", kg4, wk_cols, preferred_element_type=f32)
        + jnp.einsum("hrd,hed->hre", vg4, wv_cols, preferred_element_type=f32)
    ).astype(bf16)
    passage_grad = jnp.sum(row_part.astype(f32), axis=0).astype(bf16).reshape(16, 64, 512)

    qhat_grad = jnp.sum(q_back[owner].astype(f32).reshape(6, 4, 64, 256), axis=1).reshape(384, 256)
    grad_out = cotangent.astype(f32)
    gate_grad = (read_dot - jnp.sum(grad_out * mixer_out, axis=-1)) * gate_open * (1.0 - gate_open)
    query_grad = (
        query_scale * qhat_grad
        - query_scale**3 * query_float * jnp.mean(query_float * qhat_grad, axis=-1, keepdims=True)
    ).astype(bf16)
    qg4, gg4 = comm([ring("tp"), ring("tp")], [query_grad, rows_of(gate_grad)], 4)
    gg4 = gg4[:, :3].reshape(4, 384)
    token_part = (
        jnp.einsum("htd,hed->hte", qg4, wq_cols, preferred_element_type=f32)
        + gg4[:, :, None] * gw_cols[:, 0].astype(f32)[:, None, :]
    ).astype(bf16)
    token_grad = jnp.sum(token_part.astype(f32), axis=0).astype(bf16)
    return token_grad, passage_grad, key_weight_grad


def solution(mesh):
    torus = Mesh(mesh.devices.reshape(8, 4, 2, mesh.shape["tp"]), ("st_0", "st_1", "st_2", "tp"))
    return jax.shard_map(
        body,
        mesh=torus,
        in_specs=(
            P(ST, "tp"),
            P(ST, "tp"),
            P(ST, "tp"),
            P(ST, "tp"),
            P(ST, "tp"),
            P("tp", ST),
            P("tp", ST),
            P("tp"),
            P(ST, None, None),
            P(ST, None),
            P(None, "tp"),
            P(None, "tp"),
            P(None, "tp"),
            P("tp", None),
        ),
        out_specs=(P(ST, "tp"), P(ST, None, "tp"), P(ST, "tp")),
        check_vma=False,
    )
```

time: 379 us -> 233 us (0.61)
  matrix products: 78.2 us -> 20.7 us
  Pallas kernels: 198 us -> 160 us
  waiting for transfers between devices: 19.8 us -> 0.01 us
  local copies, waits for them, and re-layouts: 43.8 us -> 30.3 us
  starting transfers between devices: 16 us -> 6.22 us
  other arithmetic: 17.1 us -> 12.8 us
    pallas_call x6 -> x1, Pallas kernels: 137 us -> 13.3 us  [comm(): pl.pallas_call(functools.partial(comm_kernel, jobs), out_shape=outs, in_s...]
    pallas_call x1 -> x2, Pallas kernels: 42.1 us -> 123 us  [the longest x1 81 us: forward(): pl.pallas_call(forward_kernel, out_shape=[slots, slots, sds((8, 8, 8, 128...]
    dot_general x39 -> x0, matrix products: 45.4 us -> none  [the longest x6 9.18 us: advance(): jnp.einsum('hcm,hme->hce', attend_blk, new_values)]
    all_to_all x2 -> x0, waiting for transfers between devices: 19.8 us -> none  [the longest x1 19.8 us: body(): lax.all_to_all(q_slots, YC, split_axis=0, concat_axis=0, tiled=True)]
    all_to_all x2 -> x0, starting transfers between devices: 9.13 us -> none  [the longest x1 4.61 us: body(): lax.all_to_all(cot_slots, YC, split_axis=0, concat_axis=0, tiled=True)]
    gather x3 -> x0, local copies, waits for them, and re-layouts: 7.53 us -> none  [the longest x1 3.49 us: body(): q_slots = q_z.reshape(48, 64, 256)[slot_block]]
    add x2 -> x0, other arithmetic: 4.6 us -> none  [the longest x1 2.65 us: body(): w_c[0] + w_c[1]]
    pallas_call x1, Pallas kernels: 19.6 us -> 23.8 us  [stats_exchange(): pl.pallas_call(stats_kernel, out_shape=[jax.ShapeDtypeStruct(x.shape, f),...]
  transfers between devices with their start and end apart: 3 -> 1, of which waited for: 1 -> 0; matrix products, arithmetic and copies ran while one was open for 28% -> 11% of each run, Pallas kernels for 35% -> 18%
where the time goes in v2:
time: 233 us; the launch traced here: 231 us
  Pallas kernels  160 us (69%)
  local copies, waits for them, and re-layouts  30.3 us (13%)
  matrix products  20.7 us (9%)
  other arithmetic  12.8 us (5%)
  starting transfers between devices  6.22 us (3%)
    pallas_call x1, Pallas kernels, forward(): pl.pallas_call(forward_kernel, out_shape=[slots, slots, sds((8, 8, 8, 128...  81 us
    pallas_call x1, Pallas kernels, tail(): pl.pallas_call(tail_kernel, out_shape=[jax.ShapeDtypeStruct((4, 1024, 256...  42.2 us
    pallas_call x1, Pallas kernels, stats_exchange(): pl.pallas_call(stats_kernel, out_shape=[jax.ShapeDtypeStruct(x.shape, f),...  23.8 us
    pallas_call x1, Pallas kernels, comm(): pl.pallas_call(functools.partial(comm_kernel, jobs), out_shape=outs, in_s...  13.3 us
    unnamed x40, local copies, waits for them, and re-layouts  6.53 us
    all_to_all x1, starting transfers between devices, body(): q_back = lax.all_to_all(q_part, ST, split_axis=0, concat_axis=0, tiled=True)  6.22 us
    dot_general x1, matrix products, body(): lax.dot_general(flat_rows, key_grad, CONTRACT_FIRST, preferred_element_ty...  4.81 us
  transfers between devices with their start and end apart: 1, of which 0 were waited for; matrix products, arithmetic and copies ran while one was open for 11% of the time, Pallas kernels for 18%

profile of v2, /device:TPU:2, one launch (start us, length us, event | category | flops | bytes accessed | tf_op | source)
XLA Modules:
  0.0 231.4 jit_solution(5076838915688923655)
XLA Ops:
  0.6 0.8 copy.28
  7.9 81.0 %shard_map.157 = (bf16[8,8,64,256]{3,2,1,0:T(8,128)(2,1)}, bf16[8,8,64,256]{3,2,1,0:T(8,128)(2,1)}, f32[8,8,8,128]{3,2,1,0:T(8,128)}, s32[8,8,8,128]{3,2,1,0:T(8...) custom-call(bf16[6,64,512]{2,1,0:T(8,128)(2,1)} %bitcast.101, ...), custom_call_target="tpu_custom_call" | custom-call | tf_op jit(solution)/shard_map/pallas_call | solution.py:486
  88.9 2.3 dynamic-slice_reduce_fusion
  91.4 1.0 slice.27
  92.3 1.3 fusion.3
  93.6 1.2 fusion.4
  95.6 2.0 gather_fusion
  97.6 2.4 %fusion.1 = f32[64,64,64]{1,2,0:T(8,128)S(1)} fusion(bf16[64,64,256]{2,1,0:T(8,128)(2,1)S(1)} %gather_fusion.1, bf16[64,64,256]{2,1,0:T(8,128)(2,1)} %bitcast.81, f32[64,64]{1,0:T(8,128)S(1)} %bitcast.102), kind=kOutput, calls=%fused_computation.22 | convolution fusion | flops 137363456 | bytes 5259264 | tf_op jit(solution)/shard_map/sid,sjd->sij/dot_general | solution.py:728
  100.4 0.9 fusion.38
  101.4 1.0 copy-done.5
  104.7 0.9 broadcast_in_dim.100.m_ref
  105.5 23.8 %shard_map.158 = (f32[8,8,256]{2,1,0:T(8,128)}, f32[6,8,256]{2,1,0:T(8,128)}) custom-call(f32[8,8,256]{2,1,0:T(8,128)} %maximum_bitcast_fusion.x_ref, f32[8,6,8,256]{3,2,1,0:T(8,128)} %broadcast_in_dim.100.m_ref), custom_call_target="tpu_custom_call" | custom-call | tf_op jit(solution)/shard_map/pallas_call | solution.py:589
  129.4 0.9 slice_select_fusion.1
  130.3 2.8 %multiply_convert_fusion.3 = bf16[64,64,64]{1,2,0:T(8,128)(2,1)S(1)} fusion(f32[64,64,64]{1,2,0:T(8,128)} %copy-done.2, f32[64,64]{1,0:T(8,128)S(1)} %get-tuple-element.50, f32[64,64]{1,0:T(8,128)S(1)} %get-tuple-element.49, f32[64,64,64]{1,2,0:T(8,128)} %copy-done, pred[64]{0:T(512)(128)(4,1)S(1)} %broadcast_compare_fusion), kind=kLoop, calls=%fused_computation.12 | loop fusion | flops 1310720 | bytes 2654272 | tf_op jit(solution)/shard_map/convert_element_type | solution.py:745
  133.9 1.5 copy.31
  135.4 6.2 %all-to-all-start = ((bf16[64,64,256]{2,1,0:T(8,128)(2,1)}), bf16[64,64,256]{2,1,0:T(8,128)(2,1)}, u32[]{:S(2)}, u32[]{:S(2)}) async-start(bf16[64,64,256]{2,1,0:T(8,128)(2,1)} %bitcast.18), calls=%async_computation | async-start | bytes 4194304 | tf_op jit(solution)/shard_map/all_to_all | solution.py:748
  143.3 0.8 constant_dynamic-slice_fusion
  144.9 1.3 copy.39
  146.2 1.4 fusion.20
  147.6 1.4 reshape.474
  149.0 2.4 %convolution_convert_fusion.1 = bf16[64,64,256]{2,1,0:T(8,128)(2,1)S(1)} fusion(bf16[64,64,256]{2,1,0:T(8,128)(2,1)} %bitcast.82, f32[64,64]{1,0:T(8,128)S(1)} %bitcast.103, f32[64,64,64]{1,2,0:T(8,128)S(1)} %copy-done.1, f32[64,64]{1,0:T(8,128)S(1)} %get-tuple-element.49, pred[64]{0:T(512)(128)(4,1)S(1)} %broadcast_compare_fusion), kind=kOutput, calls=%fused_computation.17 | convolution fusion | flops 139198464 | bytes 5275712 | tf_op jit(solution)/shard_map/sij,sid->sjd/dot_general | solution.py:751
  151.4 1.3 copy.40
  154.4 4.8 %convolution_bitcast_fusion = f32[2048,256]{0,1:T(8,128)} fusion(bf16[1024,256]{1,0:T(8,128)(2,1)S(1)} %fusion.7.kg, bf16[1024,2048]{1,0:T(8,128)(2,1)} %bitcast.93), kind=kOutput, calls=%fused_computation.10 | convolution fusion | flops 1073741824 | bytes 6815744 | tf_op jit(solution)/shard_map/dot_general | solution.py:760
  159.3 2.9 %copy.33 = f32[2048,256]{1,0:T(8,128)} copy(f32[2048,256]{0,1:T(8,128)} %convolution_bitcast_fusion) | data formatting | bytes 4194304 | tf_op jit(solution)/shard_map/dot_general | solution.py:760
  162.1 1.8 copy.45
  164.0 42.2 %shard_map.160 = (bf16[4,1024,256]{2,1,0:T(8,128)(2,1)S(1)}, bf16[4,1024,256]{2,1,0:T(8,128)(2,1)S(1)}, f32[32,256]{1,0:T(8,128)S(1)}) custom-call(bf16[1024,256]{1,0:T(8,128)(2,1)S(1)} %fusion.7.kg, bf16[1024,256]{1,0:T(8,128)(2,1)S(1)} %convert_element_type.91.vg, f32[2,4,8,32,256]{4,3,2,1,0:T(8,128)S(1)} %bitcast.79), custom_call_target="tpu_custom_call" | custom-call | tf_op jit(solution)/shard_map/pallas_call | solution.py:669
  206.3 1.3 fusion.39
  207.6 2.4 %fusion = bf16[1024,512]{1,0:T(8,128)(2,1)} fusion(f32[4,1024,512]{2,1,0:T(8,128)S(1)} %fusion.39, bf16[4,1024,256]{2,1,0:T(8,128)(2,1)S(1)} %get-tuple-element.42, bf16[4,512,256]{2,1,0:T(8,128)(2,1)S(1)} %copy-done.11), kind=kOutput, calls=%fused_computation.5 | convolution fusion | flops 1079508992 | bytes 12582912 | tf_op jit(solution)/shard_map/hrd,hed->hre/dot_general | solution.py:765
  210.0 2.3 gather_fusion.2
  213.3 0.9 fusion.13.refs_0_
  214.2 13.3 %shard_map.159 = (bf16[4,384,256]{2,1,0:T(8,128)(2,1)}, f32[4,16,128]{2,1,0:T(8,128)}) custom-call(bf16[384,256]{1,0:T(8,128)(2,1)} %fusion.13.refs_0_, f32[16,128]{1,0:T(8,128)} %pad.9.refs_1_), custom_call_target="tpu_custom_call" | custom-call | tf_op jit(solution)/shard_map/pallas_call | solution.py:157
  228.2 2.6 %fusion.2 = bf16[384,512]{1,0:T(8,128)(2,1)} fusion(f32[4,512]{1,0:T(4,128)S(1)} %bitcast.107, f32[4,384]{1,0:T(4,128)S(1)} %bitcast.108, bf16[4,384,256]{2,1,0:T(8,128)(2,1)} %get-tuple-element.36, bf16[4,512,256]{2,1,0:T(8,128)(2,1)S(1)} %copy-done.15), kind=kOutput, calls=%fused_computation.24 | convolution fusion | flops 405602304 | bytes 2242560 | tf_op jit(solution)/shard_map/htd,hed->hte/dot_general | solution.py:779
  (89 shorter events, 17.4 us)
Async XLA Ops:
  88.9 6.0 %copy-start.7 = (bf16[1024,256]{1,0:T(8,128)(2,1)S(1)}, bf16[1024,256]{1,0:T(8,128)(2,1)}, u32[]{:S(2)}) copy-start(bf16[1024,256]{1,0:T(8,128)(2,1)} %get-tuple-element.30) | copy-start | bytes 1572868
  97.6 2.4 %copy-start.3 = (bf16[64,64,256]{2,1,0:T(8,128)(2,1)S(1)}, bf16[64,64,256]{2,1,0:T(8,128)(2,1)}, u32[]{:S(2)}) copy-start(bf16[64,64,256]{2,1,0:T(8,128)(2,1)} %gather_fusion) | copy-start | bytes 6291460
  97.6 2.9 %copy-start.8 = (bf16[8,8,64,256]{3,2,1,0:T(8,128)(2,1)S(1)}, bf16[8,8,64,256]{3,2,1,0:T(8,128)(2,1)}, u32[]{:S(2)}) copy-start(bf16[8,8,64,256]{3,2,1,0:T(8,128)(2,1)} %get-tuple-element.26) | copy-start | bytes 6291460
  100.0 1.3 copy-start.2
  100.4 1.9 copy-start.5
  101.4 1.7 copy-start
  130.3 2.9 %copy-start.4 = (bf16[64,64,256]{2,1,0:T(8,128)(2,1)S(1)}, bf16[64,64,256]{2,1,0:T(8,128)(2,1)}, u32[]{:S(2)}) copy-start(bf16[64,64,256]{2,1,0:T(8,128)(2,1)} %gather_fusion) | copy-start | bytes 6291460
  135.4 8.8 %copy-start.9 = (bf16[8,8,64,256]{3,2,1,0:T(8,128)(2,1)S(1)}, bf16[8,8,64,256]{3,2,1,0:T(8,128)(2,1)}, u32[]{:S(2)}) copy-start(bf16[8,8,64,256]{3,2,1,0:T(8,128)(2,1)} %get-tuple-element.26) | copy-start | bytes 6291460
  135.4 74.6 %all-to-all-start = ((bf16[64,64,256]{2,1,0:T(8,128)(2,1)}), bf16[64,64,256]{2,1,0:T(8,128)(2,1)}, u32[]{:S(2)}, u32[]{:S(2)}) async-start(bf16[64,64,256]{2,1,0:T(8,128)(2,1)} %bitcast.18), calls=%async_computation | async-start | bytes 4194304 | tf_op jit(solution)/shard_map/all_to_all | solution.py:748
  146.2 2.8 %copy-start.1 = (f32[64,64,64]{1,2,0:T(8,128)S(1)}, f32[64,64,64]{1,2,0:T(8,128)}, u32[]{:S(2)}) copy-start(f32[64,64,64]{1,2,0:T(8,128)} %copy-done) | copy-start | bytes 3145732
  152.7 1.0 copy-start.6
  164.0 42.3 %copy-start.10 = (bf16[4,512,256]{2,1,0:T(8,128)(2,1)S(1)}, bf16[4,512,256]{2,1,0:T(8,128)(2,1)}, u32[]{:S(2)}) copy-start(bf16[4,512,256]{2,1,0:T(8,128)(2,1)} %get-tuple-element.41) | copy-start | bytes 3145732
  206.3 1.3 copy-start.11
  210.0 2.4 %copy-start.12 = (bf16[384,256]{1,0:T(8,128)(2,1)S(1)}, bf16[384,256]{1,0:T(8,128)(2,1)}, u32[]{:S(2)}) copy-start(bf16[384,256]{1,0:T(8,128)(2,1)} %get-tuple-element.24) | copy-start | bytes 589828
  210.0 2.4 %copy-start.13 = (bf16[384,256]{1,0:T(8,128)(2,1)S(1)}, bf16[384,256]{1,0:T(8,128)(2,1)}, u32[]{:S(2)}) copy-start(bf16[384,256]{1,0:T(8,128)(2,1)} %param.15) | copy-start | bytes 589828
  210.0 2.4 %copy-start.14 = (f32[384,256]{1,0:T(8,128)S(1)}, f32[384,256]{1,0:T(8,128)}, u32[]{:S(2)}) copy-start(f32[384,256]{1,0:T(8,128)} %get-tuple-element.34) | copy-start | bytes 1179652
  212.3 16.0 %copy-start.15 = (bf16[4,512,256]{2,1,0:T(8,128)(2,1)S(1)}, bf16[4,512,256]{2,1,0:T(8,128)(2,1)}, u32[]{:S(2)}) copy-start(bf16[4,512,256]{2,1,0:T(8,128)(2,1)} %get-tuple-element.37) | copy-start | bytes 3145732

commit v3 on v2

--- a/solution.py
+++ b/solution.py
@@ -196,8 +196,8 @@
                 cp.start()
                 sent.append(cp)
 
-    def take(k, sent):
-        for ch in range(chunks):
+    def take(k, sent, which=None):
+        for ch in range(chunks) if which is None else (which,):
             for d in range(2):
                 copy(k, d, ch).wait_recv()
                 if k + 1 < n // 2:
@@ -213,7 +213,7 @@
         a.astype(jnp.bfloat16), b.astype(jnp.bfloat16), dims, preferred_element_type=jnp.float32)
 
 
-def mixer_pieces(mq, mk, mv, st, ld, fresh, corr, attend, qdec, kdec, cdec, state, mixed):
+def mixer_pieces(mq, mk, mv, st, ld, rate, fresh, corr, attend, qdec, kdec, cdec, state, mixed):
     f32 = jnp.float32
     row_i = lax.broadcasted_iota(jnp.int32, (64, 64), 0)
     col_i = lax.broadcasted_iota(jnp.int32, (64, 64), 1)
@@ -227,8 +227,10 @@
             v = mv[rows, cols].astype(f32)
             q = q * lax.rsqrt(jnp.sum(q * q, axis=-1, keepdims=True) + NORM_FLOOR) * 128 ** (-0.5)
             k = k * lax.rsqrt(jnp.sum(k * k, axis=-1, keepdims=True) + NORM_FLOOR)
-            ld_row = jnp.broadcast_to(ld[i:i + 1, :], (64, 64))
-            st_row = jnp.broadcast_to(st[i:i + 1, :], (64, 64))
+            pre = ld[m:m + 1, n * 64:n * 64 + 64]
+            soft = jnp.maximum(pre, 0.0) + jnp.log1p(jnp.exp(-jnp.abs(pre)))
+            ld_row = jnp.broadcast_to(-rate[m] * soft, (64, 64))
+            st_row = jnp.broadcast_to(jax.nn.sigmoid(st[m:m + 1, n * 64:n * 64 + 64]), (64, 64))
             ld_col = jnp.sum(jnp.where(row_i == col_i, ld_row, 0.0), axis=1, keepdims=True)
             st_col = jnp.sum(jnp.where(row_i == col_i, st_row, 0.0), axis=1, keepdims=True)
             cum_col = jnp.sum(jnp.where(col_i <= row_i, ld_row, 0.0), axis=1, keepdims=True)
@@ -281,11 +283,11 @@
 
 
 def forward_kernel(
-    tok, cot, tab, tab_s, wq, gw, pas, wk, wv, mq, mk, mv, st, ld,
-    cot_o, q_o, gate_o, code_o, tabs_o, qlow, gate, klow, vlow, mixed, wkc, wvc, wqc, gwc,
+    tok, cot, tab, wq, gw, pas, wk, wv, mq, mk, mv, st, ld, rate,
+    cot_o, q_o, gate_o, tabs_o, qlow, gate, klow, khat, vlow, mixed, wkc, wvc, wqc, gwc,
     t_r, t_l, t_f, c_r, c_l, c_f, q_own, q_r, q_l, q_f, g_r, g_l, g_f, b_r, b_l, b_f, tsm,
-    cst, qst, gst, codest, fresh, corr, attend, qdec, kdec, cdec, state,
-    s_t, s_c, s_q, s_g, s_b, s_m, s_cy, s_qy, s_gy, s_by, s_w0, s_w1, s_w2, s_w3,
+    cst, qst, gst, fresh, corr, attend, qdec, kdec, cdec, state,
+    s_t, s_c, s_q, s_g, s_b, s_m, s_cy, s_qy, s_gy, s_w0, s_w1, s_w2, s_w3,
 ):
     f32, bf16 = jnp.float32, jnp.bfloat16
     z = lax.axis_index("st_0")
@@ -310,24 +312,23 @@
     my_yc, _ = index_of(YC, (0, 0), 1)
     dsts = [index_of(YC, s, 1) for s in SHIFTS]
     srcs = [index_of(YC, s, -1)[0] for s in SHIFTS]
-    tabs = [None] + list(b_r) + list(b_l) + [b_f]
+    tabs = [tab] + list(b_r) + list(b_l) + [b_f]
     origins = [lax.rem(z - d + 8, 8) for d in (0, 1, 2, 3, -1, -2, -3, 4)]
 
     def table_copy(i):
-        return pltpu.make_async_copy(tabs[i].at[0], tsm.at[i - 1], s_m.at[i - 1])
+        return pltpu.make_async_copy(tabs[i].at[0], tsm.at[i], s_m.at[i])
 
     def block_for(i, j):
-        code = tab_s[z, j] if i == 0 else tsm[i - 1, z, j]
-        return lax.rem(code, 8)
+        return lax.rem(tsm[i, z, j], 8)
 
     def push(i, buf, stage, out, sems):
         zr = origins[i]
         for s in range(7):
             stage[s, zr] = buf[block_for(i, dsts[s][0])]
-        out[my_yc, zr] = buf[block_for(i, my_yc)]
+        out[zr, my_yc] = buf[block_for(i, my_yc)]
         for s in range(7):
             cp = pltpu.make_async_remote_copy(
-                src_ref=stage.at[s, zr], dst_ref=out.at[my_yc, zr], send_sem=sems.at[0, i, s],
+                src_ref=stage.at[s, zr], dst_ref=out.at[zr, my_yc], send_sem=sems.at[0, i, s],
                 recv_sem=sems.at[1, i, s], device_id=dsts[s][1], device_id_type=MESH_ID)
             cp.start()
             sent.append(cp)
@@ -336,7 +337,7 @@
         for i in range(8):
             for s in range(7):
                 pltpu.make_async_remote_copy(
-                    src_ref=out.at[srcs[s], origins[i]], dst_ref=out.at[srcs[s], origins[i]],
+                    src_ref=out.at[origins[i], srcs[s]], dst_ref=out.at[origins[i], srcs[s]],
                     send_sem=sems.at[0, i, s], recv_sem=sems.at[1, i, s], device_id=dsts[s][1],
                     device_id_type=MESH_ID).wait_recv()
 
@@ -347,11 +348,15 @@
     def project(t):
         def run():
             rows = pl.ds(t * 256, 256)
-            klow[rows, :] = quarters(pas, rows, wk).astype(bf16)
+            low = quarters(pas, rows, wk).astype(bf16)
+            klow[rows, :] = low
+            wide = low.astype(f32)
+            norm = lax.rsqrt(jnp.mean(wide * wide, axis=-1, keepdims=True) + NORM_FLOOR)
+            khat[rows, :] = (wide * norm).astype(bf16)
             vlow[rows, :] = quarters(pas, rows, wv).astype(bf16)
         return run
 
-    prep, scan = mixer_pieces(mq, mk, mv, st, ld, fresh, corr, attend, qdec, kdec, cdec, state, mixed)
+    prep, scan = mixer_pieces(mq, mk, mv, st, ld, rate, fresh, corr, attend, qdec, kdec, cdec, state, mixed)
     work = [project(t) for t in range(4)] + prep + scan
     work.reverse()
 
@@ -360,26 +365,39 @@
             if work:
                 work.pop()()
 
+    table_copy(0).start()
+    fill(1)
+    table_copy(0).wait()
     push(0, cot, cst, cot_o, s_cy)
-    fill(2)
     b_take(0, sent)
     table_copy(1).start()
     table_copy(4).start()
-    t_take(0, sent)
-    c_take(0, sent)
-    fill(1)
+    c_take(0, sent, 0)
+    t_take(0, sent, 0)
+    c_take(0, sent, 1)
+    c_take(0, sent, 2)
     for i in (1, 4):
         table_copy(i).wait()
         push(i, cots[i], cst, cot_o, s_cy)
+    t_take(0, sent, 1)
     b_take(1, sent)
     table_copy(2).start()
     table_copy(5).start()
-    c_take(1, sent)
-    fill(1)
+    c_take(1, sent, 0)
+    c_take(1, sent, 1)
+    t_take(0, sent, 2)
+    c_take(1, sent, 2)
     for i in (2, 5):
         table_copy(i).wait()
         push(i, cots[i], cst, cot_o, s_cy)
-    t_take(1, sent)
+    t_take(1, sent, 0)
+    b_take(2, sent)
+    table_copy(3).start()
+    table_copy(6).start()
+    c_take(2, sent, 0)
+    t_take(1, sent, 1)
+    c_take(2, sent, 1)
+    t_take(1, sent, 2)
 
     parts = [(tok, x), (t_r, lax.rem(x + 3, 4)), (t_l, lax.rem(x + 1, 4)), (t_f, lax.rem(x + 2, 4))]
     for half in range(2):
@@ -393,17 +411,31 @@
         wide = low.astype(f32)
         norm = lax.rsqrt(jnp.mean(wide * wide, axis=-1, keepdims=True) + NORM_FLOOR)
         q_own[half * 3:half * 3 + 3] = (wide * norm).astype(bf16).reshape(3, 64, 256)
+        if half == 0:
+            c_take(2, sent, 2)
     for b in range(6):
         acc = None
         for buf, p in parts:
-            term = lax.dot_general(gw[p], buf[b], CONTRACT_LAST, preferred_element_type=f32)
+            term = lax.dot_general(gw[:, pl.ds(pl.multiple_of(p * 512, 512), 512)], buf[b], CONTRACT_LAST, preferred_element_type=f32)
             acc = term if acc is None else acc + term
-        gate[b, :, 0:64] = jax.nn.sigmoid(acc[0:8])
+        gate[b, :, 0:64] = jnp.broadcast_to(jax.nn.sigmoid(acc[0:1]), (8, 64))
         gate[b, :, 64:128] = jnp.zeros((8, 64), f32)
     g_start(0, sent)
     q_start(0, sent)
     wcp = []
-    for src, dst, sem in ((gw, gwc, s_w3), (wk, wkc, s_w0), (wv, wvc, s_w1), (wq, wqc, s_w2)):
+    for i in range(1, 4):
+        to, frm = lax.rem(x + i, 4), lax.rem(x + 4 - i, 4)
+        cols = pl.ds(pl.multiple_of(to * 512, 512), 512)
+        mine = pltpu.make_async_remote_copy(
+            src_ref=gw.at[:, cols], dst_ref=gwc.at[x], send_sem=s_w3.at[0, i - 1], recv_sem=s_w3.at[1, i - 1],
+            device_id={"tp": to}, device_id_type=MESH_ID)
+        mine.start()
+        sent.append(mine)
+        wcp.append((mine, pltpu.make_async_remote_copy(
+            src_ref=gw.at[:, cols], dst_ref=gwc.at[frm], send_sem=s_w3.at[0, i - 1], recv_sem=s_w3.at[1, i - 1],
+            device_id={"tp": to}, device_id_type=MESH_ID)))
+    gwc[x] = gw[:, pl.ds(pl.multiple_of(x * 512, 512), 512)]
+    for src, dst, sem in ((wk, wkc, s_w0), (wv, wvc, s_w1), (wq, wqc, s_w2)):
         mine, cps = a2a_copies(dict(axes=("tp",)), src, dst, sem)
         for cp, _ in cps:
             cp.start()
@@ -411,11 +443,6 @@
         dst[mine] = src[mine]
         wcp += cps
 
-    b_take(2, sent)
-    table_copy(3).start()
-    table_copy(6).start()
-    c_take(2, sent)
-    fill(1)
     for i in (3, 6):
         table_copy(i).wait()
         push(i, cots[i], cst, cot_o, s_cy)
@@ -423,48 +450,38 @@
     table_copy(7).start()
     c_take(3, sent)
     push(0, q_own, qst, q_o, s_qy)
-    fill(1)
     table_copy(7).wait()
     push(7, c_f, cst, cot_o, s_cy)
-    g_take(0, sent)
-    q_take(0, sent)
-    for i in (1, 4):
-        push(i, qs[i], qst, q_o, s_qy)
-    fill(5)
-    g_take(1, sent)
-    q_take(1, sent)
-    for i in (2, 5):
-        push(i, qs[i], qst, q_o, s_qy)
-    fill(5)
-    g_take(2, sent)
-    q_take(2, sent)
-    for i in (3, 6):
-        push(i, qs[i], qst, q_o, s_qy)
-    fill(3)
-    g_take(3, sent)
-    q_take(3, sent)
-    push(7, q_f, qst, q_o, s_qy)
+    for k, some in ((0, (1, 4)), (1, (2, 5)), (2, (3, 6)), (3, (7,))):
+        g_take(k, sent)
+        for ch in range(3):
+            q_take(k, sent, ch)
+            if ch < 2 and k < 3:
+                fill(1)
+        for i in some:
+            push(i, qs[i], qst, q_o, s_qy)
+        fill(1)
+    left_half = lax.broadcasted_iota(jnp.int32, (8, 128), 1) < 64
+
+    def side_for(i, j):
+        return jnp.where(left_half, gs[i][block_for(i, j)], tsm[i, z, j].astype(f32))
+
     for i in range(8):
         zr = origins[i]
-        table = tab if i == 0 else tabs[i]
-        row = table[0, pl.ds(z, 1), :]
-        codest[zr] = jnp.broadcast_to(row, (8, 128))
-        tabs_o[zr] = jnp.broadcast_to(row, (8, 128))
-        code_o[my_yc, zr] = jnp.broadcast_to(row, (8, 128))
+        tabs_o[zr] = jnp.broadcast_to(tabs[i][0, pl.ds(z, 1), :], (8, 128))
         for s in range(7):
-            gst[s, zr] = gs[i][block_for(i, dsts[s][0])]
-        gate_o[my_yc, zr] = gs[i][block_for(i, my_yc)]
+            gst[s, zr] = side_for(i, dsts[s][0])
+        gate_o[zr, my_yc] = side_for(i, my_yc)
     side = []
     for s in range(7):
-        for src, dst, sems in ((codest, code_o, s_by), (gst.at[s], gate_o, s_gy)):
-            cp = pltpu.make_async_remote_copy(
-                src_ref=src, dst_ref=dst.at[my_yc], send_sem=sems.at[0, s], recv_sem=sems.at[1, s],
-                device_id=dsts[s][1], device_id_type=MESH_ID)
-            cp.start()
-            sent.append(cp)
-            side.append(pltpu.make_async_remote_copy(
-                src_ref=src, dst_ref=dst.at[srcs[s]], send_sem=sems.at[0, s], recv_sem=sems.at[1, s],
-                device_id=dsts[s][1], device_id_type=MESH_ID))
+        cp = pltpu.make_async_remote_copy(
+            src_ref=gst.at[s], dst_ref=gate_o.at[:, my_yc], send_sem=s_gy.at[0, s], recv_sem=s_gy.at[1, s],
+            device_id=dsts[s][1], device_id_type=MESH_ID)
+        cp.start()
+        sent.append(cp)
+        side.append(pltpu.make_async_remote_copy(
+            src_ref=gst.at[s], dst_ref=gate_o.at[:, srcs[s]], send_sem=s_gy.at[0, s], recv_sem=s_gy.at[1, s],
+            device_id=dsts[s][1], device_id_type=MESH_ID))
     fill(99)
     for r in side:
         r.wait_recv()
@@ -486,10 +503,10 @@
     return pl.pallas_call(
         forward_kernel,
         out_shape=[
-            slots, slots, sds((8, 8, 8, 128), f32), sds((8, 8, 8, 128), i32), sds((8, 8, 128), i32),
+            slots, slots, sds((8, 8, 8, 128), f32), sds((8, 8, 128), i32),
             sds((384, 256), bf16), sds((6, 8, 128), f32), sds((1024, 256), bf16), sds((1024, 256), bf16),
-            sds((384, 256), f32), wide, wide, wide, sds((4, 16, 512), bf16)],
-        in_specs=[v, v, v, pl.BlockSpec(memory_space=pltpu.SMEM)] + [v] * 10,
+            sds((1024, 256), bf16), sds((384, 256), f32), wide, wide, wide, sds((4, 1, 512), bf16)],
+        in_specs=[v] * 13 + [pl.BlockSpec(memory_space=pltpu.SMEM)],
         out_specs=[v] * 14,
         scratch_shapes=[
             pltpu.VMEM((6, 64, 512), bf16), pltpu.VMEM((6, 64, 512), bf16), pltpu.VMEM((6, 64, 512), bf16),
@@ -498,14 +515,13 @@
             [pltpu.VMEM((6, 64, 256), bf16)] * 3, [pltpu.VMEM((6, 64, 256), bf16)] * 3, pltpu.VMEM((6, 64, 256), bf16),
             [pltpu.VMEM((6, 8, 128), f32)] * 3, [pltpu.VMEM((6, 8, 128), f32)] * 3, pltpu.VMEM((6, 8, 128), f32),
             [pltpu.VMEM((2, 8, 128), i32)] * 3, [pltpu.VMEM((2, 8, 128), i32)] * 3, pltpu.VMEM((2, 8, 128), i32),
-            pltpu.SMEM((7, 8, 128), i32),
+            pltpu.SMEM((8, 8, 128), i32),
             pltpu.VMEM((7, 8, 64, 256), bf16), pltpu.VMEM((7, 8, 64, 256), bf16), pltpu.VMEM((7, 8, 8, 128), f32),
-            pltpu.VMEM((8, 8, 128), i32),
             pltpu.VMEM((12, 64, 128), f32), pltpu.VMEM((12, 64, 128), bf16), pltpu.VMEM((12, 64, 64), bf16),
             pltpu.VMEM((12, 64, 128), bf16), pltpu.VMEM((12, 64, 128), bf16), pltpu.VMEM((12, 8, 128), f32),
             pltpu.VMEM((2, 128, 128), f32),
-            dma((2, 2, 6)), dma((2, 2, 12)), dma((2, 2, 12)), dma((2, 2, 4)), dma((2, 2, 4)), dma((7,)),
-            dma((2, 8, 7)), dma((2, 8, 7)), dma((2, 7)), dma((2, 7)),
+            dma((2, 2, 6)), dma((2, 2, 12)), dma((2, 2, 12)), dma((2, 2, 4)), dma((2, 2, 4)), dma((8,)),
+            dma((2, 8, 7)), dma((2, 8, 7)), dma((2, 7)),
             dma((2, 3)), dma((2, 3)), dma((2, 3)), dma((2, 3))],
         compiler_params=pltpu.CompilerParams(
             collective_id=cid, has_side_effects=True, vmem_limit_bytes=60 * 1024 * 1024),
@@ -533,12 +549,25 @@
         pl.semaphore_signal(barrier, inc=1, device_id=p, device_id_type=MESH_ID)
     pl.semaphore_wait(barrier, len(peers))
     sent = []
-    mine, cps = a2a_copies(job, x_ref, got, s1)
-    for cp, _ in cps:
+    my_yc, _ = index_of(YC, (0, 0), 1)
+    dsts = [index_of(YC, s, 1) for s in SHIFTS]
+    srcs = [index_of(YC, s, -1)[0] for s in SHIFTS]
+
+    def swap(s, sems, out):
+        if out:
+            src, dst, land = back.at[dsts[s][0]], o_ref.at[:, my_yc], o_ref.at[:, srcs[s]]
+        else:
+            src, dst, land = x_ref.at[:, dsts[s][0]], got.at[my_yc], got.at[srcs[s]]
+        return [pltpu.make_async_remote_copy(
+            src_ref=src, dst_ref=d, send_sem=sems.at[0, s], recv_sem=sems.at[1, s],
+            device_id=dsts[s][1], device_id_type=MESH_ID) for d in (dst, land)]
+
+    first = [swap(s, s1, False) for s in range(7)]
+    for cp, _ in first:
         cp.start()
         sent.append(cp)
-    got[mine] = x_ref[mine]
-    for _, r in cps:
+    got[my_yc] = x_ref[:, my_yc]
+    for _, r in first:
         r.wait_recv()
     for b in range(6):
         acc = got[0] * m_ref[0, b]
@@ -572,12 +601,12 @@
         for b in range(1, 6):
             acc = acc + whole[b] * m_ref[j, b]
         back[j] = acc
-    mine, cps3 = a2a_copies(job, back, o_ref, s3)
-    for cp, _ in cps3:
+    last = [swap(s, s3, True) for s in range(7)]
+    for cp, _ in last:
         cp.start()
         sent.append(cp)
-    o_ref[mine] = back[mine]
-    for _, r in cps3:
+    o_ref[:, my_yc] = back[my_yc]
+    for _, r in last:
         r.wait_recv()
     for cp in sent:
         cp.wait_send()
@@ -599,7 +628,9 @@
     )(x, mask)
 
 
-def tail_kernel(kg, vg, w, kg_o, vg_o, w_o, wc, wcs, wy, wys, wz, s_k, s_v, s_c, s_y, s_z):
+def tail_kernel(
+    kg, vg, pas, wkc, wvc, rows_o, w_o, kg4, vg4, acc, w, wc, wcs, wy, wys, wz, s_k, s_v, s_c, s_y, s_z):
+    f32, bf16 = jnp.float32, jnp.bfloat16
     barrier = pltpu.get_barrier_semaphore()
     peers = ring_peers(ring("tp")) + a2a_peers(a2a("st_2")) + a2a_peers(a2a("st_1")) + a2a_peers(a2a("st_0"))
     for p in peers:
@@ -607,7 +638,7 @@
     pl.semaphore_wait(barrier, len(peers))
     sent = []
     rings = []
-    for src, dst, sems in ((kg, kg_o, s_k), (vg, vg_o, s_v)):
+    for src, dst, sems in ((kg, kg4, s_k), (vg, vg4, s_v)):
         c, a, steps, chunks = ring_starts(ring("tp", 2), src, dst, sems)
         rings.append((c, a))
         for ch in range(2):
@@ -616,29 +647,48 @@
                 cp.start()
                 sent.append(cp)
     core = lax.axis_index("st_2")
+    x = lax.axis_index("tp")
+
+    def add_head(k_of, v_of, h, first, final):
+        for t in range(4):
+            rows = pl.ds(t * 256, 256)
+            part = lax.dot_general(k_of(rows), wkc[h], CONTRACT_LAST, preferred_element_type=f32)
+            part = part + lax.dot_general(v_of(rows), wvc[h], CONTRACT_LAST, preferred_element_type=f32)
+            part = part.astype(bf16).astype(f32)
+            part = part if first else acc[rows, :] + part
+            if final:
+                rows_o[rows, :] = part.astype(bf16)
+            else:
+                acc[rows, :] = part
+
+    for t in range(8):
+        cols = pl.ds(t * 256, 256)
+        part = lax.dot_general(pas[:, cols], kg[...], CONTRACT_FIRST, preferred_element_type=f32)
+        w[t] = part.reshape(4, 2, 32, 256)
     pair = pltpu.make_async_remote_copy(
-        src_ref=w.at[1 - core], dst_ref=wc, send_sem=s_c.at[0], recv_sem=s_c.at[1],
+        src_ref=w.at[:, :, 1 - core], dst_ref=wc, send_sem=s_c.at[0], recv_sem=s_c.at[1],
         device_id={"st_2": 1 - core}, device_id_type=MESH_ID)
     pair.start()
     sent.append(pair)
-    x = lax.axis_index("tp")
-    kg_o[x] = kg[...]
-    vg_o[x] = vg[...]
+    add_head(lambda r: kg[r, :], lambda r: vg[r, :], x, True, False)
     pair.wait_recv()
-    for y in range(4):
-        wcs[y] = w[core, y] + wc[y]
+    for k in range(8):
+        for y in range(4):
+            wcs[y, k] = w[k, y, core] + wc[k, y]
     ym, ycp = a2a_copies(a2a("st_1"), wcs, wy, s_y)
     for cp, _ in ycp:
         cp.start()
         sent.append(cp)
     wy[ym] = wcs[ym]
-    for c, a in rings:
-        for ch in range(2):
+    for ch in range(2):
+        for c, a in rings:
             for d in range(2):
                 a(0, d, ch).wait_recv()
                 cp = c(1, d, ch)
                 cp.start()
                 sent.append(cp)
+    for h in (lax.rem(x + 1, 4), lax.rem(x + 3, 4)):
+        add_head(lambda r: kg4[h, r], lambda r: vg4[h, r], h, False, False)
     for _, r in ycp:
         r.wait_recv()
     for k in range(8):
@@ -648,38 +698,40 @@
         cp.start()
         sent.append(cp)
     wz[zm] = wys[zm]
-    for c, a in rings:
-        for ch in range(2):
+    for ch in range(2):
+        for c, a in rings:
             for d in range(2):
                 a(1, d, ch).wait_recv()
+    far = lax.rem(x + 2, 4)
+    add_head(lambda r: kg4[far, r], lambda r: vg4[far, r], far, False, True)
     for _, r in zcp:
         r.wait_recv()
-    acc = wz[0]
+    total = wz[0]
     for k in range(1, 8):
-        acc = acc + wz[k]
-    w_o[...] = acc
+        total = total + wz[k]
+    w_o[...] = total
     for cp in sent:
         cp.wait_send()
 
 
-def tail(kg, vg, w, cid):
+def tail(kg, vg, pas, wkc, wvc, cid):
     v = pl.BlockSpec(memory_space=pltpu.VMEM)
     f32, bf16 = jnp.float32, jnp.bfloat16
     dma = pltpu.SemaphoreType.DMA
     return pl.pallas_call(
         tail_kernel,
-        out_shape=[
-            jax.ShapeDtypeStruct((4, 1024, 256), bf16), jax.ShapeDtypeStruct((4, 1024, 256), bf16),
-            jax.ShapeDtypeStruct((32, 256), f32)],
-        in_specs=[v] * 3,
-        out_specs=[v] * 3,
+        out_shape=[jax.ShapeDtypeStruct((1024, 512), bf16), jax.ShapeDtypeStruct((32, 256), f32)],
+        in_specs=[v] * 5,
+        out_specs=[v] * 2,
         scratch_shapes=[
-            pltpu.VMEM((4, 8, 32, 256), f32), pltpu.VMEM((4, 8, 32, 256), f32), pltpu.VMEM((4, 8, 32, 256), f32),
+            pltpu.VMEM((4, 1024, 256), bf16), pltpu.VMEM((4, 1024, 256), bf16), pltpu.VMEM((1024, 512), f32),
+            pltpu.VMEM((8, 4, 2, 32, 256), f32), pltpu.VMEM((8, 4, 32, 256), f32),
+            pltpu.VMEM((4, 8, 32, 256), f32), pltpu.VMEM((4, 8, 32, 256), f32),
             pltpu.VMEM((8, 32, 256), f32), pltpu.VMEM((8, 32, 256), f32),
             dma((2, 2, 4)), dma((2, 2, 4)), dma((2,)), dma((2, 3)), dma((2, 7))],
         compiler_params=pltpu.CompilerParams(
-            collective_id=cid, has_side_effects=True, vmem_limit_bytes=40 * 1024 * 1024),
-    )(kg, vg, w)
+            collective_id=cid, has_side_effects=True, vmem_limit_bytes=56 * 1024 * 1024),
+    )(kg, vg, pas, wkc, wvc)
 
 
 def body(
@@ -689,7 +741,6 @@
     f32, bf16 = jnp.float32, jnp.bfloat16
     scale = SCORE_GAIN * 256 ** (-0.5)
     z = lax.axis_index("st_0")
-    my_yc = lax.axis_index(YC)
     ids = passage_ids.reshape(24)
     owner, local = ids // 16, ids % 16
     match = owner[None, :] == jnp.arange(64, dtype=jnp.int32)[:, None]
@@ -697,28 +748,25 @@
     code = jnp.sum(jnp.where(match, code_of[None, :], 0), axis=-1, dtype=jnp.int32)
     code = jnp.where(jnp.any(match, axis=-1), code, 128).reshape(8, 8)
     table = jnp.pad(code[None], ((0, 1), (0, 0), (0, 120)))
-    gw4 = jnp.broadcast_to(gate_weight.reshape(4, 1, 512), (4, 16, 512))
-    strength = jax.nn.sigmoid(beta_pre).reshape(12, 64)
-    log_decay = (-decay_rate[:, None] * jax.nn.softplus(decay_pre)).reshape(12, 64)
     flat_rows = passages.reshape(1024, 2048)
-    (cot_here, q_here, gate_o, code_o, tabs, query_low, gate6, key_low, value_all, mixer_out,
+    quarter = (4, 512, 256)
+    (cot_here, q_here, gate_o, tabs, query_low, gate6, key_low, key_hat, value_all, mixer_out,
      wk_cols, wv_cols, wq_cols, gw_cols) = forward(
-        [tokens.reshape(6, 64, 512), cotangent.reshape(6, 64, 256), table, code,
-         query_weight.reshape(4, 512, 256), gw4, flat_rows, key_weight.reshape(4, 512, 256), value_weight.reshape(4, 512, 256),
-         mix_query, mix_key, mix_value, strength, log_decay], 1)
+        [tokens.reshape(6, 64, 512), cotangent.reshape(6, 64, 256), table,
+         query_weight.reshape(quarter), gate_weight, flat_rows, key_weight.reshape(quarter),
+         value_weight.reshape(quarter), mix_query, mix_key, mix_value, beta_pre, decay_pre, decay_rate], 1)
     cot_here, q_here = cot_here.reshape(64, 64, 256), q_here.reshape(64, 64, 256)
     codes = tabs[:, 0, :8]
-    gate_here = gate_o[:, :, 0, :64].reshape(64, 64)
-    code_here = lax.dynamic_slice(code_o, (0, 0, 0, my_yc), (8, 8, 1, 1)).reshape(64)
+    side = gate_o[:, :, 0, :].reshape(64, 128)
+    gate_here = side[:, :64]
+    code_here = side[:, 64].astype(jnp.int32)
     used = code_here < 128
     loc = jnp.where(used, code_here // 8, 0)
     gate_open = gate6[:, 0, :64].reshape(384)
     query_float = query_low.astype(f32)
     query_scale = lax.rsqrt(jnp.mean(query_float * query_float, axis=-1, keepdims=True) + NORM_FLOOR)
-
     key_float = key_low.astype(f32)
     key_scale = lax.rsqrt(jnp.mean(key_float * key_float, axis=-1, keepdims=True) + NORM_FLOOR)
-    key_hat = (key_float * key_scale).astype(bf16)
     k_sel = key_hat.reshape(16, 64, 256)[loc]
     v_sel = value_all.reshape(16, 64, 256)[loc]
 
@@ -744,7 +792,6 @@
     probs_low = probs.astype(bf16)
     score_grad = (probs * (grad_probs - inner[:, :, None])).astype(bf16)
     q_part = (scale * jnp.einsum("sij,sjd->sid", score_grad, k_sel, preferred_element_type=f32)).astype(bf16)
-    q_part = jnp.moveaxis(q_part.reshape(8, 8, 64, 256), 0, 1).reshape(64, 64, 256)
     q_back = lax.all_to_all(q_part, ST, split_axis=0, concat_axis=0, tiled=True)
 
     key_term = (scale * jnp.einsum("sij,sid->sjd", score_grad, q_here, preferred_element_type=f32)).astype(bf16)
@@ -757,14 +804,8 @@
         - key_scale**3 * key_float * jnp.mean(key_float * key_grad_hat, axis=-1, keepdims=True)
     ).astype(bf16)
     value_grad_low = value_grad.astype(bf16)
-    weight_term = lax.dot_general(flat_rows, key_grad, CONTRACT_FIRST, preferred_element_type=f32)
-    weight_term = jnp.transpose(weight_term.reshape(8, 4, 2, 32, 256), (2, 1, 0, 3, 4))
-    kg4, vg4, key_weight_grad = tail(key_grad, value_grad_low, weight_term, 3)
-    row_part = (
-        jnp.einsum("hrd,hed->hre", kg4, wk_cols, preferred_element_type=f32)
-        + jnp.einsum("hrd,hed->hre", vg4, wv_cols, preferred_element_type=f32)
-    ).astype(bf16)
-    passage_grad = jnp.sum(row_part.astype(f32), axis=0).astype(bf16).reshape(16, 64, 512)
+    passage_grad, key_weight_grad = tail(key_grad, value_grad_low, flat_rows, wk_cols, wv_cols, 3)
+    passage_grad = passage_grad.reshape(16, 64, 512)
 
     qhat_grad = jnp.sum(q_back[owner].astype(f32).reshape(6, 4, 64, 256), axis=1).reshape(384, 256)
     grad_out = cotangent.astype(f32)
@@ -773,11 +814,11 @@
         query_scale * qhat_grad
         - query_scale**3 * query_float * jnp.mean(query_float * qhat_grad, axis=-1, keepdims=True)
     ).astype(bf16)
-    qg4, gg4 = comm([ring("tp"), ring("tp")], [query_grad, rows_of(gate_grad)], 4)
+    qg4, gg4 = comm([ring("tp", 2), ring("tp")], [query_grad, rows_of(gate_grad)], 4)
     gg4 = gg4[:, :3].reshape(4, 384)
     token_part = (
         jnp.einsum("htd,hed->hte", qg4, wq_cols, preferred_element_type=f32)
-        + gg4[:, :, None] * gw_cols[:, 0].astype(f32)[:, None, :]
+        + gg4[:, :, None] * gw_cols.astype(f32)
     ).astype(bf16)
     token_grad = jnp.sum(token_part.astype(f32), axis=0).astype(bf16)
     return token_grad, passage_grad, key_weight_grad

time: 233 us -> 209 us (0.90)
  local copies, waits for them, and re-layouts: 30.3 us -> 21.9 us
  matrix products: 20.7 us -> 13.5 us
  other arithmetic: 12.8 us -> 7.66 us
    dot_general x3 -> x0, matrix products: 8.49 us -> none  [the longest x1 4.81 us: body(): lax.dot_general(flat_rows, key_grad, CONTRACT_FIRST, preferred_element_ty...]
    pallas_call x1, Pallas kernels: 81 us -> 72.7 us  [forward(): pl.pallas_call(forward_kernel, out_shape=[slots, slots, sds((8, 8, 8, 128...]
    reshape x6 -> x0, local copies, waits for them, and re-layouts: 4.83 us -> none  [the longest x1 1.83 us: body(): weight_term.reshape(8, 4, 2, 32, 256)]
    pallas_call x1, Pallas kernels: 42.2 us -> 46.9 us  [tail(): pl.pallas_call(tail_kernel, out_shape=[jax.ShapeDtypeStruct((1024, 512),...]
    dot_general x1 -> x0, local copies, waits for them, and re-layouts: 2.89 us -> none  [body(): lax.dot_general(flat_rows, key_grad, CONTRACT_FIRST, preferred_element_ty...]
    unnamed x40 -> x44, local copies, waits for them, and re-layouts: 6.53 us -> 7.67 us
  transfers between devices with their start and end apart: 1 -> 1, of which waited for: 0 -> 0; matrix products, arithmetic and copies ran while one was open for 11% -> 6% of each run, Pallas kernels for 18% -> 22%
where the time goes in v3:
time: 209 us
  Pallas kernels  158 us (76%)
  local copies, waits for them, and re-layouts  21.9 us (10%)
  matrix products  13.5 us (6%)
  other arithmetic  7.66 us (4%)
  starting transfers between devices  6.92 us (3%)
    pallas_call x1, Pallas kernels, forward(): pl.pallas_call(forward_kernel, out_shape=[slots, slots, sds((8, 8, 8, 128...  72.7 us
    pallas_call x1, Pallas kernels, tail(): pl.pallas_call(tail_kernel, out_shape=[jax.ShapeDtypeStruct((1024, 512),...  46.9 us
    pallas_call x1, Pallas kernels, stats_exchange(): pl.pallas_call(stats_kernel, out_shape=[jax.ShapeDtypeStruct(x.shape, f),...  23.2 us
    pallas_call x1, Pallas kernels, comm(): pl.pallas_call(functools.partial(comm_kernel, jobs), out_shape=outs, in_s...  14.9 us
    unnamed x44, local copies, waits for them, and re-layouts  7.67 us
    all_to_all x1, starting transfers between devices, body(): q_back = lax.all_to_all(q_part, ST, split_axis=0, concat_axis=0, tiled=True)  6.92 us
  transfers between devices with their start and end apart: 1, of which 0 were waited for; matrix products, arithmetic and copies ran while one was open for 6% of the time, Pallas kernels for 22%

profile of v3, /device:TPU:2, one launch (start us, length us, event | category | flops | bytes accessed | tf_op | source)
XLA Modules:
  0.0 208.6 jit_solution(10996676901224328701)
XLA Ops:
  0.6 0.8 copy.27
  2.4 72.7 %shard_map.157 = (bf16[8,8,64,256]{3,2,1,0:T(8,128)(2,1)}, bf16[8,8,64,256]{3,2,1,0:T(8,128)(2,1)}, f32[8,8,8,128]{3,2,1,0:T(8,128)}, s32[8,8,128]{2,1,0:T(8,128...) custom-call(bf16[6,64,512]{2,1,0:T(8,128)(2,1)} %bitcast.98, ...), custom_call_target="tpu_custom_call" | custom-call | tf_op jit(solution)/shard_map/pallas_call | solution.py:503
  75.1 1.0 slice.30
  76.3 1.8 gather_fusion.1
  78.1 2.0 gather_fusion
  80.1 2.4 %fusion = f32[64,64,64]{1,2,0:T(8,128)S(1)} fusion(bf16[64,64,256]{2,1,0:T(8,128)(2,1)S(1)} %gather_fusion.1, bf16[64,64,256]{2,1,0:T(8,128)(2,1)} %bitcast.81, f32[64,64]{1,0:T(8,128)S(1)} %bitcast.100), kind=kOutput, calls=%fused_computation.14 | convolution fusion | flops 137363456 | bytes 5259264 | tf_op jit(solution)/shard_map/sid,sjd->sij/dot_general | solution.py:776
  82.9 0.9 fusion.35
  83.9 1.0 copy-done.5
  84.8 0.7 multiply_reduce_fusion
  85.6 0.8 slice.33
  86.4 0.7 maximum_bitcast_fusion.x_ref
  87.1 0.9 broadcast_in_dim.90.m_ref
  88.0 23.2 %shard_map.158 = (f32[8,8,256]{2,1,0:T(8,128)}, f32[6,8,256]{2,1,0:T(8,128)}) custom-call(f32[8,8,256]{2,1,0:T(8,128)} %maximum_bitcast_fusion.x_ref, f32[8,6,8,256]{3,2,1,0:T(8,128)} %broadcast_in_dim.90.m_ref), custom_call_target="tpu_custom_call" | custom-call | tf_op jit(solution)/shard_map/pallas_call | solution.py:618
  111.2 0.9 slice_select_fusion.1
  112.2 2.8 %multiply_convert_fusion.3 = bf16[64,64,64]{1,2,0:T(8,128)(2,1)S(1)} fusion(f32[64,64,64]{1,2,0:T(8,128)} %copy-done.2, f32[64,64]{1,0:T(8,128)S(1)} %get-tuple-element.50, f32[64,64]{1,0:T(8,128)S(1)} %get-tuple-element.49, f32[64,64,64]{1,2,0:T(8,128)} %copy-done, pred[64]{0:T(512)(128)(4,1)S(1)} %bitcast_compare_fusion), kind=kLoop, calls=%fused_computation.8 | loop fusion | flops 1310720 | bytes 2654272 | tf_op jit(solution)/shard_map/convert_element_type | solution.py:793
  115.0 2.1 %multiply_convert_fusion.1 = bf16[64,64,256]{2,1,0:T(8,128)(2,1)} fusion(bf16[64,64,64]{1,2,0:T(8,128)(2,1)S(1)} %multiply_convert_fusion.3, bf16[64,64,256]{2,1,0:T(8,128)(2,1)S(1)} %copy-done.4), kind=kOutput, calls=%fused_computation.5 | convolution fusion | flops 136314880 | bytes 4718592 | tf_op jit(solution)/shard_map/sij,sjd->sid/dot_general | solution.py:794
  117.1 6.9 %all-to-all-start = ((bf16[64,64,256]{2,1,0:T(8,128)(2,1)}), bf16[64,64,256]{2,1,0:T(8,128)(2,1)}, u32[]{:S(2)}, u32[]{:S(2)}) async-start(bf16[64,64,256]{2,1,0:T(8,128)(2,1)} %multiply_convert_fusion.1), calls=%async_computation | async-start | bytes 4194304 | tf_op jit(solution)/shard_map/all_to_all | solution.py:795
  124.1 2.4 %convolution_convert_fusion.1 = bf16[64,64,256]{2,1,0:T(8,128)(2,1)S(1)} fusion(bf16[64,64,256]{2,1,0:T(8,128)(2,1)} %bitcast.82, f32[64,64]{1,0:T(8,128)S(1)} %bitcast.101, f32[64,64,64]{1,2,0:T(8,128)S(1)} %copy-done.1, f32[64,64]{1,0:T(8,128)S(1)} %get-tuple-element.49, pred[64]{0:T(512)(128)(4,1)S(1)} %bitcast_compare_fusion), kind=kOutput, calls=%fused_computation.13 | convolution fusion | flops 139198464 | bytes 5275712 | tf_op jit(solution)/shard_map/sij,sid->sjd/dot_general | solution.py:798
  126.6 1.3 copy.38
  127.9 1.2 convolution_convert_fusion
  129.1 2.1 convert_element_type.102.vg
  131.8 1.3 copy.37
  134.5 1.3 fusion.5.kg
  135.8 46.9 %shard_map.160 = (bf16[1024,512]{1,0:T(8,128)(2,1)}, f32[32,256]{1,0:T(8,128)}) custom-call(bf16[1024,256]{1,0:T(8,128)(2,1)} %fusion.5.kg, bf16[1024,256]{1,0:T(8,128)(2,1)} %convert_element_type.102.vg, bf16[1024,2048]{1,0:T(8,128)(2,1)} %bitcast.80, bf16[4,512,256]{2,1,0:T(8,128)(2,1)} %get-tuple-element.39.wkc, bf16[4,512,256]{2,1,0:T(8,128)(2,1)} %get-tuple-element.40.wvc), custom_call_target="tpu_custom_call" | custom-call | tf_op jit(solution)/shard_map/pallas_call | solution.py:721
  182.7 0.9 constant_dynamic-slice_fusion
  183.7 0.8 slice_reduce_fusion
  184.6 2.2 %gather_fusion.2 = bf16[24,64,256]{2,1,0:T(8,128)(2,1)S(1)} fusion(bf16[64,64,256]{2,1,0:T(8,128)(2,1)} %all-to-all-done, s32[1024]{0:T(1024)S(1)} %pad_clamp_fusion), kind=kCustom, calls=%fused_computation.2 | custom fusion | bytes 1572960 | tf_op jit(solution)/shard_map/gather | solution.py:810
  187.8 0.9 fusion.11.refs_0_
  188.7 14.9 %shard_map.159 = (bf16[4,384,256]{2,1,0:T(8,128)(2,1)}, f32[4,16,128]{2,1,0:T(8,128)}) custom-call(bf16[384,256]{1,0:T(8,128)(2,1)} %fusion.11.refs_0_, f32[16,128]{1,0:T(8,128)} %pad.9.refs_1_), custom_call_target="tpu_custom_call" | custom-call | tf_op jit(solution)/shard_map/pallas_call | solution.py:157
  203.6 0.7 slice_bitcast_fusion
  204.4 2.7 %fusion.1 = bf16[384,512]{1,0:T(8,128)(2,1)} fusion(f32[4,512]{1,0:T(4,128)S(1)} %bitcast.105, f32[4,384]{1,0:T(4,128)S(1)} %bitcast.106, bf16[4,384,256]{2,1,0:T(8,128)(2,1)} %get-tuple-element.34, bf16[4,512,256]{2,1,0:T(8,128)(2,1)S(1)} %copy-done.16), kind=kOutput, calls=%fused_computation.19 | convolution fusion | flops 405602304 | bytes 2242560 | tf_op jit(solution)/shard_map/htd,hed->hte/dot_general | solution.py:820
  207.1 1.0 copy.47
  (73 shorter events, 5.7 us)
Async XLA Ops:
  76.3 1.8 copy-start.6
  80.1 2.4 %copy-start.3 = (bf16[64,64,256]{2,1,0:T(8,128)(2,1)S(1)}, bf16[64,64,256]{2,1,0:T(8,128)(2,1)}, u32[]{:S(2)}) copy-start(bf16[64,64,256]{2,1,0:T(8,128)(2,1)} %gather_fusion) | copy-start | bytes 6291460
  80.1 2.9 %copy-start.7 = (bf16[8,8,64,256]{3,2,1,0:T(8,128)(2,1)S(1)}, bf16[8,8,64,256]{3,2,1,0:T(8,128)(2,1)}, u32[]{:S(2)}) copy-start(bf16[8,8,64,256]{3,2,1,0:T(8,128)(2,1)} %get-tuple-element.25) | copy-start | bytes 6291460
  82.5 1.3 copy-start.2
  82.9 1.9 copy-start.5
  83.9 1.7 copy-start
  112.2 2.9 %copy-start.4 = (bf16[64,64,256]{2,1,0:T(8,128)(2,1)S(1)}, bf16[64,64,256]{2,1,0:T(8,128)(2,1)}, u32[]{:S(2)}) copy-start(bf16[64,64,256]{2,1,0:T(8,128)(2,1)} %gather_fusion) | copy-start | bytes 6291460
  117.1 7.0 %copy-start.1 = (f32[64,64,64]{1,2,0:T(8,128)S(1)}, f32[64,64,64]{1,2,0:T(8,128)}, u32[]{:S(2)}) copy-start(f32[64,64,64]{1,2,0:T(8,128)} %copy-done) | copy-start | bytes 3145732
  117.1 67.5 %all-to-all-start = ((bf16[64,64,256]{2,1,0:T(8,128)(2,1)}), bf16[64,64,256]{2,1,0:T(8,128)(2,1)}, u32[]{:S(2)}, u32[]{:S(2)}) async-start(bf16[64,64,256]{2,1,0:T(8,128)(2,1)} %multiply_convert_fusion.1), calls=%async_computation | async-start | bytes 4194304 | tf_op jit(solution)/shard_map/all_to_all | solution.py:795
  127.9 3.3 %copy-start.8 = (bf16[8,8,64,256]{3,2,1,0:T(8,128)(2,1)S(1)}, bf16[8,8,64,256]{3,2,1,0:T(8,128)(2,1)}, u32[]{:S(2)}) copy-start(bf16[8,8,64,256]{3,2,1,0:T(8,128)(2,1)} %get-tuple-element.25) | copy-start | bytes 6291460
  133.1 1.0 copy-start.9
  135.8 48.7 %copy-start.15 = (bf16[4,1,512]{2,1,0:T(2,128)(2,1)S(1)}, bf16[4,1,512]{2,1,0:T(2,128)(2,1)}, u32[]{:S(2)}) copy-start(bf16[4,1,512]{2,1,0:T(2,128)(2,1)} %get-tuple-element.37) | copy-start | bytes 12292
  182.7 4.2 %copy-start.11 = (bf16[384,256]{1,0:T(8,128)(2,1)S(1)}, bf16[384,256]{1,0:T(8,128)(2,1)}, u32[]{:S(2)}) copy-start(bf16[384,256]{1,0:T(8,128)(2,1)} %get-tuple-element.23) | copy-start | bytes 589828
  182.7 4.2 %copy-start.12 = (bf16[384,256]{1,0:T(8,128)(2,1)S(1)}, bf16[384,256]{1,0:T(8,128)(2,1)}, u32[]{:S(2)}) copy-start(bf16[384,256]{1,0:T(8,128)(2,1)} %param.15) | copy-start | bytes 589828
  182.7 4.2 %copy-start.13 = (f32[384,256]{1,0:T(8,128)S(1)}, f32[384,256]{1,0:T(8,128)}, u32[]{:S(2)}) copy-start(f32[384,256]{1,0:T(8,128)} %get-tuple-element.32) | copy-start | bytes 1179652
  186.8 17.6 %copy-start.16 = (bf16[4,512,256]{2,1,0:T(8,128)(2,1)S(1)}, bf16[4,512,256]{2,1,0:T(8,128)(2,1)}, u32[]{:S(2)}) copy-start(bf16[4,512,256]{2,1,0:T(8,128)(2,1)} %get-tuple-element.35) | copy-start | bytes 3145732
  204.4 2.7 %copy-start.10 = (bf16[1024,512]{1,0:T(8,128)(2,1)S(1)}, bf16[1024,512]{1,0:T(8,128)(2,1)}, u32[]{:S(2)}) copy-start(bf16[1024,512]{1,0:T(8,128)(2,1)} %get-tuple-element.41) | copy-start | bytes 3145732
  207.1 1.0 copy-start.14

commit v4 on v3

--- a/solution.py
+++ b/solution.py
@@ -189,8 +189,8 @@
             send_sem=sems.at[0, d, k * chunks + ch], recv_sem=sems.at[1, d, k * chunks + ch],
             device_id={axis: lax.rem(me + sgn + n, n)}, device_id_type=MESH_ID)
 
-    def start(k, sent):
-        for ch in range(chunks):
+    def start(k, sent, which=None):
+        for ch in range(chunks) if which is None else (which,):
             for d in range(2):
                 cp = copy(k, d, ch)
                 cp.start()
@@ -283,15 +283,17 @@
 
 
 def forward_kernel(
-    tok, cot, tab, wq, gw, pas, wk, wv, mq, mk, mv, st, ld, rate,
+    tok, cot, tab, wq, gw, pas_hbm, wk, wv, mq, mk, mv, st, ld, rate,
     cot_o, q_o, gate_o, tabs_o, qlow, gate, klow, khat, vlow, mixed, wkc, wvc, wqc, gwc,
     t_r, t_l, t_f, c_r, c_l, c_f, q_own, q_r, q_l, q_f, g_r, g_l, g_f, b_r, b_l, b_f, tsm,
-    cst, qst, gst, fresh, corr, attend, qdec, kdec, cdec, state,
-    s_t, s_c, s_q, s_g, s_b, s_m, s_cy, s_qy, s_gy, s_w0, s_w1, s_w2, s_w3,
+    cst, qst, gst, pas, fresh, corr, attend, qdec, kdec, cdec, state,
+    s_t, s_c, s_q, s_g, s_b, s_m, s_cy, s_qy, s_gy, s_p, s_w0, s_w1, s_w2, s_w3,
 ):
     f32, bf16 = jnp.float32, jnp.bfloat16
     z = lax.axis_index("st_0")
     x = lax.axis_index("tp")
+    store = pltpu.make_async_copy(pas_hbm, pas, s_p)
+    store.start()
     jobs = [ring_peers(dict(axis="tp")), ring_peers(dict(axis="st_0")), a2a_peers(dict(axes=YC)),
             a2a_peers(dict(axes=("tp",)))]
     barrier = pltpu.get_barrier_semaphore()
@@ -306,7 +308,8 @@
     q_start, q_take = near_ring("st_0", q_own, q_r, q_l, q_f, s_q, 3)
     g_start, g_take = near_ring("st_0", gate, g_r, g_l, g_f, s_g, 1)
     b_start(0, sent)
-    t_start(0, sent)
+    t_start(0, sent, 0)
+    t_start(0, sent, 1)
     c_start(0, sent)
 
     my_yc, _ = index_of(YC, (0, 0), 1)
@@ -359,69 +362,76 @@
     prep, scan = mixer_pieces(mq, mk, mv, st, ld, rate, fresh, corr, attend, qdec, kdec, cdec, state, mixed)
     work = [project(t) for t in range(4)] + prep + scan
     work.reverse()
+    count_all = len(work)
 
     def fill(count):
+        if len(work) == count_all and count:
+            store.wait()
         for _ in range(count):
             if work:
                 work.pop()()
 
+    parts = [(tok, x), (t_r, lax.rem(x + 3, 4)), (t_l, lax.rem(x + 1, 4)), (t_f, lax.rem(x + 2, 4))]
+
+    def queries(ch):
+        acc = None
+        for buf, p in parts:
+            term = jnp.dot(buf[ch * 2:ch * 2 + 2].reshape(128, 512), wq[p], preferred_element_type=f32)
+            acc = term if acc is None else acc + term
+        low = acc.astype(bf16)
+        qlow[ch * 128:ch * 128 + 128, :] = low
+        wide = low.astype(f32)
+        norm = lax.rsqrt(jnp.mean(wide * wide, axis=-1, keepdims=True) + NORM_FLOOR)
+        q_own[ch * 2:ch * 2 + 2] = (wide * norm).astype(bf16).reshape(2, 64, 256)
+        for b in range(ch * 2, ch * 2 + 2):
+            acc = None
+            for buf, p in parts:
+                cols = pl.ds(pl.multiple_of(p * 512, 512), 512)
+                term = lax.dot_general(gw[:, cols], buf[b], CONTRACT_LAST, preferred_element_type=f32)
+                acc = term if acc is None else acc + term
+            gate[b, :, 0:64] = jnp.broadcast_to(jax.nn.sigmoid(acc[0:1]), (8, 64))
+            gate[b, :, 64:128] = jnp.zeros((8, 64), f32)
+        q_start(0, sent, ch)
+
+    def cot_push(*some):
+        for i in some:
+            table_copy(i).wait()
+            push(i, cots[i], cst, cot_o, s_cy)
+
     table_copy(0).start()
     fill(1)
-    table_copy(0).wait()
-    push(0, cot, cst, cot_o, s_cy)
+    cot_push(0)
     b_take(0, sent)
     table_copy(1).start()
     table_copy(4).start()
     c_take(0, sent, 0)
     t_take(0, sent, 0)
+    t_start(0, sent, 2)
     c_take(0, sent, 1)
     c_take(0, sent, 2)
-    for i in (1, 4):
-        table_copy(i).wait()
-        push(i, cots[i], cst, cot_o, s_cy)
+    cot_push(1, 4)
     t_take(0, sent, 1)
     b_take(1, sent)
     table_copy(2).start()
     table_copy(5).start()
     c_take(1, sent, 0)
+    t_take(1, sent, 0)
+    queries(0)
     c_take(1, sent, 1)
+    c_take(1, sent, 2)
+    cot_push(2, 5)
     t_take(0, sent, 2)
-    c_take(1, sent, 2)
-    for i in (2, 5):
-        table_copy(i).wait()
-        push(i, cots[i], cst, cot_o, s_cy)
-    t_take(1, sent, 0)
     b_take(2, sent)
     table_copy(3).start()
     table_copy(6).start()
     c_take(2, sent, 0)
     t_take(1, sent, 1)
+    queries(1)
     c_take(2, sent, 1)
+    c_take(2, sent, 2)
     t_take(1, sent, 2)
-
-    parts = [(tok, x), (t_r, lax.rem(x + 3, 4)), (t_l, lax.rem(x + 1, 4)), (t_f, lax.rem(x + 2, 4))]
-    for half in range(2):
-        acc = None
-        for buf, p in parts:
-            rows = buf[half * 3:half * 3 + 3].reshape(192, 512)
-            term = jnp.dot(rows, wq[p], preferred_element_type=f32)
-            acc = term if acc is None else acc + term
-        low = acc.astype(bf16)
-        qlow[half * 192:half * 192 + 192, :] = low
-        wide = low.astype(f32)
-        norm = lax.rsqrt(jnp.mean(wide * wide, axis=-1, keepdims=True) + NORM_FLOOR)
-        q_own[half * 3:half * 3 + 3] = (wide * norm).astype(bf16).reshape(3, 64, 256)
-        if half == 0:
-            c_take(2, sent, 2)
-    for b in range(6):
-        acc = None
-        for buf, p in parts:
-            term = lax.dot_general(gw[:, pl.ds(pl.multiple_of(p * 512, 512), 512)], buf[b], CONTRACT_LAST, preferred_element_type=f32)
-            acc = term if acc is None else acc + term
-        gate[b, :, 0:64] = jnp.broadcast_to(jax.nn.sigmoid(acc[0:1]), (8, 64))
-        gate[b, :, 64:128] = jnp.zeros((8, 64), f32)
+    queries(2)
     g_start(0, sent)
-    q_start(0, sent)
     wcp = []
     for i in range(1, 4):
         to, frm = lax.rem(x + i, 4), lax.rem(x + 4 - i, 4)
@@ -443,24 +453,26 @@
         dst[mine] = src[mine]
         wcp += cps
 
-    for i in (3, 6):
-        table_copy(i).wait()
-        push(i, cots[i], cst, cot_o, s_cy)
+    q_take(0, sent, 0)
+    cot_push(3, 6)
+    q_take(0, sent, 1)
     b_take(3, sent)
     table_copy(7).start()
     c_take(3, sent)
     push(0, q_own, qst, q_o, s_qy)
-    table_copy(7).wait()
-    push(7, c_f, cst, cot_o, s_cy)
-    for k, some in ((0, (1, 4)), (1, (2, 5)), (2, (3, 6)), (3, (7,))):
-        g_take(k, sent)
-        for ch in range(3):
-            q_take(k, sent, ch)
-            if ch < 2 and k < 3:
-                fill(1)
+    q_take(0, sent, 2)
+    cot_push(7)
+    g_take(0, sent)
+    for k, some in ((1, (1, 4)), (2, (2, 5)), (3, (3, 6))):
+        q_take(k, sent, 0)
         for i in some:
             push(i, qs[i], qst, q_o, s_qy)
         fill(1)
+        q_take(k, sent, 1)
+        fill(1)
+        q_take(k, sent, 2)
+        g_take(k, sent)
+    push(7, q_f, qst, q_o, s_qy)
     left_half = lax.broadcasted_iota(jnp.int32, (8, 128), 1) < 64
 
     def side_for(i, j):
@@ -506,7 +518,7 @@
             slots, slots, sds((8, 8, 8, 128), f32), sds((8, 8, 128), i32),
             sds((384, 256), bf16), sds((6, 8, 128), f32), sds((1024, 256), bf16), sds((1024, 256), bf16),
             sds((1024, 256), bf16), sds((384, 256), f32), wide, wide, wide, sds((4, 1, 512), bf16)],
-        in_specs=[v] * 13 + [pl.BlockSpec(memory_space=pltpu.SMEM)],
+        in_specs=[v] * 5 + [pl.BlockSpec(memory_space=pl.ANY)] + [v] * 7 + [pl.BlockSpec(memory_space=pltpu.SMEM)],
         out_specs=[v] * 14,
         scratch_shapes=[
             pltpu.VMEM((6, 64, 512), bf16), pltpu.VMEM((6, 64, 512), bf16), pltpu.VMEM((6, 64, 512), bf16),
@@ -517,11 +529,11 @@
             [pltpu.VMEM((2, 8, 128), i32)] * 3, [pltpu.VMEM((2, 8, 128), i32)] * 3, pltpu.VMEM((2, 8, 128), i32),
             pltpu.SMEM((8, 8, 128), i32),
             pltpu.VMEM((7, 8, 64, 256), bf16), pltpu.VMEM((7, 8, 64, 256), bf16), pltpu.VMEM((7, 8, 8, 128), f32),
-            pltpu.VMEM((12, 64, 128), f32), pltpu.VMEM((12, 64, 128), bf16), pltpu.VMEM((12, 64, 64), bf16),
+            pltpu.VMEM((1024, 2048), bf16), pltpu.VMEM((12, 64, 128), f32), pltpu.VMEM((12, 64, 128), bf16), pltpu.VMEM((12, 64, 64), bf16),
             pltpu.VMEM((12, 64, 128), bf16), pltpu.VMEM((12, 64, 128), bf16), pltpu.VMEM((12, 8, 128), f32),
             pltpu.VMEM((2, 128, 128), f32),
             dma((2, 2, 6)), dma((2, 2, 12)), dma((2, 2, 12)), dma((2, 2, 4)), dma((2, 2, 4)), dma((8,)),
-            dma((2, 8, 7)), dma((2, 8, 7)), dma((2, 7)),
+            dma((2, 8, 7)), dma((2, 8, 7)), dma((2, 7)), dma,
             dma((2, 3)), dma((2, 3)), dma((2, 3)), dma((2, 3))],
         compiler_params=pltpu.CompilerParams(
             collective_id=cid, has_side_effects=True, vmem_limit_bytes=60 * 1024 * 1024),
@@ -629,10 +641,12 @@
 
 
 def tail_kernel(
-    kg, vg, pas, wkc, wvc, rows_o, w_o, kg4, vg4, acc, w, wc, wcs, wy, wys, wz, s_k, s_v, s_c, s_y, s_z):
+    kg, vg, pas_hbm, wkc, wvc, rows_o, w_o, kg4, vg4, acc, pas, w, wc, wcs, wy, s_k, s_v, s_c, s_y, s_p):
     f32, bf16 = jnp.float32, jnp.bfloat16
+    store = pltpu.make_async_copy(pas_hbm, pas, s_p)
+    store.start()
     barrier = pltpu.get_barrier_semaphore()
-    peers = ring_peers(ring("tp")) + a2a_peers(a2a("st_2")) + a2a_peers(a2a("st_1")) + a2a_peers(a2a("st_0"))
+    peers = ring_peers(ring("tp")) + a2a_peers(a2a("st_2")) + a2a_peers(a2a("st_1"))
     for p in peers:
         pl.semaphore_signal(barrier, inc=1, device_id=p, device_id_type=MESH_ID)
     pl.semaphore_wait(barrier, len(peers))
@@ -661,6 +675,7 @@
             else:
                 acc[rows, :] = part
 
+    store.wait()
     for t in range(8):
         cols = pl.ds(t * 256, 256)
         part = lax.dot_general(pas[:, cols], kg[...], CONTRACT_FIRST, preferred_element_type=f32)
@@ -689,27 +704,16 @@
                 sent.append(cp)
     for h in (lax.rem(x + 1, 4), lax.rem(x + 3, 4)):
         add_head(lambda r: kg4[h, r], lambda r: vg4[h, r], h, False, False)
-    for _, r in ycp:
-        r.wait_recv()
-    for k in range(8):
-        wys[k] = (wy[0, k] + wy[1, k]) + (wy[2, k] + wy[3, k])
-    zm, zcp = a2a_copies(a2a("st_0"), wys, wz, s_z)
-    for cp, _ in zcp:
-        cp.start()
-        sent.append(cp)
-    wz[zm] = wys[zm]
     for ch in range(2):
         for c, a in rings:
             for d in range(2):
                 a(1, d, ch).wait_recv()
     far = lax.rem(x + 2, 4)
     add_head(lambda r: kg4[far, r], lambda r: vg4[far, r], far, False, True)
-    for _, r in zcp:
+    for _, r in ycp:
         r.wait_recv()
-    total = wz[0]
-    for k in range(1, 8):
-        total = total + wz[k]
-    w_o[...] = total
+    for k in range(8):
+        w_o[k] = (wy[0, k] + wy[1, k]) + (wy[2, k] + wy[3, k])
     for cp in sent:
         cp.wait_send()
 
@@ -720,15 +724,15 @@
     dma = pltpu.SemaphoreType.DMA
     return pl.pallas_call(
         tail_kernel,
-        out_shape=[jax.ShapeDtypeStruct((1024, 512), bf16), jax.ShapeDtypeStruct((32, 256), f32)],
-        in_specs=[v] * 5,
+        out_shape=[jax.ShapeDtypeStruct((1024, 512), bf16), jax.ShapeDtypeStruct((8, 32, 256), f32)],
+        in_specs=[v, v, pl.BlockSpec(memory_space=pl.ANY), v, v],
         out_specs=[v] * 2,
         scratch_shapes=[
             pltpu.VMEM((4, 1024, 256), bf16), pltpu.VMEM((4, 1024, 256), bf16), pltpu.VMEM((1024, 512), f32),
+            pltpu.VMEM((1024, 2048), bf16),
             pltpu.VMEM((8, 4, 2, 32, 256), f32), pltpu.VMEM((8, 4, 32, 256), f32),
             pltpu.VMEM((4, 8, 32, 256), f32), pltpu.VMEM((4, 8, 32, 256), f32),
-            pltpu.VMEM((8, 32, 256), f32), pltpu.VMEM((8, 32, 256), f32),
-            dma((2, 2, 4)), dma((2, 2, 4)), dma((2,)), dma((2, 3)), dma((2, 7))],
+            dma((2, 2, 4)), dma((2, 2, 4)), dma((2,)), dma((2, 3)), dma],
         compiler_params=pltpu.CompilerParams(
             collective_id=cid, has_side_effects=True, vmem_limit_bytes=56 * 1024 * 1024),
     )(kg, vg, pas, wkc, wvc)
@@ -796,15 +800,16 @@
 
     key_term = (scale * jnp.einsum("sij,sid->sjd", score_grad, q_here, preferred_element_type=f32)).astype(bf16)
     value_term = jnp.einsum("sij,sid->sjd", probs_low, g_here, preferred_element_type=f32).astype(bf16)
-    onehot = ((loc[None, :] == jnp.arange(16, dtype=jnp.int32)[:, None]) & used[None, :]).astype(bf16)
-    key_grad_hat = jnp.dot(onehot, key_term.reshape(64, -1), preferred_element_type=f32).reshape(1024, 256)
-    value_grad = jnp.dot(onehot, value_term.reshape(64, -1), preferred_element_type=f32).reshape(1024, 256)
+    onehot = ((loc[:, None] == jnp.arange(16, dtype=jnp.int32)[None, :]) & used[:, None]).astype(bf16)
+    key_grad_hat = jnp.einsum("sp,sjd->pjd", onehot, key_term, preferred_element_type=f32)
+    value_grad = jnp.einsum("sp,sjd->pjd", onehot, value_term, preferred_element_type=f32)
+    key_grad_hat, value_grad = key_grad_hat.reshape(1024, 256), value_grad.reshape(1024, 256)
     key_grad = (
         key_scale * key_grad_hat
         - key_scale**3 * key_float * jnp.mean(key_float * key_grad_hat, axis=-1, keepdims=True)
     ).astype(bf16)
     value_grad_low = value_grad.astype(bf16)
-    passage_grad, key_weight_grad = tail(key_grad, value_grad_low, flat_rows, wk_cols, wv_cols, 3)
+    passage_grad, weight_term = tail(key_grad, value_grad_low, flat_rows, wk_cols, wv_cols, 3)
     passage_grad = passage_grad.reshape(16, 64, 512)
 
     qhat_grad = jnp.sum(q_back[owner].astype(f32).reshape(6, 4, 64, 256), axis=1).reshape(384, 256)
@@ -814,7 +819,9 @@
         query_scale * qhat_grad
         - query_scale**3 * query_float * jnp.mean(query_float * qhat_grad, axis=-1, keepdims=True)
     ).astype(bf16)
-    qg4, gg4 = comm([ring("tp", 2), ring("tp")], [query_grad, rows_of(gate_grad)], 4)
+    qg4, gg4, w_z = comm(
+        [ring("tp", 2), ring("tp"), a2a("st_0")], [query_grad, rows_of(gate_grad), weight_term], 4)
+    key_weight_grad = jnp.sum(w_z, axis=0)
     gg4 = gg4[:, :3].reshape(4, 384)
     token_part = (
         jnp.einsum("htd,hed->hte", qg4, wq_cols, preferred_element_type=f32)

time: 209 us -> 206 us (0.986)
  local copies, waits for them, and re-layouts: 21.9 us -> 17.6 us
    unnamed x44 -> x39, local copies, waits for them, and re-layouts: 7.67 us -> 4.06 us
    pallas_call x1, Pallas kernels: 46.9 us -> 43.5 us  [tail(): pl.pallas_call(tail_kernel, out_shape=[jax.ShapeDtypeStruct((1024, 512),...]
    pallas_call x1, Pallas kernels: 14.9 us -> 17.9 us  [comm(): pl.pallas_call(functools.partial(comm_kernel, jobs), out_shape=outs, in_s...]
  transfers between devices with their start and end apart: 1 -> 1, of which waited for: 0 -> 0; matrix products, arithmetic and copies ran while one was open for 6% -> 5% of each run, Pallas kernels for 22% -> 21%
where the time goes in v4:
time: 206 us; the launch traced here: 205 us
  Pallas kernels  156 us (76%)
  local copies, waits for them, and re-layouts  17.6 us (9%)
  matrix products  14.4 us (7%)
  other arithmetic  9.22 us (4%)
  starting transfers between devices  7.41 us (4%)
    pallas_call x1, Pallas kernels, forward(): pl.pallas_call(forward_kernel, out_shape=[slots, slots, sds((8, 8, 8, 128...  71.2 us
    pallas_call x1, Pallas kernels, tail(): pl.pallas_call(tail_kernel, out_shape=[jax.ShapeDtypeStruct((1024, 512),...  43.5 us
    pallas_call x1, Pallas kernels, stats_exchange(): pl.pallas_call(stats_kernel, out_shape=[jax.ShapeDtypeStruct(x.shape, f),...  23 us
    pallas_call x1, Pallas kernels, comm(): pl.pallas_call(functools.partial(comm_kernel, jobs), out_shape=outs, in_s...  17.9 us
    all_to_all x1, starting transfers between devices, body(): q_back = lax.all_to_all(q_part, ST, split_axis=0, concat_axis=0, tiled=True)  7.41 us
  transfers between devices with their start and end apart: 1, of which 0 were waited for; matrix products, arithmetic and copies ran while one was open for 5% of the time, Pallas kernels for 21%

profile of v4, /device:TPU:2, one launch (start us, length us, event | category | flops | bytes accessed | tf_op | source)
XLA Modules:
  0.0 205.2 jit_solution(4031080247109070029)
XLA Ops:
  0.6 0.8 copy.33
  2.4 71.2 %shard_map.157 = (bf16[8,8,64,256]{3,2,1,0:T(8,128)(2,1)}, bf16[8,8,64,256]{3,2,1,0:T(8,128)(2,1)}, f32[8,8,8,128]{3,2,1,0:T(8,128)}, s32[8,8,128]{2,1,0:T(8,128...) custom-call(bf16[6,64,512]{2,1,0:T(8,128)(2,1)} %bitcast.87, ...), custom_call_target="tpu_custom_call" | custom-call | tf_op jit(solution)/shard_map/pallas_call | solution.py:515
  73.5 1.0 slice.30
  74.7 1.8 gather_fusion.1
  76.5 2.0 gather_fusion
  78.5 2.4 %fusion.4 = f32[64,64,64]{1,2,0:T(8,128)S(1)} fusion(bf16[64,64,256]{2,1,0:T(8,128)(2,1)S(1)} %gather_fusion.1, bf16[64,64,256]{2,1,0:T(8,128)(2,1)} %bitcast.73, f32[64,64]{1,0:T(8,128)S(1)} %bitcast.89), kind=kOutput, calls=%fused_computation.17 | convolution fusion | flops 137363456 | bytes 5259264 | tf_op jit(solution)/shard_map/sid,sjd->sij/dot_general | solution.py:780
  81.4 0.9 fusion.41
  82.3 1.0 copy-done.5
  83.3 0.7 multiply_reduce_fusion
  84.0 0.8 slice.33
  84.9 0.7 maximum_bitcast_fusion.x_ref
  85.6 0.9 broadcast_in_dim.87.m_ref
  86.5 23.0 %shard_map.158 = (f32[8,8,256]{2,1,0:T(8,128)}, f32[6,8,256]{2,1,0:T(8,128)}) custom-call(f32[8,8,256]{2,1,0:T(8,128)} %maximum_bitcast_fusion.x_ref, f32[8,6,8,256]{3,2,1,0:T(8,128)} %broadcast_in_dim.87.m_ref), custom_call_target="tpu_custom_call" | custom-call | tf_op jit(solution)/shard_map/pallas_call | solution.py:630
  109.5 0.9 slice_select_fusion.1
  110.5 2.8 %multiply_convert_fusion.3 = bf16[64,64,64]{1,2,0:T(8,128)(2,1)S(1)} fusion(f32[64,64,64]{1,2,0:T(8,128)} %copy-done.2, f32[64,64]{1,0:T(8,128)S(1)} %get-tuple-element.54, f32[64,64]{1,0:T(8,128)S(1)} %get-tuple-element.53, f32[64,64,64]{1,2,0:T(8,128)} %copy-done, pred[64]{0:T(512)(128)(4,1)S(1)} %compare_bitcast_fusion), kind=kLoop, calls=%fused_computation.11 | loop fusion | flops 1310720 | bytes 2654272 | tf_op jit(solution)/shard_map/convert_element_type | solution.py:797
  113.3 2.1 %multiply_convert_fusion.1 = bf16[64,64,256]{2,1,0:T(8,128)(2,1)} fusion(bf16[64,64,64]{1,2,0:T(8,128)(2,1)S(1)} %multiply_convert_fusion.3, bf16[64,64,256]{2,1,0:T(8,128)(2,1)S(1)} %copy-done.4), kind=kOutput, calls=%fused_computation.4 | convolution fusion | flops 136314880 | bytes 4718592 | tf_op jit(solution)/shard_map/sij,sjd->sid/dot_general | solution.py:798
  115.4 7.4 %all-to-all-start = ((bf16[64,64,256]{2,1,0:T(8,128)(2,1)}), bf16[64,64,256]{2,1,0:T(8,128)(2,1)}, u32[]{:S(2)}, u32[]{:S(2)}) async-start(bf16[64,64,256]{2,1,0:T(8,128)(2,1)} %multiply_convert_fusion.1), calls=%async_computation | async-start | bytes 4194304 | tf_op jit(solution)/shard_map/all_to_all | solution.py:799
  122.9 2.4 %convolution_convert_fusion = bf16[64,64,256]{2,1,0:T(8,128)(2,1)S(1)} fusion(bf16[64,64,256]{2,1,0:T(8,128)(2,1)} %bitcast.74, f32[64,64]{1,0:T(8,128)S(1)} %bitcast.90, f32[64,64,64]{1,2,0:T(8,128)S(1)} %copy-done.1, f32[64,64]{1,0:T(8,128)S(1)} %get-tuple-element.53, pred[64]{0:T(512)(128)(4,1)S(1)} %compare_bitcast_fusion), kind=kOutput, calls=%fused_computation.16 | convolution fusion | flops 139198464 | bytes 5275712 | tf_op jit(solution)/shard_map/sij,sid->sjd/dot_general | solution.py:802
  125.4 1.2 fusion.6
  126.6 1.0 copy.41
  128.3 1.2 fusion.2
  130.1 0.8 constant_dynamic-slice_fusion
  131.1 0.8 slice_reduce_fusion
  132.3 1.3 fusion.12.kg
  133.5 43.5 %shard_map.159 = (bf16[1024,512]{1,0:T(8,128)(2,1)}, f32[8,32,256]{2,1,0:T(8,128)}) custom-call(bf16[1024,256]{1,0:T(8,128)(2,1)} %fusion.12.kg, bf16[1024,256]{1,0:T(8,128)(2,1)} %bitcast.81, bf16[1024,2048]{1,0:T(8,128)(2,1)} %bitcast.72, bf16[4,512,256]{2,1,0:T(8,128)(2,1)} %get-tuple-element.36.wkc, bf16[4,512,256]{2,1,0:T(8,128)(2,1)} %get-tuple-element.37.wvc), custom_call_target="tpu_custom_call" | custom-call | tf_op jit(solution)/shard_map/pallas_call | solution.py:725
  177.1 2.3 %gather_fusion.2 = bf16[24,64,256]{2,1,0:T(8,128)(2,1)S(1)} fusion(bf16[64,64,256]{2,1,0:T(8,128)(2,1)} %all-to-all-done, s32[1024]{0:T(1024)S(1)} %pad_clamp_fusion), kind=kCustom, calls=%fused_computation.2 | custom fusion | bytes 1572960 | tf_op jit(solution)/shard_map/gather | solution.py:815
  180.5 0.9 fusion.18.refs_0_
  181.4 17.9 %shard_map.160 = (bf16[4,384,256]{2,1,0:T(8,128)(2,1)}, f32[4,16,128]{2,1,0:T(8,128)}, f32[8,32,256]{2,1,0:T(8,128)}) custom-call(bf16[384,256]{1,0:T(8,128)(2,1)} %fusion.18.refs_0_, f32[16,128]{1,0:T(8,128)} %pad.9.refs_1_, f32[8,32,256]{2,1,0:T(8,128)} %get-tuple-element.38.refs_2_), custom_call_target="tpu_custom_call" | custom-call | tf_op jit(solution)/shard_map/pallas_call | solution.py:157
  199.3 0.7 slice_bitcast_fusion
  200.0 1.6 reduce_sum.125
  201.6 2.7 %fusion.5 = bf16[384,512]{1,0:T(8,128)(2,1)} fusion(f32[4,512]{1,0:T(4,128)S(1)} %bitcast.94, f32[4,384]{1,0:T(4,128)S(1)} %bitcast.95, bf16[4,384,256]{2,1,0:T(8,128)(2,1)} %get-tuple-element.39, bf16[4,512,256]{2,1,0:T(8,128)(2,1)S(1)} %copy-done.15), kind=kOutput, calls=%fused_computation.22 | convolution fusion | flops 405602304 | bytes 2242560 | tf_op jit(solution)/shard_map/htd,hed->hte/dot_general | solution.py:827
  204.3 1.0 copy.60
  (67 shorter events, 4.7 us)
Async XLA Ops:
  74.7 1.8 copy-start.6
  78.5 2.4 %copy-start.3 = (bf16[64,64,256]{2,1,0:T(8,128)(2,1)S(1)}, bf16[64,64,256]{2,1,0:T(8,128)(2,1)}, u32[]{:S(2)}) copy-start(bf16[64,64,256]{2,1,0:T(8,128)(2,1)} %gather_fusion) | copy-start | bytes 6291460
  78.5 2.9 %copy-start.7 = (bf16[8,8,64,256]{3,2,1,0:T(8,128)(2,1)S(1)}, bf16[8,8,64,256]{3,2,1,0:T(8,128)(2,1)}, u32[]{:S(2)}) copy-start(bf16[8,8,64,256]{3,2,1,0:T(8,128)(2,1)} %get-tuple-element.26) | copy-start | bytes 6291460
  81.0 1.3 copy-start.2
  81.4 1.9 copy-start.5
  82.3 1.7 copy-start
  110.5 2.9 %copy-start.4 = (bf16[64,64,256]{2,1,0:T(8,128)(2,1)S(1)}, bf16[64,64,256]{2,1,0:T(8,128)(2,1)}, u32[]{:S(2)}) copy-start(bf16[64,64,256]{2,1,0:T(8,128)(2,1)} %gather_fusion) | copy-start | bytes 6291460
  115.4 7.5 %copy-start.1 = (f32[64,64,64]{1,2,0:T(8,128)S(1)}, f32[64,64,64]{1,2,0:T(8,128)}, u32[]{:S(2)}) copy-start(f32[64,64,64]{1,2,0:T(8,128)} %copy-done) | copy-start | bytes 3145732
  115.4 61.7 %all-to-all-start = ((bf16[64,64,256]{2,1,0:T(8,128)(2,1)}), bf16[64,64,256]{2,1,0:T(8,128)(2,1)}, u32[]{:S(2)}, u32[]{:S(2)}) async-start(bf16[64,64,256]{2,1,0:T(8,128)(2,1)} %multiply_convert_fusion.1), calls=%async_computation | async-start | bytes 4194304 | tf_op jit(solution)/shard_map/all_to_all | solution.py:799
  125.4 2.2 %copy-start.8 = (bf16[8,8,64,256]{3,2,1,0:T(8,128)(2,1)S(1)}, bf16[8,8,64,256]{3,2,1,0:T(8,128)(2,1)}, u32[]{:S(2)}) copy-start(bf16[8,8,64,256]{3,2,1,0:T(8,128)(2,1)} %get-tuple-element.26) | copy-start | bytes 6291460
  128.3 3.6 %copy-start.14 = (bf16[4,1,512]{2,1,0:T(2,128)(2,1)S(1)}, bf16[4,1,512]{2,1,0:T(2,128)(2,1)}, u32[]{:S(2)}) copy-start(bf16[4,1,512]{2,1,0:T(2,128)(2,1)} %get-tuple-element.42) | copy-start | bytes 12292
  128.3 3.6 %copy-start.9 = (bf16[1024,256]{1,0:T(8,128)(2,1)S(1)}, bf16[1024,256]{1,0:T(8,128)(2,1)}, u32[]{:S(2)}) copy-start(bf16[1024,256]{1,0:T(8,128)(2,1)} %get-tuple-element.35) | copy-start | bytes 1572868
  177.1 2.5 %copy-start.11 = (bf16[384,256]{1,0:T(8,128)(2,1)S(1)}, bf16[384,256]{1,0:T(8,128)(2,1)}, u32[]{:S(2)}) copy-start(bf16[384,256]{1,0:T(8,128)(2,1)} %get-tuple-element.24) | copy-start | bytes 589828
  177.1 2.5 %copy-start.12 = (bf16[384,256]{1,0:T(8,128)(2,1)S(1)}, bf16[384,256]{1,0:T(8,128)(2,1)}, u32[]{:S(2)}) copy-start(bf16[384,256]{1,0:T(8,128)(2,1)} %param.15) | copy-start | bytes 589828
  177.1 2.5 %copy-start.13 = (f32[384,256]{1,0:T(8,128)S(1)}, f32[384,256]{1,0:T(8,128)}, u32[]{:S(2)}) copy-start(f32[384,256]{1,0:T(8,128)} %get-tuple-element.33) | copy-start | bytes 1179652
  179.4 22.2 %copy-start.15 = (bf16[4,512,256]{2,1,0:T(8,128)(2,1)S(1)}, bf16[4,512,256]{2,1,0:T(8,128)(2,1)}, u32[]{:S(2)}) copy-start(bf16[4,512,256]{2,1,0:T(8,128)(2,1)} %get-tuple-element.40) | copy-start | bytes 3145732
  201.6 2.7 %copy-start.10 = (bf16[1024,512]{1,0:T(8,128)(2,1)S(1)}, bf16[1024,512]{1,0:T(8,128)(2,1)}, u32[]{:S(2)}) copy-start(bf16[1024,512]{1,0:T(8,128)(2,1)} %get-tuple-element.43) | copy-start | bytes 3145732

commit v5 on v4

--- a/solution.py
+++ b/solution.py
@@ -302,6 +302,7 @@
         pl.semaphore_signal(barrier, inc=1, device_id=p, device_id_type=MESH_ID)
     pl.semaphore_wait(barrier, len(peers))
     sent = []
+    kept = []
     b_start, b_take = near_ring("st_0", tab, b_r, b_l, b_f, s_b, 1)
     c_start, c_take = near_ring("st_0", cot, c_r, c_l, c_f, s_c, 3)
     t_start, t_take = near_ring("tp", tok, [t_r], [t_l], t_f, s_t, 3)
@@ -328,13 +329,16 @@
         zr = origins[i]
         for s in range(7):
             stage[s, zr] = buf[block_for(i, dsts[s][0])]
-        out[zr, my_yc] = buf[block_for(i, my_yc)]
+        stage[7, zr] = buf[block_for(i, my_yc)]
         for s in range(7):
             cp = pltpu.make_async_remote_copy(
                 src_ref=stage.at[s, zr], dst_ref=out.at[zr, my_yc], send_sem=sems.at[0, i, s],
                 recv_sem=sems.at[1, i, s], device_id=dsts[s][1], device_id_type=MESH_ID)
             cp.start()
             sent.append(cp)
+        cp = pltpu.make_async_copy(stage.at[7, zr], out.at[zr, my_yc], sems.at[0, i, 7])
+        cp.start()
+        kept.append(cp)
 
     def pulled(out, sems):
         for i in range(8):
@@ -450,7 +454,9 @@
         for cp, _ in cps:
             cp.start()
             sent.append(cp)
-        dst[mine] = src[mine]
+        cp = pltpu.make_async_copy(src.at[mine], dst.at[mine], sem.at[0, 3])
+        cp.start()
+        kept.append(cp)
         wcp += cps
 
     q_take(0, sent, 0)
@@ -503,6 +509,8 @@
     pulled(q_o, s_qy)
     for cp in sent:
         cp.wait_send()
+    for cp in kept:
+        cp.wait()
 
 
 def forward(ins, cid):
@@ -510,6 +518,7 @@
     f32, bf16, i32 = jnp.float32, jnp.bfloat16, jnp.int32
     sds = jax.ShapeDtypeStruct
     dma = pltpu.SemaphoreType.DMA
+    far = pl.BlockSpec(memory_space=pl.ANY)
     slots = sds((8, 8, 64, 256), bf16)
     wide = sds((4, 512, 256), bf16)
     return pl.pallas_call(
@@ -519,7 +528,7 @@
             sds((384, 256), bf16), sds((6, 8, 128), f32), sds((1024, 256), bf16), sds((1024, 256), bf16),
             sds((1024, 256), bf16), sds((384, 256), f32), wide, wide, wide, sds((4, 1, 512), bf16)],
         in_specs=[v] * 5 + [pl.BlockSpec(memory_space=pl.ANY)] + [v] * 7 + [pl.BlockSpec(memory_space=pltpu.SMEM)],
-        out_specs=[v] * 14,
+        out_specs=[far, far] + [v] * 8 + [far] * 3 + [v],
         scratch_shapes=[
             pltpu.VMEM((6, 64, 512), bf16), pltpu.VMEM((6, 64, 512), bf16), pltpu.VMEM((6, 64, 512), bf16),
             [pltpu.VMEM((6, 64, 256), bf16)] * 3, [pltpu.VMEM((6, 64, 256), bf16)] * 3, pltpu.VMEM((6, 64, 256), bf16),
@@ -528,13 +537,13 @@
             [pltpu.VMEM((6, 8, 128), f32)] * 3, [pltpu.VMEM((6, 8, 128), f32)] * 3, pltpu.VMEM((6, 8, 128), f32),
             [pltpu.VMEM((2, 8, 128), i32)] * 3, [pltpu.VMEM((2, 8, 128), i32)] * 3, pltpu.VMEM((2, 8, 128), i32),
             pltpu.SMEM((8, 8, 128), i32),
-            pltpu.VMEM((7, 8, 64, 256), bf16), pltpu.VMEM((7, 8, 64, 256), bf16), pltpu.VMEM((7, 8, 8, 128), f32),
+            pltpu.VMEM((8, 8, 64, 256), bf16), pltpu.VMEM((8, 8, 64, 256), bf16), pltpu.VMEM((7, 8, 8, 128), f32),
             pltpu.VMEM((1024, 2048), bf16), pltpu.VMEM((12, 64, 128), f32), pltpu.VMEM((12, 64, 128), bf16), pltpu.VMEM((12, 64, 64), bf16),
             pltpu.VMEM((12, 64, 128), bf16), pltpu.VMEM((12, 64, 128), bf16), pltpu.VMEM((12, 8, 128), f32),
             pltpu.VMEM((2, 128, 128), f32),
             dma((2, 2, 6)), dma((2, 2, 12)), dma((2, 2, 12)), dma((2, 2, 4)), dma((2, 2, 4)), dma((8,)),
-            dma((2, 8, 7)), dma((2, 8, 7)), dma((2, 7)), dma,
-            dma((2, 3)), dma((2, 3)), dma((2, 3)), dma((2, 3))],
+            dma((2, 8, 8)), dma((2, 8, 8)), dma((2, 7)), dma,
+            dma((2, 4)), dma((2, 4)), dma((2, 4)), dma((2, 4))],
         compiler_params=pltpu.CompilerParams(
             collective_id=cid, has_side_effects=True, vmem_limit_bytes=60 * 1024 * 1024),
     )(*ins)

time: 206 us -> 204 us (level)
  no operation moved by 1% of the time
where the time goes in v5:
time: 204 us; the launch traced here: 203 us
  Pallas kernels  154 us (75%)
  local copies, waits for them, and re-layouts  17.6 us (9%)
  matrix products  14.4 us (7%)
  other arithmetic  9.22 us (5%)
  starting transfers between devices  7.13 us (3%)
    pallas_call x1, Pallas kernels, forward(): pl.pallas_call(forward_kernel, out_shape=[slots, slots, sds((8, 8, 8, 128...  69.5 us
    pallas_call x1, Pallas kernels, tail(): pl.pallas_call(tail_kernel, out_shape=[jax.ShapeDtypeStruct((1024, 512),...  43.5 us
    pallas_call x1, Pallas kernels, stats_exchange(): pl.pallas_call(stats_kernel, out_shape=[jax.ShapeDtypeStruct(x.shape, f),...  23.2 us
    pallas_call x1, Pallas kernels, comm(): pl.pallas_call(functools.partial(comm_kernel, jobs), out_shape=outs, in_s...  17.9 us
    all_to_all x1, starting transfers between devices, body(): q_back = lax.all_to_all(q_part, ST, split_axis=0, concat_axis=0, tiled=True)  7.13 us
  transfers between devices with their start and end apart: 1, of which 0 were waited for; matrix products, arithmetic and copies ran while one was open for 5% of the time, Pallas kernels for 21%

profile of v5, /device:TPU:2, one launch (start us, length us, event | category | flops | bytes accessed | tf_op | source)
XLA Modules:
  0.0 203.5 jit_solution(4641879050814158628)
XLA Ops:
  0.6 0.8 copy.33
  2.4 69.5 %shard_map.157 = (bf16[8,8,64,256]{3,2,1,0:T(8,128)(2,1)}, bf16[8,8,64,256]{3,2,1,0:T(8,128)(2,1)}, f32[8,8,8,128]{3,2,1,0:T(8,128)}, s32[8,8,128]{2,1,0:T(8,128...) custom-call(bf16[6,64,512]{2,1,0:T(8,128)(2,1)} %bitcast.87, ...), custom_call_target="tpu_custom_call" | custom-call | tf_op jit(solution)/shard_map/pallas_call | solution.py:524
  71.9 1.0 slice.30
  73.0 1.8 gather_fusion.1
  74.8 2.0 gather_fusion
  76.8 2.4 %fusion.4 = f32[64,64,64]{1,2,0:T(8,128)S(1)} fusion(bf16[64,64,256]{2,1,0:T(8,128)(2,1)S(1)} %gather_fusion.1, bf16[64,64,256]{2,1,0:T(8,128)(2,1)} %bitcast.73, f32[64,64]{1,0:T(8,128)S(1)} %bitcast.89), kind=kOutput, calls=%fused_computation.17 | convolution fusion | flops 137363456 | bytes 5259264 | tf_op jit(solution)/shard_map/sid,sjd->sij/dot_general | solution.py:789
  79.7 0.9 fusion.41
  80.6 1.0 copy-done.5
  81.6 0.7 multiply_reduce_fusion
  82.3 0.8 slice.33
  83.2 0.7 maximum_bitcast_fusion.x_ref
  83.9 0.9 broadcast_in_dim.87.m_ref
  84.8 23.2 %shard_map.158 = (f32[8,8,256]{2,1,0:T(8,128)}, f32[6,8,256]{2,1,0:T(8,128)}) custom-call(f32[8,8,256]{2,1,0:T(8,128)} %maximum_bitcast_fusion.x_ref, f32[8,6,8,256]{3,2,1,0:T(8,128)} %broadcast_in_dim.87.m_ref), custom_call_target="tpu_custom_call" | custom-call | tf_op jit(solution)/shard_map/pallas_call | solution.py:639
  108.0 0.9 slice_select_fusion.1
  109.0 2.8 %multiply_convert_fusion.3 = bf16[64,64,64]{1,2,0:T(8,128)(2,1)S(1)} fusion(f32[64,64,64]{1,2,0:T(8,128)} %copy-done.2, f32[64,64]{1,0:T(8,128)S(1)} %get-tuple-element.54, f32[64,64]{1,0:T(8,128)S(1)} %get-tuple-element.53, f32[64,64,64]{1,2,0:T(8,128)} %copy-done, pred[64]{0:T(512)(128)(4,1)S(1)} %compare_bitcast_fusion), kind=kLoop, calls=%fused_computation.11 | loop fusion | flops 1310720 | bytes 2654272 | tf_op jit(solution)/shard_map/convert_element_type | solution.py:806
  111.8 2.1 %multiply_convert_fusion.1 = bf16[64,64,256]{2,1,0:T(8,128)(2,1)} fusion(bf16[64,64,64]{1,2,0:T(8,128)(2,1)S(1)} %multiply_convert_fusion.3, bf16[64,64,256]{2,1,0:T(8,128)(2,1)S(1)} %copy-done.4), kind=kOutput, calls=%fused_computation.4 | convolution fusion | flops 136314880 | bytes 4718592 | tf_op jit(solution)/shard_map/sij,sjd->sid/dot_general | solution.py:807
  113.9 7.1 %all-to-all-start = ((bf16[64,64,256]{2,1,0:T(8,128)(2,1)}), bf16[64,64,256]{2,1,0:T(8,128)(2,1)}, u32[]{:S(2)}, u32[]{:S(2)}) async-start(bf16[64,64,256]{2,1,0:T(8,128)(2,1)} %multiply_convert_fusion.1), calls=%async_computation | async-start | bytes 4194304 | tf_op jit(solution)/shard_map/all_to_all | solution.py:808
  121.2 2.4 %convolution_convert_fusion = bf16[64,64,256]{2,1,0:T(8,128)(2,1)S(1)} fusion(bf16[64,64,256]{2,1,0:T(8,128)(2,1)} %bitcast.74, f32[64,64]{1,0:T(8,128)S(1)} %bitcast.90, f32[64,64,64]{1,2,0:T(8,128)S(1)} %copy-done.1, f32[64,64]{1,0:T(8,128)S(1)} %get-tuple-element.53, pred[64]{0:T(512)(128)(4,1)S(1)} %compare_bitcast_fusion), kind=kOutput, calls=%fused_computation.16 | convolution fusion | flops 139198464 | bytes 5275712 | tf_op jit(solution)/shard_map/sij,sid->sjd/dot_general | solution.py:811
  123.6 1.2 fusion.6
  124.8 1.0 copy.41
  126.5 1.2 fusion.2
  128.4 0.8 constant_dynamic-slice_fusion
  129.3 0.8 slice_reduce_fusion
  130.5 1.3 fusion.12.kg
  131.8 43.5 %shard_map.159 = (bf16[1024,512]{1,0:T(8,128)(2,1)}, f32[8,32,256]{2,1,0:T(8,128)}) custom-call(bf16[1024,256]{1,0:T(8,128)(2,1)} %fusion.12.kg, bf16[1024,256]{1,0:T(8,128)(2,1)} %bitcast.81, bf16[1024,2048]{1,0:T(8,128)(2,1)} %bitcast.72, bf16[4,512,256]{2,1,0:T(8,128)(2,1)} %get-tuple-element.36.wkc, bf16[4,512,256]{2,1,0:T(8,128)(2,1)} %get-tuple-element.37.wvc), custom_call_target="tpu_custom_call" | custom-call | tf_op jit(solution)/shard_map/pallas_call | solution.py:734
  175.4 2.3 %gather_fusion.2 = bf16[24,64,256]{2,1,0:T(8,128)(2,1)S(1)} fusion(bf16[64,64,256]{2,1,0:T(8,128)(2,1)} %all-to-all-done, s32[1024]{0:T(1024)S(1)} %pad_clamp_fusion), kind=kCustom, calls=%fused_computation.2 | custom fusion | bytes 1572960 | tf_op jit(solution)/shard_map/gather | solution.py:824
  178.7 0.9 fusion.18.refs_0_
  179.6 17.9 %shard_map.160 = (bf16[4,384,256]{2,1,0:T(8,128)(2,1)}, f32[4,16,128]{2,1,0:T(8,128)}, f32[8,32,256]{2,1,0:T(8,128)}) custom-call(bf16[384,256]{1,0:T(8,128)(2,1)} %fusion.18.refs_0_, f32[16,128]{1,0:T(8,128)} %pad.9.refs_1_, f32[8,32,256]{2,1,0:T(8,128)} %get-tuple-element.38.refs_2_), custom_call_target="tpu_custom_call" | custom-call | tf_op jit(solution)/shard_map/pallas_call | solution.py:157
  197.5 0.7 slice_bitcast_fusion
  198.3 1.6 reduce_sum.125
  199.8 2.7 %fusion.5 = bf16[384,512]{1,0:T(8,128)(2,1)} fusion(f32[4,512]{1,0:T(4,128)S(1)} %bitcast.94, f32[4,384]{1,0:T(4,128)S(1)} %bitcast.95, bf16[4,384,256]{2,1,0:T(8,128)(2,1)} %get-tuple-element.39, bf16[4,512,256]{2,1,0:T(8,128)(2,1)S(1)} %copy-done.15), kind=kOutput, calls=%fused_computation.22 | convolution fusion | flops 405602304 | bytes 2242560 | tf_op jit(solution)/shard_map/htd,hed->hte/dot_general | solution.py:836
  202.5 1.0 copy.60
  (67 shorter events, 4.7 us)
Async XLA Ops:
  73.0 1.8 copy-start.6
  76.8 2.4 %copy-start.3 = (bf16[64,64,256]{2,1,0:T(8,128)(2,1)S(1)}, bf16[64,64,256]{2,1,0:T(8,128)(2,1)}, u32[]{:S(2)}) copy-start(bf16[64,64,256]{2,1,0:T(8,128)(2,1)} %gather_fusion) | copy-start | bytes 6291460
  76.8 2.9 %copy-start.7 = (bf16[8,8,64,256]{3,2,1,0:T(8,128)(2,1)S(1)}, bf16[8,8,64,256]{3,2,1,0:T(8,128)(2,1)}, u32[]{:S(2)}) copy-start(bf16[8,8,64,256]{3,2,1,0:T(8,128)(2,1)} %get-tuple-element.26) | copy-start | bytes 6291460
  79.3 1.3 copy-start.2
  79.7 1.9 copy-start.5
  80.6 1.7 copy-start
  109.0 2.9 %copy-start.4 = (bf16[64,64,256]{2,1,0:T(8,128)(2,1)S(1)}, bf16[64,64,256]{2,1,0:T(8,128)(2,1)}, u32[]{:S(2)}) copy-start(bf16[64,64,256]{2,1,0:T(8,128)(2,1)} %gather_fusion) | copy-start | bytes 6291460
  113.9 7.2 %copy-start.1 = (f32[64,64,64]{1,2,0:T(8,128)S(1)}, f32[64,64,64]{1,2,0:T(8,128)}, u32[]{:S(2)}) copy-start(f32[64,64,64]{1,2,0:T(8,128)} %copy-done) | copy-start | bytes 3145732
  113.9 61.4 %all-to-all-start = ((bf16[64,64,256]{2,1,0:T(8,128)(2,1)}), bf16[64,64,256]{2,1,0:T(8,128)(2,1)}, u32[]{:S(2)}, u32[]{:S(2)}) async-start(bf16[64,64,256]{2,1,0:T(8,128)(2,1)} %multiply_convert_fusion.1), calls=%async_computation | async-start | bytes 4194304 | tf_op jit(solution)/shard_map/all_to_all | solution.py:808
  123.6 2.2 %copy-start.8 = (bf16[8,8,64,256]{3,2,1,0:T(8,128)(2,1)S(1)}, bf16[8,8,64,256]{3,2,1,0:T(8,128)(2,1)}, u32[]{:S(2)}) copy-start(bf16[8,8,64,256]{3,2,1,0:T(8,128)(2,1)} %get-tuple-element.26) | copy-start | bytes 6291460
  126.5 3.6 %copy-start.14 = (bf16[4,1,512]{2,1,0:T(2,128)(2,1)S(1)}, bf16[4,1,512]{2,1,0:T(2,128)(2,1)}, u32[]{:S(2)}) copy-start(bf16[4,1,512]{2,1,0:T(2,128)(2,1)} %get-tuple-element.42) | copy-start | bytes 12292
  126.5 3.6 %copy-start.9 = (bf16[1024,256]{1,0:T(8,128)(2,1)S(1)}, bf16[1024,256]{1,0:T(8,128)(2,1)}, u32[]{:S(2)}) copy-start(bf16[1024,256]{1,0:T(8,128)(2,1)} %get-tuple-element.35) | copy-start | bytes 1572868
  175.3 2.5 %copy-start.11 = (bf16[384,256]{1,0:T(8,128)(2,1)S(1)}, bf16[384,256]{1,0:T(8,128)(2,1)}, u32[]{:S(2)}) copy-start(bf16[384,256]{1,0:T(8,128)(2,1)} %get-tuple-element.24) | copy-start | bytes 589828
  175.3 2.5 %copy-start.12 = (bf16[384,256]{1,0:T(8,128)(2,1)S(1)}, bf16[384,256]{1,0:T(8,128)(2,1)}, u32[]{:S(2)}) copy-start(bf16[384,256]{1,0:T(8,128)(2,1)} %param.15) | copy-start | bytes 589828
  175.3 2.5 %copy-start.13 = (f32[384,256]{1,0:T(8,128)S(1)}, f32[384,256]{1,0:T(8,128)}, u32[]{:S(2)}) copy-start(f32[384,256]{1,0:T(8,128)} %get-tuple-element.33) | copy-start | bytes 1179652
  177.7 22.2 %copy-start.15 = (bf16[4,512,256]{2,1,0:T(8,128)(2,1)S(1)}, bf16[4,512,256]{2,1,0:T(8,128)(2,1)}, u32[]{:S(2)}) copy-start(bf16[4,512,256]{2,1,0:T(8,128)(2,1)} %get-tuple-element.40) | copy-start | bytes 3145732
  199.8 2.7 %copy-start.10 = (bf16[1024,512]{1,0:T(8,128)(2,1)S(1)}, bf16[1024,512]{1,0:T(8,128)(2,1)}, u32[]{:S(2)}) copy-start(bf16[1024,512]{1,0:T(8,128)(2,1)} %get-tuple-element.43) | copy-start | bytes 3145732
